TPU v7x, 32 devices: a whole 2x2x4 slice. The times are simulated.
32 devices in a mesh: dp: 4 (over y, x), kv: 4 (over z), tp: 2 (over core).
Axes of the slice: x: 2, y: 2, z: 4, core: 2. Of those that a mesh axis runs over, the one named last changes fastest.
Arguments:
- piece_rows: bfloat16 [256, 2048], P(('dp', 'kv')), parts along dimension 0, may hold values from -6 to 6
- decode_rows: bfloat16 [16, 2048], P(('dp', 'kv')), parts along dimension 0, may hold values from -6 to 6
- prompt_latent: bfloat16 [4096, 512], P(('dp', 'kv')), parts along dimension 0, may hold values from -512 to 512
- prompt_rope_key: bfloat16 [4096, 32], P(('dp', 'kv')), parts along dimension 0, may hold values from -6 to 6
- decode_latent: bfloat16 [16, 512, 512], P(('dp', 'kv')), parts along dimension 0, may hold values from -512 to 512
- decode_rope_key: bfloat16 [16, 512, 32], P(('dp', 'kv')), parts along dimension 0, may hold values from -6 to 6
- dec_lengths: int32 [16], P(('dp', 'kv')), parts along dimension 0, may hold values from 1 to 512, as said below
- w_qdown: bfloat16 [2048, 512], replicated, may hold values from -0.125 to 0.125
- q_gain: float32 [512], replicated, may hold values from 0.1 to 1.9
- w_qup: bfloat16 [512, 16, 96], P(None, 'tp'), may hold values from -0.25 to 0.25
- w_kvdown: bfloat16 [2048, 512], replicated, may hold values from -0.125 to 0.125
- w_krope: bfloat16 [2048, 32], replicated, may hold values from -0.125 to 0.125
- kv_gain: float32 [512], replicated, may hold values from 0.1 to 1.9
- w_kup: bfloat16 [512, 16, 64], P(None, 'tp'), may hold values from -0.25 to 0.25
- w_vup: bfloat16 [512, 16, 64], P(None, 'tp'), may hold values from -0.25 to 0.25
- w_out: bfloat16 [16, 64, 2048], P('tp'), may hold values from -0.1875 to 0.1875
Outputs:
- piece_out: bfloat16 [256, 2048], P(('dp', 'kv')), parts along dimension 0
- decode_out: bfloat16 [16, 2048], P(('dp', 'kv')), parts along dimension 0
- piece_latent: bfloat16 [256, 512], P(('dp', 'kv')), parts along dimension 0
- piece_rope: bfloat16 [256, 32], P(('dp', 'kv')), parts along dimension 0
- decode_new_latent: bfloat16 [16, 512], P(('dp', 'kv')), parts along dimension 0
- decode_new_rope: bfloat16 [16, 32], P(('dp', 'kv')), parts along dimension 0
There are 4 independent parts, one for each index of `dp`. A program takes and returns all parts, laid end to end along the dimension named above; an argument that names none is the same for every part. Nothing has to cross between parts.
Inputs may be any that keep to these rules, and one draw needn't show every extreme that they name: `dec_lengths`: each group of requests has some decoding sequence with exactly 512 cached rows.
All inputs are finite; a program needn't handle non-finite values.
Results may differ from a plain program's by a relative error of at most 0.03.
Values may be sent and summed in bfloat16 or wider, within the bound.
No kernel may reach another device: no remote copies, remote signals or barrier semaphores. Data moves between devices by JAX's collectives and lax.ppermute only.
A program may use at most 64 MiB of HBM per device.

v0:
```python
import jax
import jax.numpy as jnp
from jax import lax
from jax.sharding import PartitionSpec as P

NOPE_DIM = 64
ROPE_DIM = 32


def rms_scale(values, gain):
    return values * lax.rsqrt(jnp.mean(values * values, axis=-1, keepdims=True) + 1e-06) * gain


def rotate(values, positions):
    half = values.shape[-1] // 2
    inverse = jnp.power(10000.0, -jnp.arange(half, dtype=jnp.float32) * 2.0 / values.shape[-1])
    angle = positions.astype(jnp.float32)[:, None] * inverse[None, :]
    angle = angle.reshape((positions.shape[0],) + (1,) * (values.ndim - 2) + (half,))
    cosine, sine = (jnp.cos(angle), jnp.sin(angle))
    first, second = (values[..., :half], values[..., half:])
    return jnp.concatenate([first * cosine - second * sine, second * cosine + first * sine], -1)


def query_heads(latent_rows, w_qup, positions):
    full = jnp.einsum("rq,qhe->rhe", latent_rows, w_qup, preferred_element_type=jnp.float32)
    nope = full[..., :NOPE_DIM].astype(jnp.bfloat16)
    turned = rotate(full[..., NOPE_DIM:], positions).astype(jnp.bfloat16)
    return (nope, turned)


def decode_attend(
    dec_nope,
    dec_qrope,
    dec_latent,
    dec_rope,
    decode_latent,
    decode_rope_key,
    dec_lengths,
    w_kup,
    w_vup,
    scale,
):
    absorbed = jnp.einsum(
        "bhe,lhe->bhl", dec_nope, w_kup, preferred_element_type=jnp.float32
    ).astype(jnp.bfloat16)
    cached = (
        jnp.einsum("bhl,bcl->bhc", absorbed, decode_latent, preferred_element_type=jnp.float32)
        + jnp.einsum("bhe,bce->bhc", dec_qrope, decode_rope_key, preferred_element_type=jnp.float32)
    ) * scale
    valid = (
        jnp.arange(decode_latent.shape[1], dtype=jnp.int32)[None, None, :]
        < dec_lengths[:, None, None]
    )
    cached = jnp.where(valid, cached, -1e30)
    own = (
        jnp.einsum("bhl,bl->bh", absorbed, dec_latent, preferred_element_type=jnp.float32)
        + jnp.einsum("bhe,be->bh", dec_qrope, dec_rope, preferred_element_type=jnp.float32)
    ) * scale
    top = jnp.maximum(jnp.max(cached, axis=-1), own)
    cached_w = jnp.exp(cached - top[..., None])
    own_w = jnp.exp(own - top)
    denom = jnp.sum(cached_w, axis=-1) + own_w
    cached_p = (cached_w / denom[..., None]).astype(jnp.bfloat16)
    own_p = (own_w / denom).astype(jnp.bfloat16).astype(jnp.float32)
    context = (
        jnp.einsum("bhc,bcl->bhl", cached_p, decode_latent, preferred_element_type=jnp.float32)
        + own_p[..., None] * dec_latent.astype(jnp.float32)[:, None, :]
    ).astype(jnp.bfloat16)
    return jnp.einsum("bhl,lhv->bhv", context, w_vup, preferred_element_type=jnp.float32).astype(
        jnp.bfloat16
    )


def per_device(
    piece_rows,
    decode_rows,
    prompt_latent,
    prompt_rope_key,
    decode_latent,
    decode_rope_key,
    dec_lengths,
    w_qdown,
    q_gain,
    w_qup,
    w_kvdown,
    w_krope,
    kv_gain,
    w_kup,
    w_vup,
    w_out,
):
    scale = (NOPE_DIM + ROPE_DIM) ** (-0.5)
    shards = lax.axis_size("kv")
    index = lax.axis_index("kv")
    piece_dev = piece_rows.shape[0]
    cache_dev = prompt_latent.shape[0]
    piece_all = piece_dev * shards
    context_len = cache_dev * shards
    rows = jnp.concatenate([piece_rows, decode_rows], 0)
    query_latent = rms_scale(
        jnp.dot(rows, w_qdown, preferred_element_type=jnp.float32), q_gain
    ).astype(jnp.bfloat16)
    latent_new = rms_scale(
        jnp.dot(rows, w_kvdown, preferred_element_type=jnp.float32), kv_gain
    ).astype(jnp.bfloat16)
    piece_pos = context_len + index * piece_dev + jnp.arange(piece_dev, dtype=jnp.int32)
    positions = jnp.concatenate([piece_pos, dec_lengths])
    rope_new = rotate(jnp.dot(rows, w_krope, preferred_element_type=jnp.float32), positions).astype(
        jnp.bfloat16
    )
    block_rows = lax.all_gather(query_latent[:piece_dev], "kv", axis=0, tiled=True)
    block_pos = context_len + jnp.int32(0) + jnp.arange(block_rows.shape[0], dtype=jnp.int32)
    nope, turned = query_heads(block_rows, w_qup, block_pos)
    queries = jnp.concatenate([nope, turned], -1)
    dec_nope, dec_qrope = query_heads(query_latent[piece_dev:], w_qup, dec_lengths)
    dec_latent = latent_new[piece_dev:]
    dec_rope = rope_new[piece_dev:]
    key_latent = jnp.concatenate([prompt_latent, latent_new[:piece_dev]], 0)
    key_turned = jnp.concatenate([prompt_rope_key, rope_new[:piece_dev]], 0)
    key_pos = jnp.concatenate(
        [index * cache_dev + jnp.arange(cache_dev, dtype=jnp.int32), piece_pos]
    )
    key_nope = jnp.einsum(
        "sl,lhe->she", key_latent, w_kup, preferred_element_type=jnp.float32
    ).astype(jnp.bfloat16)
    values = jnp.einsum(
        "sl,lhe->she", key_latent, w_vup, preferred_element_type=jnp.float32
    ).astype(jnp.bfloat16)
    block = min(512, piece_all)
    count = piece_all // block

    def attend(number):
        start = number * block
        block_q = lax.dynamic_slice_in_dim(queries, start, block, 0)
        query_pos = context_len + start + jnp.arange(block, dtype=jnp.int32)
        scores = (
            jnp.einsum(
                "qhe,she->qhs",
                block_q[..., :NOPE_DIM],
                key_nope,
                preferred_element_type=jnp.float32,
            )
            + jnp.einsum(
                "qhe,se->qhs",
                block_q[..., NOPE_DIM:],
                key_turned,
                preferred_element_type=jnp.float32,
            )
        ) * scale
        scores = jnp.where(key_pos[None, None, :] <= query_pos[:, None, None], scores, -1e30)
        top = jnp.max(scores, axis=-1)
        weights = jnp.exp(scores - top[..., None])
        total = jnp.sum(weights, axis=-1)
        part = jnp.einsum(
            "qhs,she->qhe", weights.astype(jnp.bfloat16), values, preferred_element_type=jnp.float32
        )
        return (part.astype(jnp.bfloat16), top, total)

    parts, tops, totals = lax.map(attend, jnp.arange(count, dtype=jnp.int32))
    heads_dev = parts.shape[2]
    value_dim = parts.shape[3]
    parts = parts.reshape(shards, piece_dev, heads_dev * value_dim)
    tops = tops.reshape(shards, piece_dev, heads_dev)
    totals = totals.reshape(shards, piece_dev, heads_dev)
    got_parts, got_tops, got_totals = (
        lax.all_to_all(parts, "kv", split_axis=0, concat_axis=0, tiled=True),
        lax.all_to_all(
            tops.astype(jnp.bfloat16), "kv", split_axis=0, concat_axis=0, tiled=True
        ).astype(tops.dtype),
        lax.all_to_all(
            totals.astype(jnp.bfloat16), "kv", split_axis=0, concat_axis=0, tiled=True
        ).astype(totals.dtype),
    )
    best = jnp.max(got_tops, axis=0)
    factors = jnp.exp(got_tops - best[None])
    denom = jnp.sum(got_totals * factors, axis=0)
    got_parts = got_parts.reshape(shards, piece_dev, heads_dev, value_dim).astype(jnp.float32)
    piece_heads = (jnp.sum(got_parts * factors[..., None], axis=0) / denom[..., None]).astype(
        jnp.bfloat16
    )
    decode_heads = decode_attend(
        dec_nope,
        dec_qrope,
        dec_latent,
        dec_rope,
        decode_latent,
        decode_rope_key,
        dec_lengths,
        w_kup,
        w_vup,
        scale,
    )
    all_heads = jnp.concatenate([piece_heads, decode_heads], 0)
    term = jnp.einsum("rhv,hvd->rd", all_heads, w_out, preferred_element_type=jnp.float32)
    term = term.astype(jnp.bfloat16).astype(jnp.float32)
    summed = lax.psum(term.astype(jnp.bfloat16), "tp")
    return (
        summed[:piece_dev],
        summed[piece_dev:],
        latent_new[:piece_dev],
        rope_new[:piece_dev],
        dec_latent,
        dec_rope,
    )


def solution(mesh):
    in_specs = (
        P(("dp", "kv"), None),
        P(("dp", "kv"), None),
        P(("dp", "kv"), None),
        P(("dp", "kv"), None),
        P(("dp", "kv"), None, None),
        P(("dp", "kv"), None, None),
        P(("dp", "kv")),
        P(),
        P(),
        P(None, "tp", None),
        P(),
        P(),
        P(),
        P(None, "tp", None),
        P(None, "tp", None),
        P("tp", None, None),
    )
    out_specs = (
        P(("dp", "kv"), None),
        P(("dp", "kv"), None),
        P(("dp", "kv"), None),
        P(("dp", "kv"), None),
        P(("dp", "kv"), None),
        P(("dp", "kv"), None),
    )
    return jax.shard_map(
        per_device, mesh=mesh, in_specs=in_specs, out_specs=out_specs, check_vma=False
    )
```

profile of v0, /device:TPU:0, one launch (start us, length us, event | category | flops | bytes accessed | tf_op | source)
XLA Modules:
  0.0 92.9 jit_solution(17966602315402983139)
XLA Ops:
  8.1 0.8 constant_dynamic-update-slice_fusion.1
  9.2 0.7 constant_dynamic-update-slice_fusion
  9.9 1.1 %fusion.68 = f32[17,32]{1,0:T(8,128)S(1)} fusion(bf16[17,2048]{1,0:T(8,128)(2,1)S(1)} %constant_dynamic-update-slice_fusion, bf16[2048,32]{0,1:T(8,128)(2,1)} %param.27), kind=kOutput, calls=%fused_computation.120 | convolution fusion | flops 2228224 | bytes 202880 | tf_op jit(solution)/shard_map/dot_general | solution.py:108
  11.3 2.2 %multiply_reduce_fusion.2 = (f32[17]{0:T(128)S(1)}, f32[17,512]{1,0:T(8,128)S(1)}) fusion(bf16[17,2048]{1,0:T(8,128)(2,1)S(1)} %constant_dynamic-update-slice_fusion, bf16[2048,512]{1,0:T(8,128)(2,1)} %param.26), kind=kOutput, calls=%fused_computation.49 | convolution fusion | flops 35668976 | bytes 2201668 | tf_op jit(solution)/shard_map/dot_general | solution.py:104
  13.5 2.2 %multiply_reduce_fusion.1 = (f32[17]{0:T(128)S(1)}, f32[17,512]{1,0:T(8,128)S(1)}) fusion(bf16[17,2048]{1,0:T(8,128)(2,1)S(1)} %constant_dynamic-update-slice_fusion, bf16[2048,512]{1,0:T(8,128)(2,1)} %param.23), kind=kOutput, calls=%fused_computation.46 | convolution fusion | flops 35668976 | bytes 2201668 | tf_op jit(solution)/shard_map/dot_general | solution.py:101
  15.9 14.9 %all_gather.3 = bf16[64,512]{1,0:T(8,128)(2,1)S(1)} all-gather(bf16[16,512]{1,0:T(8,128)(2,1)S(1)} %slice.79), channel_id=1, replica_groups=mesh['dp'=4,'kv'=4,'tp'=2] {'kv'}, dimensions={0}, use_global_device_ids=true | all-gather | bytes 81920 | tf_op jit(solution)/shard_map/all_gather | solution.py:111
  30.9 0.4 fusion.26
  31.5 0.5 fusion.20
  32.8 0.6 copy.43
  33.4 4.7 %all-to-all-start.1 = ((bf16[4,16,8]{1,2,0:T(8,128)(2,1)}), bf16[4,16,8]{1,2,0:T(8,128)(2,1)S(1)}, u32[]{:S(2)}, u32[]{:S(2)}) async-start(bf16[4,16,8]{1,2,0:T(8,128)(2,1)} %copy.43), calls=%async_computation.1 | async-start | bytes 16384 | tf_op jit(solution)/shard_map/all_to_all | solution.py:167
  38.2 1.5 %fusion.53 = f32[1,8,96]{2,0,1:T(1,128)S(1)} fusion(bf16[512,8,96]{0,2,1:T(8,128)(2,1)} %param.25, bf16[17,512]{1,0:T(8,128)(2,1)S(1)} %multiply_convert_fusion), kind=kOutput, calls=%fused_computation.88 | convolution fusion | flops 786432 | bytes 791552 | tf_op jit(solution)/shard_map/rq,qhe->rhe/dot_general | solution.py:25
  40.2 1.3 %fusion.14 = f32[8,512]{1,0:T(8,128)S(1)} fusion(bf16[1,512,512]{2,1,0:T(8,128)(2,1)} %param.20, bf16[8,1,512]{2,1,0:T(2,128)(2,1)S(1)} %fusion.49), kind=kOutput, calls=%fused_computation.22 | convolution fusion | flops 4194304 | bytes 548864 | tf_op jit(solution)/shard_map/bhl,bcl->bhc/dot_general | solution.py:47
  42.2 1.3 %fusion.8 = bf16[8,512,1]{1,0,2:T(8,128)(2,1)S(1)} fusion(bf16[1,512,512]{2,1,0:T(8,128)(2,1)} %param.20, f32[8,512]{1,0:T(8,128)S(1)} %get-tuple-element.52, f32[512]{0:T(512)S(1)} %mul.290, f32[8]{0:T(128)S(1)} %get-tuple-element.44, f32[8]{0:T(128)S(1)} %get-tuple-element.43, f32[8]{0:T(128)S(1)} %get-tuple-element.53), kind=kOutput, calls=%fused_computation.13 | convolution fusion | flops 4218880 | bytes 551008 | tf_op jit(solution)/shard_map/bhc,bcl->bhl/dot_general | solution.py:66
  43.8 0.5 fusion.21
  45.0 0.6 copy.45
  45.7 5.1 %all-to-all-start.2 = ((bf16[4,16,8]{1,2,0:T(8,128)(2,1)}), bf16[4,16,8]{1,2,0:T(8,128)(2,1)S(1)}, u32[]{:S(2)}, u32[]{:S(2)}) async-start(bf16[4,16,8]{1,2,0:T(8,128)(2,1)} %copy.45), calls=%async_computation.2 | async-start | bytes 16384 | tf_op jit(solution)/shard_map/all_to_all | solution.py:170
  50.9 0.8 reshape.289
  51.7 4.6 %all-to-all-done.2 = bf16[4,16,8]{1,2,0:T(8,128)(2,1)S(1)} async-done(((bf16[4,16,8]{1,2,0:T(8,128)(2,1)}), bf16[4,16,8]{1,2,0:T(8,128)(2,1)S(1)}, u32[]{:S(2)}, u32[]{:S(2)}) %all-to-all-start.2) | async-done | bytes 1056 | tf_op jit(solution)/shard_map/all_to_all | solution.py:170
  56.3 3.3 %all-to-all-start = ((bf16[4,16,512]{2,1,0:T(8,128)(2,1)}), bf16[4,16,512]{2,1,0:T(8,128)(2,1)S(1)}, u32[]{:S(2)}, u32[]{:S(2)}) async-start(bf16[4,16,512]{2,1,0:T(8,128)(2,1)} %reshape.289), calls=%async_computation | async-start | bytes 131072 | tf_op jit(solution)/shard_map/all_to_all | solution.py:166
  60.0 5.3 %all-to-all-done = bf16[4,16,512]{2,1,0:T(8,128)(2,1)S(1)} async-done(((bf16[4,16,512]{2,1,0:T(8,128)(2,1)}), bf16[4,16,512]{2,1,0:T(8,128)(2,1)S(1)}, u32[]{:S(2)}, u32[]{:S(2)}) %all-to-all-start) | async-done | bytes 65568 | tf_op jit(solution)/shard_map/all_to_all | solution.py:166
  65.6 1.1 %fusion = bf16[17,2048]{1,0:T(8,128)(2,1)} fusion(bf16[8,64,2048]{2,1,0:T(8,128)(2,1)S(1)} %copy-done, bf16[1,8,64]{2,0,1:T(2,128)(2,1)S(1)} %copy.47, bf16[16,8,64]{2,0,1:T(8,128)(2,1)S(1)} %fusion.28), kind=kOutput, calls=%fused_computation.1 | convolution fusion | flops 35721216 | bytes 2184192 | tf_op jit(solution)/shard_map/rhv,hvd->rd/dot_general | solution.py:194
  66.7 16.5 %all-reduce.2.cloned.1.call-done = bf16[17,2048]{1,0:T(8,128)(2,1)} async-done(((bf16[17,2048]{1,0:T(8,128)(2,1)}), bf16[17,2048]{1,0:T(8,128)(2,1)}) %all-reduce.2.cloned.1.call-update) | async-done | bytes 69648 | tf_op jit(solution)/shard_map/psum | solution.py:196
  83.2 1.4 %slice.90 = bf16[1,2048]{1,0:T(2,128)(2,1)} slice(bf16[17,2048]{1,0:T(8,128)(2,1)} %all-reduce.2.cloned.1.call-done), slice={[16:17], [0:2048]} | slice | bytes 8192 | tf_op jit(solution)/shard_map/slice | solution.py:199
  84.6 1.5 %slice.89 = bf16[16,2048]{1,0:T(8,128)(2,1)} slice(bf16[17,2048]{1,0:T(8,128)(2,1)} %all-reduce.2.cloned.1.call-done), slice={[0:16], [0:2048]} | slice | bytes 131072 | tf_op jit(solution)/shard_map/slice | solution.py:198
  (84 shorter events, 4.9 us)
Async XLA Ops:
  7.2 58.4 %copy-start = (bf16[8,64,2048]{2,1,0:T(8,128)(2,1)S(1)}, bf16[8,64,2048]{2,1,0:T(8,128)(2,1)}, u32[]{:S(2)}) copy-start(bf16[8,64,2048]{2,1,0:T(8,128)(2,1)} %param.31) | copy-start | bytes 6291460
  11.2 4.5 %copy-start.9 = (bf16[16,32]{1,0:T(8,128)(2,1)}, bf16[16,32]{1,0:T(8,128)(2,1)S(1)}, u32[]{:S(2)}) copy-start(bf16[16,32]{1,0:T(8,128)(2,1)S(1)} %fusion.48) | copy-start | bytes 3076
  11.3 4.4 %copy-start.10 = (f32[512]{0:T(512)S(1)}, f32[512]{0:T(512)}, u32[]{:S(2)}) copy-start(f32[512]{0:T(512)} %param.28) | copy-start | bytes 6148
  11.3 4.5 %copy-start.11 = (f32[512]{0:T(512)S(1)}, f32[512]{0:T(512)}, u32[]{:S(2)}) copy-start(f32[512]{0:T(512)} %param.24) | copy-start | bytes 6148
  11.3 19.6 %copy-start.1 = (bf16[512,8,96]{0,2,1:T(8,128)(2,1)S(1)}, bf16[512,8,96]{0,2,1:T(8,128)(2,1)}, u32[]{:S(2)}) copy-start(bf16[512,8,96]{0,2,1:T(8,128)(2,1)} %param.25) | copy-start | bytes 2359300
  13.4 18.1 %copy-start.2 = (bf16[512,8,64]{0,2,1:T(8,128)(2,1)S(1)}, bf16[512,8,64]{0,2,1:T(8,128)(2,1)}, u32[]{:S(2)}) copy-start(bf16[512,8,64]{0,2,1:T(8,128)(2,1)} %param.29) | copy-start | bytes 1572868
  13.5 18.1 %copy-start.3 = (bf16[256,512]{1,0:T(8,128)(2,1)S(1)}, bf16[256,512]{1,0:T(8,128)(2,1)}, u32[]{:S(2)}) copy-start(bf16[256,512]{1,0:T(8,128)(2,1)} %param.18) | copy-start | bytes 786436
  15.6 16.3 %copy-start.8 = (bf16[256,32]{0,1:T(8,128)(2,1)S(1)}, bf16[256,32]{0,1:T(8,128)(2,1)}, u32[]{:S(2)}) copy-start(bf16[256,32]{0,1:T(8,128)(2,1)} %param.19) | copy-start | bytes 49156
  15.8 28.0 %copy-start.6 = (bf16[16,512]{1,0:T(8,128)(2,1)}, bf16[16,512]{1,0:T(8,128)(2,1)S(1)}, u32[]{:S(2)}) copy-start(bf16[16,512]{1,0:T(8,128)(2,1)S(1)} %slice.78) | copy-start | bytes 49156
  32.3 9.2 %copy-start.7 = (bf16[1,512,32]{1,2,0:T(8,128)(2,1)S(1)}, bf16[1,512,32]{1,2,0:T(8,128)(2,1)}, u32[]{:S(2)}) copy-start(bf16[1,512,32]{1,2,0:T(8,128)(2,1)} %param.21) | copy-start | bytes 98308
  33.4 12.3 %all-to-all-start.1 = ((bf16[4,16,8]{1,2,0:T(8,128)(2,1)}), bf16[4,16,8]{1,2,0:T(8,128)(2,1)S(1)}, u32[]{:S(2)}, u32[]{:S(2)}) async-start(bf16[4,16,8]{1,2,0:T(8,128)(2,1)} %copy.43), calls=%async_computation.1 | async-start | bytes 16384 | tf_op jit(solution)/shard_map/all_to_all | solution.py:167
  38.1 5.4 %copy-start.5 = (bf16[512,8,64]{0,2,1:T(8,128)(2,1)S(1)}, bf16[512,8,64]{0,2,1:T(8,128)(2,1)}, u32[]{:S(2)}) copy-start(bf16[512,8,64]{0,2,1:T(8,128)(2,1)} %param.30) | copy-start | bytes 1572868
  38.1 5.7 %copy-start.4 = (bf16[256,512]{1,0:T(8,128)(2,1)S(1)}, bf16[256,512]{1,0:T(8,128)(2,1)}, u32[]{:S(2)}) copy-start(bf16[256,512]{1,0:T(8,128)(2,1)} %param.18) | copy-start | bytes 786436
  38.2 6.1 %copy-start.13 = (bf16[1,32]{1,0:T(2,128)(2,1)}, bf16[1,32]{1,0:T(2,128)(2,1)S(1)}, u32[]{:S(2)}) copy-start(bf16[1,32]{1,0:T(2,128)(2,1)S(1)} %pad_maximum_fusion.4) | copy-start | bytes 196
  38.2 6.0 %copy-start.12 = (bf16[1,512]{1,0:T(2,128)(2,1)}, bf16[1,512]{1,0:T(2,128)(2,1)S(1)}, u32[]{:S(2)}) copy-start(bf16[1,512]{1,0:T(2,128)(2,1)S(1)} %get-tuple-element.25) | copy-start | bytes 3076
  45.7 10.7 %all-to-all-start.2 = ((bf16[4,16,8]{1,2,0:T(8,128)(2,1)}), bf16[4,16,8]{1,2,0:T(8,128)(2,1)S(1)}, u32[]{:S(2)}, u32[]{:S(2)}) async-start(bf16[4,16,8]{1,2,0:T(8,128)(2,1)} %copy.45), calls=%async_computation.2 | async-start | bytes 16384 | tf_op jit(solution)/shard_map/all_to_all | solution.py:170
  56.3 9.0 %all-to-all-start = ((bf16[4,16,512]{2,1,0:T(8,128)(2,1)}), bf16[4,16,512]{2,1,0:T(8,128)(2,1)S(1)}, u32[]{:S(2)}, u32[]{:S(2)}) async-start(bf16[4,16,512]{2,1,0:T(8,128)(2,1)} %reshape.289), calls=%async_computation | async-start | bytes 131072 | tf_op jit(solution)/shard_map/all_to_all | solution.py:166
  59.6 23.6 %all-reduce.2.cloned.1.call-start = ((), (), s32[]{:S(2)}) async-start(), calls=%async_computation.3 | async-start | bytes 196608 | tf_op jit(solution)/shard_map/psum | solution.py:196
Sparse Core Ops, SparseCore 0:
  66.8 16.3 all-reduce.1
where the time goes:
time: 93.7 us; the launch traced here: 92.9 us
  waiting for transfers between devices  26.5 us (28%)
  between operations  15.2 us (16%)
  blocking collectives  14.9 us (16%)
  matrix products  13.9 us (15%)
  starting transfers between devices  13.2 us (14%)
  local copies, waits for them, and re-layouts  7.29 us (8%)
  other arithmetic  1.88 us (2%)
    psum x1, waiting for transfers between devices, per_device(): summed = lax.psum(term.astype(jnp.bfloat16), 'tp')  16.5 us
    all_gather x1, blocking collectives, per_device(): lax.all_gather(query_latent[:piece_dev], 'kv', axis=0, tiled=True)  14.9 us
    all_to_all x1, waiting for transfers between devices, per_device(): lax.all_to_all(parts, 'kv', split_axis=0, concat_axis=0, tiled=True)  5.31 us
    all_to_all x1, starting transfers between devices, per_device(): lax.all_to_all(totals.astype(jnp.bfloat16), 'kv', split_axis=0, concat_ax...  5.09 us
    all_to_all x1, starting transfers between devices, per_device(): lax.all_to_all(tops.astype(jnp.bfloat16), 'kv', split_axis=0, concat_axis...  4.73 us
    all_to_all x1, waiting for transfers between devices, per_device(): lax.all_to_all(totals.astype(jnp.bfloat16), 'kv', split_axis=0, concat_ax...  4.64 us
    all_to_all x1, starting transfers between devices, per_device(): lax.all_to_all(parts, 'kv', split_axis=0, concat_axis=0, tiled=True)  3.29 us
    dot_general x1, matrix products, per_device(): jnp.dot(rows, w_kvdown, preferred_element_type=jnp.float32)  2.16 us
  transfers between devices with their start and end apart: 4, of which 3 were waited for; matrix products, arithmetic and copies ran while one was open for 9% of the time, Pallas kernels for 0%

commit v1 on v0

--- a/solution.py
+++ b/solution.py
@@ -5,6 +5,7 @@
 
 NOPE_DIM = 64
 ROPE_DIM = 32
+MAX_PERMUTES = 8
 
 
 def rms_scale(values, gain):
@@ -26,6 +27,34 @@
     nope = full[..., :NOPE_DIM].astype(jnp.bfloat16)
     turned = rotate(full[..., NOPE_DIM:], positions).astype(jnp.bfloat16)
     return (nope, turned)
+
+
+def shift(values, axis, step):
+    size = lax.axis_size(axis)
+    return lax.ppermute(values, axis, [(i, (i + step) % size) for i in range(size)])
+
+
+def gather_blocks(values, axis):
+    size = lax.axis_size(axis)
+    if size > MAX_PERMUTES:
+        blocks = lax.all_gather(values, axis, axis=0)
+        return jnp.roll(jnp.flip(blocks, 0), lax.axis_index(axis) + 1, axis=0)
+    return jnp.stack([values] + [shift(values, axis, s) for s in range(1, size)])
+
+
+def return_blocks(blocks, axis):
+    size = lax.axis_size(axis)
+    if size > MAX_PERMUTES:
+        ordered = jnp.flip(jnp.roll(blocks, -lax.axis_index(axis) - 1, axis=0), 0)
+        return lax.all_to_all(ordered, axis, split_axis=0, concat_axis=0, tiled=True)
+    return jnp.stack([blocks[0]] + [shift(blocks[s], axis, size - s) for s in range(1, size)])
+
+
+def split3(values):
+    high = lax.reduce_precision(values, 8, 7)
+    rest = values - high
+    middle = lax.reduce_precision(rest, 8, 7)
+    return [piece.astype(jnp.bfloat16) for piece in (high, middle, rest - middle)]
 
 
 def decode_attend(
@@ -94,24 +123,23 @@
     index = lax.axis_index("kv")
     piece_dev = piece_rows.shape[0]
     cache_dev = prompt_latent.shape[0]
-    piece_all = piece_dev * shards
     context_len = cache_dev * shards
     rows = jnp.concatenate([piece_rows, decode_rows], 0)
     query_latent = rms_scale(
         jnp.dot(rows, w_qdown, preferred_element_type=jnp.float32), q_gain
     ).astype(jnp.bfloat16)
+    block_rows = gather_blocks(query_latent[:piece_dev], "kv").reshape(-1, query_latent.shape[1])
     latent_new = rms_scale(
         jnp.dot(rows, w_kvdown, preferred_element_type=jnp.float32), kv_gain
     ).astype(jnp.bfloat16)
-    piece_pos = context_len + index * piece_dev + jnp.arange(piece_dev, dtype=jnp.int32)
+    offsets = jnp.arange(piece_dev, dtype=jnp.int32)
+    piece_pos = context_len + index * piece_dev + offsets
     positions = jnp.concatenate([piece_pos, dec_lengths])
     rope_new = rotate(jnp.dot(rows, w_krope, preferred_element_type=jnp.float32), positions).astype(
         jnp.bfloat16
     )
-    block_rows = lax.all_gather(query_latent[:piece_dev], "kv", axis=0, tiled=True)
-    block_pos = context_len + jnp.int32(0) + jnp.arange(block_rows.shape[0], dtype=jnp.int32)
-    nope, turned = query_heads(block_rows, w_qup, block_pos)
-    queries = jnp.concatenate([nope, turned], -1)
+    owners = (index - jnp.arange(shards, dtype=jnp.int32) + shards) % shards
+    query_pos = (context_len + owners[:, None] * piece_dev + offsets[None, :]).reshape(-1)
     dec_nope, dec_qrope = query_heads(query_latent[piece_dev:], w_qup, dec_lengths)
     dec_latent = latent_new[piece_dev:]
     dec_rope = rope_new[piece_dev:]
@@ -126,58 +154,24 @@
     values = jnp.einsum(
         "sl,lhe->she", key_latent, w_vup, preferred_element_type=jnp.float32
     ).astype(jnp.bfloat16)
-    block = min(512, piece_all)
-    count = piece_all // block
-
-    def attend(number):
-        start = number * block
-        block_q = lax.dynamic_slice_in_dim(queries, start, block, 0)
-        query_pos = context_len + start + jnp.arange(block, dtype=jnp.int32)
-        scores = (
-            jnp.einsum(
-                "qhe,she->qhs",
-                block_q[..., :NOPE_DIM],
-                key_nope,
-                preferred_element_type=jnp.float32,
-            )
-            + jnp.einsum(
-                "qhe,se->qhs",
-                block_q[..., NOPE_DIM:],
-                key_turned,
-                preferred_element_type=jnp.float32,
-            )
-        ) * scale
-        scores = jnp.where(key_pos[None, None, :] <= query_pos[:, None, None], scores, -1e30)
-        top = jnp.max(scores, axis=-1)
-        weights = jnp.exp(scores - top[..., None])
-        total = jnp.sum(weights, axis=-1)
-        part = jnp.einsum(
-            "qhs,she->qhe", weights.astype(jnp.bfloat16), values, preferred_element_type=jnp.float32
-        )
-        return (part.astype(jnp.bfloat16), top, total)
-
-    parts, tops, totals = lax.map(attend, jnp.arange(count, dtype=jnp.int32))
-    heads_dev = parts.shape[2]
-    value_dim = parts.shape[3]
-    parts = parts.reshape(shards, piece_dev, heads_dev * value_dim)
-    tops = tops.reshape(shards, piece_dev, heads_dev)
-    totals = totals.reshape(shards, piece_dev, heads_dev)
-    got_parts, got_tops, got_totals = (
-        lax.all_to_all(parts, "kv", split_axis=0, concat_axis=0, tiled=True),
-        lax.all_to_all(
-            tops.astype(jnp.bfloat16), "kv", split_axis=0, concat_axis=0, tiled=True
-        ).astype(tops.dtype),
-        lax.all_to_all(
-            totals.astype(jnp.bfloat16), "kv", split_axis=0, concat_axis=0, tiled=True
-        ).astype(totals.dtype),
-    )
-    best = jnp.max(got_tops, axis=0)
-    factors = jnp.exp(got_tops - best[None])
-    denom = jnp.sum(got_totals * factors, axis=0)
-    got_parts = got_parts.reshape(shards, piece_dev, heads_dev, value_dim).astype(jnp.float32)
-    piece_heads = (jnp.sum(got_parts * factors[..., None], axis=0) / denom[..., None]).astype(
-        jnp.bfloat16
-    )
+    nope, turned = query_heads(block_rows, w_qup, query_pos)
+    scores = (
+        jnp.einsum("qhe,she->qhs", nope, key_nope, preferred_element_type=jnp.float32)
+        + jnp.einsum("qhe,se->qhs", turned, key_turned, preferred_element_type=jnp.float32)
+    ) * scale
+    scores = jnp.where(key_pos[None, None, :] <= query_pos[:, None, None], scores, -1e30)
+    top = jnp.max(scores, axis=-1)
+    weights = jnp.exp(scores - top[..., None])
+    total = jnp.sum(weights, axis=-1)
+    part = jnp.einsum(
+        "qhs,she->qhe", weights.astype(jnp.bfloat16), values, preferred_element_type=jnp.float32
+    )
+    heads_dev, value_dim = part.shape[1:]
+    width = heads_dev * value_dim
+    packed = jnp.concatenate(
+        [part.astype(jnp.bfloat16).reshape(-1, width)] + split3(top) + split3(total), -1
+    ).reshape(shards, piece_dev, -1)
+    got = return_blocks(packed, "kv")
     decode_heads = decode_attend(
         dec_nope,
         dec_qrope,
@@ -190,10 +184,23 @@
         w_vup,
         scale,
     )
+    got_parts = got[..., :width].reshape(shards, piece_dev, heads_dev, value_dim)
+    stats = got[..., width:].astype(jnp.float32).reshape(shards, piece_dev, 2, 3, heads_dev)
+    stats = stats[..., 0, :] + stats[..., 1, :] + stats[..., 2, :]
+    got_tops, got_totals = stats[:, :, 0], stats[:, :, 1]
+    best = jnp.max(got_tops, axis=0)
+    factors = jnp.exp(got_tops - best[None])
+    denom = jnp.sum(got_totals * factors, axis=0)
+    piece_heads = (
+        jnp.sum(got_parts.astype(jnp.float32) * factors[..., None], axis=0) / denom[..., None]
+    ).astype(jnp.bfloat16)
     all_heads = jnp.concatenate([piece_heads, decode_heads], 0)
     term = jnp.einsum("rhv,hvd->rd", all_heads, w_out, preferred_element_type=jnp.float32)
-    term = term.astype(jnp.bfloat16).astype(jnp.float32)
-    summed = lax.psum(term.astype(jnp.bfloat16), "tp")
+    term = term.astype(jnp.bfloat16)
+    summed = term.astype(jnp.float32)
+    for step in range(1, lax.axis_size("tp")):
+        summed = summed + shift(term, "tp", step).astype(jnp.float32)
+    summed = summed.astype(jnp.bfloat16)
     return (
         summed[:piece_dev],
         summed[piece_dev:],

time: 93.7 us -> 46.5 us (0.50)
  waiting for transfers between devices: 26.5 us -> 3.6 us
  blocking collectives: 14.9 us -> 0 us
  between operations: 15.2 us -> 1.73 us
  other arithmetic: 1.88 us -> 8.94 us
  starting transfers between devices: 13.2 us -> 11.8 us
    psum x1 -> x0, waiting for transfers between devices: 16.5 us -> none  [per_device(): summed = lax.psum(term.astype(jnp.bfloat16), 'tp')]
    all_gather x1 -> x0, blocking collectives: 14.9 us -> none  [per_device(): lax.all_gather(query_latent[:piece_dev], 'kv', axis=0, tiled=True)]
    all_to_all x3 -> x0, starting transfers between devices: 13.1 us -> none  [the longest x1 5.09 us: per_device(): lax.all_to_all(totals.astype(jnp.bfloat16), 'kv', split_axis=0, concat_ax...]
    ppermute x0 -> x7, starting transfers between devices: none -> 11.8 us  [shift(): lax.ppermute(values, axis, [(i, (i + step) % size) for i in range(size)])]
    all_to_all x3 -> x0, waiting for transfers between devices: 9.95 us -> none  [the longest x1 5.31 us: per_device(): lax.all_to_all(parts, 'kv', split_axis=0, concat_axis=0, tiled=True)]
    ppermute x0 -> x7, waiting for transfers between devices: none -> 3.6 us  [shift(): lax.ppermute(values, axis, [(i, (i + step) % size) for i in range(size)])]
    unnamed x2, matrix products: 0.92 us -> 2.76 us
    dot_general x1, matrix products: 2.16 us -> 0.49 us  [per_device(): jnp.dot(rows, w_kvdown, preferred_element_type=jnp.float32)]
  transfers between devices with their start and end apart: 4 -> 7, of which waited for: 3 -> 3; matrix products, arithmetic and copies ran while one was open for 9% -> 37% of each run, Pallas kernels for 0% -> 0%
where the time goes in v1:
time: 46.5 us; the launch traced here: 46.1 us
  matrix products  13 us (28%)
  starting transfers between devices  11.8 us (25%)
  other arithmetic  8.94 us (19%)
  local copies, waits for them, and re-layouts  7.08 us (15%)
  waiting for transfers between devices  3.6 us (8%)
  between operations  1.73 us (4%)
    ppermute x7, starting transfers between devices, shift(): lax.ppermute(values, axis, [(i, (i + step) % size) for i in range(size)])  11.8 us
    ppermute x7, waiting for transfers between devices, shift(): lax.ppermute(values, axis, [(i, (i + step) % size) for i in range(size)])  3.6 us
    unnamed x2, matrix products  2.76 us
    dot_general x1, matrix products, per_device(): jnp.dot(rows, w_qdown, preferred_element_type=jnp.float32)  2.16 us
    dot_general x1, matrix products, per_device(): jnp.einsum('qhs,she->qhe', weights.astype(jnp.bfloat16), values, preferre...  1.5 us
    convert_element_type x2, other arithmetic, rotate(): angle = positions.astype(jnp.float32)[:, None] * inverse[None, :]  1.42 us
    le x1, other arithmetic, per_device(): key_pos[None, None, :] <= query_pos[:, None, None]  1.34 us
    unnamed x47, local copies, waits for them, and re-layouts  1.33 us
  transfers between devices with their start and end apart: 7, of which 3 were waited for; matrix products, arithmetic and copies ran while one was open for 37% of the time, Pallas kernels for 0%

profile of v1, /device:TPU:0, one launch (start us, length us, event | category | flops | bytes accessed | tf_op | source)
XLA Modules:
  0.0 46.1 jit_solution(15546463482660829502)
XLA Ops:
  0.7 1.0 %constant_dynamic-update-slice_fusion.1 = bf16[17,2048]{1,0:T(8,128)(2,1)S(1)} fusion(bf16[16,2048]{1,0:T(8,128)(2,1)} %param.16), kind=kLoop, calls=%fused_computation.85 | loop fusion | bytes 131072
  1.7 0.8 %constant_dynamic-update-slice_fusion = bf16[17,2048]{1,0:T(8,128)(2,1)S(1)} fusion(bf16[17,2048]{1,0:T(8,128)(2,1)S(1)} %constant_dynamic-update-slice_fusion.1, bf16[1,2048]{1,0:T(2,128)(2,1)} %param.17), kind=kLoop, calls=%fused_computation.84 | loop fusion | bytes 12288 | tf_op jit(solution)/shard_map/concatenate | solution.py:127
  2.5 2.2 %multiply_reduce_fusion.1 = (f32[17]{0:T(128)S(1)}, f32[17,512]{1,0:T(8,128)S(1)}) fusion(bf16[17,2048]{1,0:T(8,128)(2,1)S(1)} %constant_dynamic-update-slice_fusion, bf16[2048,512]{1,0:T(8,128)(2,1)} %param.23), kind=kOutput, calls=%fused_computation.45 | convolution fusion | flops 35668976 | bytes 2201668 | tf_op jit(solution)/shard_map/dot_general | solution.py:129
  5.4 4.1 %collective-permute-start.1 = (bf16[16,512]{1,0:T(8,128)(2,1)}, bf16[16,512]{1,0:T(8,128)(2,1)}, u32[]{:S(2)}, u32[]{:S(2)}) collective-permute-start(bf16[16,512]{1,0:T(8,128)(2,1)} %get-tuple-element.17), channel_id=1, source_target_pairs={{0,4},{2,6},{4,0},{6,2},{1,5},{3,7},{5,1},{7,3},{8,12},{10,14},{12... | collective-permute-start | bytes 49160 | tf_op jit(solution)/shard_map/ppermute | solution.py:34
  9.4 1.6 %collective-permute-start = (bf16[16,512]{1,0:T(8,128)(2,1)}, bf16[16,512]{1,0:T(8,128)(2,1)}, u32[]{:S(2)}, u32[]{:S(2)}) collective-permute-start(bf16[16,512]{1,0:T(8,128)(2,1)} %get-tuple-element.17), channel_id=1, source_target_pairs={{0,2},{2,4},{4,6},{6,0},{1,3},{3,5},{5,7},{7,1},{8,10},{10,12},{12... | collective-permute-start | bytes 49160 | tf_op jit(solution)/shard_map/ppermute | solution.py:34
  11.0 2.2 %collective-permute-start.2 = (bf16[16,512]{1,0:T(8,128)(2,1)}, bf16[16,512]{1,0:T(8,128)(2,1)}, u32[]{:S(2)}, u32[]{:S(2)}) collective-permute-start(bf16[16,512]{1,0:T(8,128)(2,1)} %get-tuple-element.17), channel_id=1, source_target_pairs={{0,6},{2,0},{4,2},{6,4},{1,7},{3,1},{5,3},{7,5},{8,14},{10,8},{12,... | collective-permute-start | bytes 49160 | tf_op jit(solution)/shard_map/ppermute | solution.py:34
  14.4 1.1 %fusion.69 = (bf16[512]{0:T(512)(128)(2,1)}, bf16[1,512]{1,0:T(2,128)(2,1)}) fusion(bf16[17,512]{1,0:T(8,128)(2,1)S(1)} %multiply_convert_fusion.1), kind=kLoop, calls=%fused_computation.140 | loop fusion | bytes 3072 | tf_op jit(solution)/shard_map/slice | solution.py:144
  16.7 0.7 %add_convert_fusion.3 = f32[17]{0:T(128)} fusion(s32[1]{0:T(128)} %copy.91, s32[16]{0:T(128)S(1)} %iota_add_fusion.2), kind=kLoop, calls=%fused_computation.122 | loop fusion | flops 34 | bytes 136 | tf_op jit(solution)/shard_map/convert_element_type | solution.py:18
  17.9 0.7 %multiply_sine_fusion.2 = (f32[16]{0:T(128)}, f32[16]{0:T(128)}) fusion(f32[]{:T(128)} %bitcast.32), kind=kLoop, calls=%fused_computation.130 | loop fusion | flops 48 | bytes 132 | tf_op jit(solution)/shard_map/sin | solution.py:20
  18.6 0.7 %iota_add_fusion = s32[4,16]{1,0:T(4,128)S(1)} fusion(s32[4]{0:T(128)} %fusion.58), kind=kLoop, calls=%fused_computation.115 | loop fusion | flops 64 | bytes 272 | tf_op jit(solution)/shard_map/add | solution.py:142
  20.0 0.8 %convert_element_type.116 = f32[64]{0:T(128)S(1)} convert(s32[64]{0:T(128)} %add.136) | non-fusion elementwise | flops 64 | bytes 512 | tf_op jit(solution)/shard_map/convert_element_type | solution.py:18
  20.7 1.3 %broadcast_compare_fusion = pred[64,272]{1,0:T(8,128)(4,1)} fusion(s32[272]{0:T(512)S(1)} %pad_add_fusion, s32[64]{0:T(128)} %add.136), kind=kLoop, calls=%fused_computation.46 | loop fusion | flops 17408 | bytes 18752 | tf_op jit(solution)/shard_map/le | solution.py:162
  22.1 1.1 %fusion.74 = f32[17,32]{1,0:T(8,128)S(1)} fusion(bf16[17,2048]{1,0:T(8,128)(2,1)S(1)} %constant_dynamic-update-slice_fusion, bf16[2048,32]{0,1:T(8,128)(2,1)} %param.27), kind=kOutput, calls=%fused_computation.145 | convolution fusion | flops 2228224 | bytes 202880 | tf_op jit(solution)/shard_map/dot_general | solution.py:138
  23.1 0.7 %mul.278 = f32[512]{0:T(512)S(1)} convert(bf16[512]{0:T(512)(128)(2,1)} %get-tuple-element.8) | non-fusion elementwise | flops 512 | bytes 3072 | tf_op jit(solution)/shard_map/mul | solution.py:96
  24.4 0.8 %convolution_bitcast_fusion.2 = f32[8]{0:T(128)S(1)} fusion(bf16[8,1,512]{2,1,0:T(2,128)(2,1)S(1)} %fusion.51, bf16[1,512]{1,0:T(2,128)(2,1)} %get-tuple-element.9), kind=kOutput, calls=%fused_computation.13 | convolution fusion | flops 8192 | bytes 9248 | tf_op jit(solution)/shard_map/bhl,bl->bh/dot_general | solution.py:85
  25.2 1.3 %fusion.13 = f32[8,512]{1,0:T(8,128)S(1)} fusion(bf16[1,512,512]{2,1,0:T(8,128)(2,1)} %param.20, bf16[8,1,512]{2,1,0:T(2,128)(2,1)S(1)} %fusion.51), kind=kOutput, calls=%fused_computation.21 | convolution fusion | flops 4194304 | bytes 548864 | tf_op jit(solution)/shard_map/bhl,bcl->bhc/dot_general | solution.py:76
  28.2 1.4 %fusion.19 = f32[272,512]{0,1} fusion(bf16[512,512]{0,1:T(8,128)(2,1)S(1)} %bitcast.125, bf16[16,512]{1,0:T(8,128)(2,1)S(1)} %slice.125, bf16[256,512]{1,0:T(8,128)(2,1)S(1)} %copy-done.5), kind=kOutput, calls=%fused_computation.31 | convolution fusion | flops 143163392 | bytes 1359872
  29.6 1.4 %fusion.20 = f32[272,512]{0,1} fusion(bf16[512,512]{0,1:T(8,128)(2,1)S(1)} %bitcast.127, bf16[16,512]{1,0:T(8,128)(2,1)S(1)} %slice.125, bf16[256,512]{1,0:T(8,128)(2,1)S(1)} %copy-done.5), kind=kOutput, calls=%fused_computation.32 | convolution fusion | flops 143163392 | bytes 1359872
  31.1 0.8 %pad_maximum_fusion.4 = bf16[4,16,512]{2,1,0:T(8,128)(2,1)S(1)} fusion(bf16[1,16,512]{2,1,0:T(8,128)(2,1)} %bitcast.7, bf16[1,16,512]{2,1,0:T(8,128)(2,1)} %bitcast.6, bf16[1,16,512]{2,1,0:T(8,128)(2,1)} %bitcast.5, bf16[1,16,512]{2,1,0:T(8,128)(2,1)S(1)} %copy-done.10), kind=kLoop, calls=%fused_computation.39 | loop fusion | flops 98304 | bytes 131072 | tf_op jit(solution)/shard_map/stack | solution.py:42
  34.3 1.5 %convolution_convert_fusion = bf16[8,64,64]{2,1,0:T(8,128)(2,1)S(1)} fusion(f32[64,8,272]{2,0,1:T(8,128)S(1)} %get-tuple-element.41, f32[64,8]{0,1:T(8,128)S(1)} %get-tuple-element.40, f32[272,8,64]{0,2,1:T(8,128)} %bitcast.123), kind=kOutput, calls=%fused_computation.6 | convolution fusion | flops 18276352 | bytes 1181696 | tf_op jit(solution)/shard_map/qhs,she->qhe/dot_general | solution.py:166
  36.6 3.3 %collective-permute-start.3 = (bf16[16,560]{1,0:T(8,128)(2,1)S(1)}, bf16[16,560]{1,0:T(8,128)(2,1)S(1)}, u32[]{:S(2)}, u32[]{:S(2)}) collective-permute-start(bf16[16,560]{1,0:T(8,128)(2,1)S(1)} %get-tuple-element.15), channel_id=1, source_target_pairs={{0,6},{2,0},{4,2},{6,4},{1,7},{3,1},{5,3},{7,5},{8,14},{10,8},{12,... | collective-permute-start | bytes 53768 | tf_op jit(solution)/shard_map/ppermute | solution.py:34
  39.9 1.7 %collective-permute-done.5 = bf16[16,560]{1,0:T(8,128)(2,1)S(1)} collective-permute-done((bf16[16,560]{1,0:T(8,128)(2,1)S(1)}, bf16[16,560]{1,0:T(8,128)(2,1)S(1)}, u32[]{:S(2)}, u32[]{:S(2)}) %collective-permute-start.5) | collective-permute-done | bytes 17952 | tf_op jit(solution)/shard_map/ppermute | solution.py:34
  43.6 1.3 %collective-permute-done.6 = bf16[17,2048]{1,0:T(8,128)(2,1)S(1)} collective-permute-done((bf16[17,2048]{1,0:T(8,128)(2,1)S(1)}, bf16[17,2048]{1,0:T(8,128)(2,1)S(1)}, u32[]{:S(2)}, u32[]{:S(2)}) %collective-permute-start.6) | collective-permute-done | bytes 69664 | tf_op jit(solution)/shard_map/ppermute | solution.py:34
  45.5 0.6 %slice.146 = bf16[16,2048]{1,0:T(8,128)(2,1)} slice(bf16[17,2048]{1,0:T(8,128)(2,1)S(1)} %add_convert_fusion.1), slice={[0:16], [0:2048]} | slice | bytes 131072 | tf_op jit(solution)/shard_map/slice | solution.py:205
  (117 shorter events, 11.5 us)
Async XLA Ops:
  0.6 42.5 %copy-start = (bf16[8,64,2048]{2,1,0:T(8,128)(2,1)S(1)}, bf16[8,64,2048]{2,1,0:T(8,128)(2,1)}, u32[]{:S(2)}) copy-start(bf16[8,64,2048]{2,1,0:T(8,128)(2,1)} %param.31) | copy-start | bytes 6291460
  0.6 4.0 %copy-start.15 = (f32[512]{0:T(512)S(1)}, f32[512]{0:T(512)}, u32[]{:S(2)}) copy-start(f32[512]{0:T(512)} %param.24) | copy-start | bytes 6148
  0.7 13.1 %copy-start.4 = (bf16[2048,512]{1,0:T(8,128)(2,1)S(1)}, bf16[2048,512]{1,0:T(8,128)(2,1)}, u32[]{:S(2)}) copy-start(bf16[2048,512]{1,0:T(8,128)(2,1)} %param.26) | copy-start | bytes 6291460
  2.5 11.8 %copy-start.16 = (f32[512]{0:T(512)S(1)}, f32[512]{0:T(512)}, u32[]{:S(2)}) copy-start(f32[512]{0:T(512)} %param.28) | copy-start | bytes 6148
  2.5 21.3 %copy-start.1 = (bf16[512,8,96]{0,2,1:T(8,128)(2,1)S(1)}, bf16[512,8,96]{0,2,1:T(8,128)(2,1)}, u32[]{:S(2)}) copy-start(bf16[512,8,96]{0,2,1:T(8,128)(2,1)} %param.25) | copy-start | bytes 2359300
  4.7 19.5 %copy-start.3 = (bf16[512,8,64]{0,2,1:T(8,128)(2,1)S(1)}, bf16[512,8,64]{0,2,1:T(8,128)(2,1)}, u32[]{:S(2)}) copy-start(bf16[512,8,64]{0,2,1:T(8,128)(2,1)} %param.29) | copy-start | bytes 1572868
  5.4 25.7 %collective-permute-start.1 = (bf16[16,512]{1,0:T(8,128)(2,1)}, bf16[16,512]{1,0:T(8,128)(2,1)}, u32[]{:S(2)}, u32[]{:S(2)}) collective-permute-start(bf16[16,512]{1,0:T(8,128)(2,1)} %get-tuple-element.17), channel_id=1, source_target_pairs={{0,4},{2,6},{4,0},{6,2},{1,5},{3,7},{5,1},{7,3},{8,12},{10,14},{12... | collective-permute-start | bytes 49160 | tf_op jit(solution)/shard_map/ppermute | solution.py:34
  9.4 21.7 %collective-permute-start = (bf16[16,512]{1,0:T(8,128)(2,1)}, bf16[16,512]{1,0:T(8,128)(2,1)}, u32[]{:S(2)}, u32[]{:S(2)}) collective-permute-start(bf16[16,512]{1,0:T(8,128)(2,1)} %get-tuple-element.17), channel_id=1, source_target_pairs={{0,2},{2,4},{4,6},{6,0},{1,3},{3,5},{5,7},{7,1},{8,10},{10,12},{12... | collective-permute-start | bytes 49160 | tf_op jit(solution)/shard_map/ppermute | solution.py:34
  11.0 20.1 %collective-permute-start.2 = (bf16[16,512]{1,0:T(8,128)(2,1)}, bf16[16,512]{1,0:T(8,128)(2,1)}, u32[]{:S(2)}, u32[]{:S(2)}) collective-permute-start(bf16[16,512]{1,0:T(8,128)(2,1)} %get-tuple-element.17), channel_id=1, source_target_pairs={{0,6},{2,0},{4,2},{6,4},{1,7},{3,1},{5,3},{7,5},{8,14},{10,8},{12,... | collective-permute-start | bytes 49160 | tf_op jit(solution)/shard_map/ppermute | solution.py:34
  15.5 14.0 %copy-start.8 = (bf16[16,512]{1,0:T(8,128)(2,1)}, bf16[16,512]{1,0:T(8,128)(2,1)S(1)}, u32[]{:S(2)}) copy-start(bf16[16,512]{1,0:T(8,128)(2,1)S(1)} %slice.125) | copy-start | bytes 49156
  19.9 6.5 %copy-start.14 = (f32[16]{0:T(128)S(1)}, f32[16]{0:T(128)}, u32[]{:S(2)}) copy-start(f32[16]{0:T(128)} %multiply_power_fusion) | copy-start | bytes 196
  19.9 6.8 %copy-start.18 = (f32[17]{0:T(128)S(1)}, f32[17]{0:T(128)}, u32[]{:S(2)}) copy-start(f32[17]{0:T(128)} %add_convert_fusion.3) | copy-start | bytes 208
  19.9 7.0 %copy-start.20 = (f32[16]{0:T(128)S(1)}, f32[16]{0:T(128)}, u32[]{:S(2)}) copy-start(f32[16]{0:T(128)} %get-tuple-element.42) | copy-start | bytes 196
  19.9 7.0 %copy-start.21 = (f32[16]{0:T(128)S(1)}, f32[16]{0:T(128)}, u32[]{:S(2)}) copy-start(f32[16]{0:T(128)} %get-tuple-element.43) | copy-start | bytes 196
  19.9 7.1 %copy-start.11 = (bf16[1,512,32]{1,2,0:T(8,128)(2,1)S(1)}, bf16[1,512,32]{1,2,0:T(8,128)(2,1)}, u32[]{:S(2)}) copy-start(bf16[1,512,32]{1,2,0:T(8,128)(2,1)} %param.21) | copy-start | bytes 98308
  19.9 7.1 %copy-start.17 = (pred[512]{0:T(512)(128)(4,1)S(1)}, pred[512]{0:T(512)(128)(4,1)}, u32[]{:S(2)}) copy-start(pred[512]{0:T(512)(128)(4,1)} %iota_compare_fusion) | copy-start | bytes 1540
  19.9 7.8 %copy-start.7 = (bf16[1,512,512]{2,1,0:T(8,128)(2,1)S(1)}, bf16[1,512,512]{2,1,0:T(8,128)(2,1)}, u32[]{:S(2)}) copy-start(bf16[1,512,512]{2,1,0:T(8,128)(2,1)} %param.20) | copy-start | bytes 1572868
  19.9 8.0 %copy-start.6 = (bf16[512,8,64]{0,2,1:T(8,128)(2,1)S(1)}, bf16[512,8,64]{0,2,1:T(8,128)(2,1)}, u32[]{:S(2)}) copy-start(bf16[512,8,64]{0,2,1:T(8,128)(2,1)} %param.30) | copy-start | bytes 1572868
  19.9 8.2 %copy-start.5 = (bf16[256,512]{1,0:T(8,128)(2,1)S(1)}, bf16[256,512]{1,0:T(8,128)(2,1)}, u32[]{:S(2)}) copy-start(bf16[256,512]{1,0:T(8,128)(2,1)} %param.18) | copy-start | bytes 786436
  26.9 4.1 %copy-start.19 = (bf16[1,32]{1,0:T(2,128)(2,1)}, bf16[1,32]{1,0:T(2,128)(2,1)S(1)}, u32[]{:S(2)}) copy-start(bf16[1,32]{1,0:T(2,128)(2,1)S(1)} %pad_maximum_fusion.7) | copy-start | bytes 196
  36.0 5.6 %collective-permute-start.5 = (bf16[16,560]{1,0:T(8,128)(2,1)S(1)}, bf16[16,560]{1,0:T(8,128)(2,1)S(1)}, u32[]{:S(2)}, u32[]{:S(2)}) collective-permute-start(bf16[16,560]{1,0:T(8,128)(2,1)S(1)} %get-tuple-element.13), channel_id=1, source_target_pairs={{0,2},{2,4},{4,6},{6,0},{1,3},{3,5},{5,7},{7,1},{8,10},{10,12},{12... | collective-permute-start | bytes 53768 | tf_op jit(solution)/shard_map/ppermute | solution.py:34
  36.1 5.6 %collective-permute-start.4 = (bf16[16,560]{1,0:T(8,128)(2,1)S(1)}, bf16[16,560]{1,0:T(8,128)(2,1)S(1)}, u32[]{:S(2)}, u32[]{:S(2)}) collective-permute-start(bf16[16,560]{1,0:T(8,128)(2,1)S(1)} %get-tuple-element.14), channel_id=1, source_target_pairs={{0,4},{2,6},{4,0},{6,2},{1,5},{3,7},{5,1},{7,3},{8,12},{10,14},{12... | collective-permute-start | bytes 53768 | tf_op jit(solution)/shard_map/ppermute | solution.py:34
  36.6 5.6 %collective-permute-start.3 = (bf16[16,560]{1,0:T(8,128)(2,1)S(1)}, bf16[16,560]{1,0:T(8,128)(2,1)S(1)}, u32[]{:S(2)}, u32[]{:S(2)}) collective-permute-start(bf16[16,560]{1,0:T(8,128)(2,1)S(1)} %get-tuple-element.15), channel_id=1, source_target_pairs={{0,6},{2,0},{4,2},{6,4},{1,7},{3,1},{5,3},{7,5},{8,14},{10,8},{12,... | collective-permute-start | bytes 53768 | tf_op jit(solution)/shard_map/ppermute | solution.py:34
  43.5 1.3 %collective-permute-start.6 = (bf16[17,2048]{1,0:T(8,128)(2,1)S(1)}, bf16[17,2048]{1,0:T(8,128)(2,1)S(1)}, u32[]{:S(2)}, u32[]{:S(2)}) collective-permute-start(bf16[17,2048]{1,0:T(8,128)(2,1)S(1)} %fusion), channel_id=1, source_target_pairs={{0,1},{1,0},{2,3},{3,2},{4,5},{5,4},{6,7},{7,6},{8,9},{9,8},{10,11... | collective-permute-start | bytes 208904 | tf_op jit(solution)/shard_map/ppermute | solution.py:34
  (5 other events, 14.0 us)

commit v2 on v1

v2 whole, which is shorter than its diff:
```python
import functools

import jax
import jax.numpy as jnp
import numpy as np
from jax import lax
from jax.experimental import pallas as pl
from jax.experimental.pallas import tpu as pltpu
from jax.sharding import PartitionSpec as P

LANES = 128
GROUP = 256
MAX_PERMUTES = 8
ROPE_BASE = 10000.0
VMEM = pl.BlockSpec(memory_space=pltpu.VMEM)
SMEM = pl.BlockSpec(memory_space=pltpu.SMEM)
HBM = pl.BlockSpec(memory_space=pltpu.HBM)
NT = (((1,), (1,)), ((), ()))
F32 = jnp.float32
BF16 = jnp.bfloat16


def dot(a, b):
    return jnp.dot(a, b, preferred_element_type=F32)


def dot_nt(a, b):
    return lax.dot_general(a, b, NT, preferred_element_type=F32)


def lane_index(shape):
    return lax.broadcasted_iota(jnp.int32, shape, len(shape) - 1)


def row_index(shape):
    return lax.broadcasted_iota(jnp.int32, shape, 0)


def rms_scale(values, gain):
    return values * lax.rsqrt(jnp.mean(values * values, axis=-1, keepdims=True) + 1e-06) * gain


def turn(values, cosine, signed_sine, rope):
    half = rope // 2
    swapped = jnp.where(
        lane_index(values.shape) % rope < half,
        pltpu.roll(values, LANES - half, 1),
        pltpu.roll(values, half, 1),
    )
    return values * cosine + swapped * signed_sine


def diagonal(values, count, width):
    owner = lane_index(values.shape) // width
    return jnp.concatenate([jnp.where(owner == j, values, 0.0) for j in range(count)], 0)


def spread_rows(row, rows):
    return jnp.broadcast_to(row.astype(F32), (rows, row.shape[1])).astype(row.dtype)


def query_latent_kernel(piece_ref, dec_ref, w_hbm, gain_ref, out_ref, dec_out_ref, w_ref, sems):
    chunks = sems.shape[0]
    depth = w_ref.shape[0] // chunks
    copies = []
    for c in range(chunks):
        part = pl.ds(c * depth, depth)
        copies.append(pltpu.make_async_copy(w_hbm.at[part], w_ref.at[part], sems.at[c]))
        copies[-1].start()
    piece = piece_ref[...]
    rows = jnp.concatenate([piece, spread_rows(dec_ref[...], piece.shape[0])], 0)
    total = jnp.zeros((rows.shape[0], w_ref.shape[1]), F32)
    for c in range(chunks):
        copies[c].wait()
        part = slice(c * depth, (c + 1) * depth)
        total = total + dot(rows[:, part], w_ref[part, :])
    latent = rms_scale(total, gain_ref[...]).astype(BF16)
    out_ref[...] = latent[: piece.shape[0]]
    dec_out_ref[...] = latent[piece.shape[0] :]


def keys_kernel(
    context,
    lengths_ref,
    piece_ref,
    dec_ref,
    w_ref,
    w_rope_ref,
    gain_ref,
    cos_ref,
    sin_ref,
    freq_ref,
    prompt_ref,
    w_kup_ref,
    w_vup_ref,
    latent_ref,
    dec_latent_ref,
    rope_ref,
    dec_rope_ref,
    key_ref,
    value_ref,
    new_key_ref,
    new_value_ref,
    new_rope_ref,
    dec_rows_ref,
    dec_rope_rows_ref,
):
    count = piece_ref.shape[0]
    rope = w_rope_ref.shape[0]
    piece = piece_ref[...]
    rows = jnp.concatenate([piece, spread_rows(dec_ref[...], count)], 0)
    latent = rms_scale(dot(rows, w_ref[...]), gain_ref[...]).astype(BF16)
    w_rope = jnp.concatenate([w_rope_ref[...]] * (LANES // rope), 0)
    raw = dot_nt(rows, w_rope)
    index = lax.axis_index("kv")
    own = pl.ds(pl.multiple_of(index * count, count), count)
    new_rope = turn(raw[:count], cos_ref[own, :], sin_ref[own, :], rope).astype(BF16)
    angle = lengths_ref[0].astype(F32) * freq_ref[...]
    sign = jnp.where(lane_index(angle.shape) % rope < rope // 2, -1.0, 1.0)
    dec_rope = turn(raw[count:], jnp.cos(angle), jnp.sin(angle) * sign, rope).astype(BF16)
    latent_ref[...] = latent[:count]
    dec_latent_ref[...] = latent[count : count + 1]
    rope_ref[...] = new_rope[:, :rope]
    dec_rope_ref[...] = dec_rope[:1, :rope]
    new_rope_ref[...] = new_rope
    dec_rows_ref[...] = latent[count:]
    dec_rope_rows_ref[...] = dec_rope
    w_kup, w_vup = w_kup_ref[...], w_vup_ref[...]
    prompt = prompt_ref[...]
    key_ref[...] = dot_nt(prompt, w_kup).astype(BF16)
    value_ref[...] = dot_nt(prompt, w_vup).astype(BF16)
    new_key_ref[...] = dot_nt(latent[:count], w_kup).astype(BF16)
    new_value_ref[...] = dot_nt(latent[:count], w_vup).astype(BF16)


def split_query_weights(w_ref, nope):
    heads = w_ref.shape[0]
    w_nope = jnp.concatenate([w_ref[h, :nope, :] for h in range(heads)], 0)
    w_rope = jnp.concatenate([w_ref[h, nope:, :] for h in range(heads)], 0)
    return w_nope, w_rope


def attend_kernel(relative, nope, *refs):
    (
        w_ref,
        key_ref,
        value_ref,
        new_key_ref,
        new_value_ref,
        new_rope_ref,
        rope_ref,
        cos_ref,
        sin_ref,
    ) = refs[:9]
    latent_refs, out_ref = refs[9:-1], refs[-1]
    shards = lax.axis_size("kv")
    index = lax.axis_index("kv")
    heads = w_ref.shape[0]
    rope = w_ref.shape[1] - nope
    count = new_key_ref.shape[0]
    latents = jnp.concatenate([ref[...] for ref in latent_refs], 0)
    queries = latents.shape[0]
    blocks = queries // count
    first = 0 if relative else pl.program_id(0) * blocks
    owners = []
    for s in range(blocks):
        owners.append(lax.rem(index - s + shards, shards) if relative else first + s)
    tables = [pl.ds(pl.multiple_of(owner * count, count), count) for owner in owners]
    cosine = jnp.concatenate([cos_ref[part, :] for part in tables], 0)
    sine = jnp.concatenate([sin_ref[part, :] for part in tables], 0)
    scale = (nope + rope) ** (-0.5)
    w_nope, w_rope = split_query_weights(w_ref, nope)
    q_nope = dot_nt(latents, w_nope).astype(BF16).astype(F32)
    q_rope = dot_nt(latents, w_rope)
    per = GROUP // nope
    rope_keys = jnp.concatenate([rope_ref[...]] * (LANES // rope), 0)
    new_rope = new_rope_ref[...]
    row = row_index((count, count))
    column = lane_index((count, count))
    allowed = jnp.concatenate(
        [index * count + column <= owner * count + row for owner in owners] * per, 0
    )
    lane = lane_index((queries, LANES))
    stats = jnp.zeros((queries, LANES), F32)
    for g in range(heads // per):
        wide = slice(g * GROUP, (g + 1) * GROUP)
        turned = turn(q_rope[:, g * LANES : (g + 1) * LANES], cosine, sine, rope)
        spread = diagonal(q_nope[:, wide], per, nope).astype(BF16)
        spread_rope = diagonal(turned, per, rope).astype(BF16)
        old = (dot_nt(spread, key_ref[:, wide]) + dot(spread_rope, rope_keys)) * scale
        new = (dot_nt(spread, new_key_ref[:, wide]) + dot_nt(spread_rope, new_rope)) * scale
        new = jnp.where(allowed, new, -1e30)
        top = jnp.maximum(
            jnp.max(old, axis=-1, keepdims=True), jnp.max(new, axis=-1, keepdims=True)
        )
        old = jnp.exp(old - top)
        new = jnp.exp(new - top)
        total = jnp.sum(old, axis=-1, keepdims=True) + jnp.sum(new, axis=-1, keepdims=True)
        mixed = dot(old.astype(BF16), value_ref[:, wide]) + dot(
            new.astype(BF16), new_value_ref[:, wide]
        )
        owner_lane = lane_index((queries, GROUP)) // nope
        part = jnp.zeros((queries, GROUP), F32)
        for j in range(per):
            own = slice(j * queries, (j + 1) * queries)
            part = jnp.where(owner_lane == j, mixed[own], part)
            h = g * per + j
            stats = jnp.where(
                lane % heads == h, jnp.where(lane < 3 * heads, top[own], total[own]), stats
            )
        out_ref[:, wide] = part.astype(BF16)
    high = stats.astype(BF16).astype(F32)
    rest = stats - high
    middle = rest.astype(BF16).astype(F32)
    piece = (lane // heads) % 3
    stats = jnp.where(piece == 0, high, jnp.where(piece == 1, middle, rest - middle))
    stats = jnp.where(lane < 6 * heads, stats, 0.0)
    out_ref[:, heads * nope :] = stats.astype(BF16)


def decode_kernel(
    nope,
    lengths_ref,
    q_ref,
    w_ref,
    w_kup_ref,
    w_vup_ref,
    latent_ref,
    rope_ref,
    new_latent_ref,
    new_rope_ref,
    freq_ref,
    out_ref,
):
    heads = w_ref.shape[0]
    rope = w_ref.shape[1] - nope
    length = lengths_ref[0]
    scale = (nope + rope) ** (-0.5)
    latents = q_ref[...]
    rows = latents.shape[0]
    w_nope, w_rope = split_query_weights(w_ref, nope)
    q_nope = dot_nt(latents, w_nope)
    q_rope = dot_nt(latents, w_rope)
    angle = length.astype(F32) * freq_ref[...]
    sign = jnp.where(lane_index(angle.shape) % rope < rope // 2, -1.0, 1.0)
    cosine, sine = jnp.cos(angle), jnp.sin(angle) * sign
    shape = q_nope.shape
    spread = jnp.where(lane_index(shape) // nope == row_index(shape), q_nope, 0.0).astype(BF16)
    absorbed = dot(spread, w_kup_ref[...]).astype(BF16)
    turned = jnp.concatenate(
        [
            turn(q_rope[:, t * LANES : (t + 1) * LANES], cosine, sine, rope)
            for t in range(heads * rope // LANES)
        ],
        1,
    )
    shape = turned.shape
    own_lane = lane_index(shape) // rope == row_index(shape)
    spread_rope = jnp.where(own_lane, turned, 0.0).astype(BF16)
    rope_keys = jnp.concatenate([rope_ref[...]] * heads, 0)
    cached = (dot_nt(absorbed, latent_ref[...]) + dot(spread_rope, rope_keys)) * scale
    cached = jnp.where(lane_index(cached.shape) < length, cached, -1e30)
    new_latent = new_latent_ref[...].astype(F32)
    new_rope = jnp.concatenate([new_rope_ref[...].astype(F32)] * (heads * rope // LANES), 1)
    own = (
        jnp.sum(absorbed.astype(F32) * new_latent, axis=-1, keepdims=True)
        + jnp.sum(spread_rope.astype(F32) * new_rope, axis=-1, keepdims=True)
    ) * scale
    top = jnp.maximum(jnp.max(cached, axis=-1, keepdims=True), own)
    cached = jnp.exp(cached - top)
    own = jnp.exp(own - top)
    total = jnp.sum(cached, axis=-1, keepdims=True) + own
    own = (own / total).astype(BF16).astype(F32)
    context = dot((cached / total).astype(BF16), latent_ref[...]) + own * new_latent
    mixed = dot_nt(context.astype(BF16), w_vup_ref[...])
    shape = mixed.shape
    value_dim = w_vup_ref.shape[0] // heads
    mixed = jnp.where(lane_index(shape) // value_dim == row_index(shape), mixed, 0.0)
    total = jnp.sum(mixed, axis=0, keepdims=True)
    out_ref[...] = jnp.broadcast_to(total, out_ref.shape).astype(BF16)


def combine_kernel(heads, dec_ref, w_ref, *refs):
    got_refs, out_ref = refs[:-1], refs[-1]
    count = dec_ref.shape[0]
    width = w_ref.shape[0]
    value_dim = width // heads

    def read(ref):
        tail = ref[:, width:].astype(F32)
        tail = (
            tail
            + pltpu.roll(tail, LANES - heads, 1)
            + pltpu.roll(tail, LANES - 2 * heads, 1)
        )
        return tail, pltpu.roll(tail, LANES - 3 * heads, 1)

    def widen(values):
        per = LANES // value_dim
        lane = lane_index((count, LANES)) // value_dim
        tiles = []
        for t in range(width // LANES):
            tile = jnp.zeros((count, LANES), F32)
            for j in range(per):
                h = t * per + j
                tile = jnp.where(lane == j, values[:, h : h + 1], tile)
            tiles.append(tile)
        return jnp.concatenate(tiles, 1)

    stats = [read(ref) for ref in got_refs]
    best = functools.reduce(jnp.maximum, [top for top, _ in stats])
    factors = [jnp.exp(top - best) for top, _ in stats]
    total = sum(factor * total for factor, (_, total) in zip(factors, stats))
    mixed = sum(
        ref[:, :width].astype(F32) * widen(factor) for ref, factor in zip(got_refs, factors)
    )
    merged = (mixed / widen(total)).astype(BF16)
    rows = jnp.concatenate([merged, dec_ref[...]], 0)
    out_ref[...] = dot(rows, w_ref[...]).astype(BF16)


def add_kernel(*refs):
    term_refs, piece_ref, dec_ref = refs[:-2], refs[-2], refs[-1]
    total = sum(ref[...].astype(F32) for ref in term_refs)
    count = piece_ref.shape[0]
    piece_ref[...] = total[:count].astype(BF16)
    dec_ref[...] = total[count : count + 1].astype(BF16)


def call(kernel, outs, in_specs, name, flops, **extra):
    many = isinstance(outs, list)
    shapes = [jax.ShapeDtypeStruct(shape, BF16) for shape in (outs if many else [outs])]
    limit = extra.pop("limit", 8 << 20)
    specs = [VMEM] * len(shapes)
    return pl.pallas_call(
        kernel,
        out_shape=shapes if many else shapes[0],
        in_specs=in_specs,
        out_specs=specs if many else specs[0],
        name=name,
        compiler_params=pltpu.CompilerParams(vmem_limit_bytes=limit),
        cost_estimate=pl.CostEstimate(flops=flops, bytes_accessed=flops // 64, transcendentals=0),
        **extra,
    )


def shift(values, axis, step):
    size = lax.axis_size(axis)
    return lax.ppermute(values, axis, [(i, (i + step) % size) for i in range(size)])


def rope_tables(context, rows, rope):
    half = rope // 2
    inverse = ROPE_BASE ** (-np.arange(half, dtype=np.float32) * 2.0 / rope)
    inverse = inverse.astype(np.float32)
    lanes = np.tile(inverse, LANES // half)[None, :]
    angle = (context + np.arange(rows, dtype=np.float32))[:, None] * lanes
    sign = np.where(np.arange(LANES) % rope < half, -1.0, 1.0)
    return (
        np.cos(angle).astype(np.float32),
        (np.sin(angle) * sign).astype(np.float32),
        lanes.astype(np.float32),
    )


def per_device(
    piece_rows,
    decode_rows,
    prompt_latent,
    prompt_rope_key,
    decode_latent,
    decode_rope_key,
    dec_lengths,
    w_qdown,
    q_gain,
    w_qup,
    w_kvdown,
    w_krope,
    kv_gain,
    w_kup,
    w_vup,
    w_out,
):
    shards = lax.axis_size("kv")
    count, model = piece_rows.shape
    cached, width = prompt_latent.shape
    context = cached * shards
    heads, nope = w_kup.shape[1:]
    value_dim = w_vup.shape[2]
    rope = w_krope.shape[1]
    assert decode_rows.shape[0] == 1
    cosine, sine, freq = rope_tables(context, count * shards, rope)
    w_query = jnp.transpose(w_qup, (1, 2, 0))
    w_key = jnp.transpose(w_kup, (1, 2, 0)).reshape(heads * nope, width)
    w_value = jnp.transpose(w_vup, (1, 2, 0)).reshape(heads * value_dim, width)
    w_last = w_out.reshape(heads * value_dim, model)
    packed_width = heads * value_dim + LANES

    q_latent, q_decode = call(
        query_latent_kernel,
        [(count, w_qdown.shape[1]), (count, w_qdown.shape[1])],
        [VMEM, VMEM, HBM, VMEM],
        "query_latent",
        2 * 2 * count * model * w_qdown.shape[1],
        scratch_shapes=[pltpu.VMEM(w_qdown.shape, BF16), pltpu.SemaphoreType.DMA((4,))],
    )(piece_rows, decode_rows, w_qdown, q_gain[None, :])

    direct = shards <= MAX_PERMUTES
    if direct:
        steps = sorted(range(1, shards), key=lambda s: -min(s, shards - s))
        arrived = {s: shift(q_latent, "kv", s) for s in steps}
        blocks = [q_latent] + [arrived[s] for s in range(1, shards)]
    else:
        blocks = [lax.all_gather(q_latent, "kv", axis=0, tiled=True)]

    (
        piece_latent,
        dec_latent,
        piece_rope,
        dec_rope,
        keys,
        values,
        new_keys,
        new_values,
        new_rope,
        dec_latent_rows,
        dec_rope_rows,
    ) = call(
        functools.partial(keys_kernel, context),
        [
            (count, width),
            (1, width),
            (count, rope),
            (1, rope),
            (cached, heads * nope),
            (cached, heads * value_dim),
            (count, heads * nope),
            (count, heads * value_dim),
            (count, LANES),
            (count, width),
            (count, LANES),
        ],
        [SMEM] + [VMEM] * 11,
        "keys",
        4 * cached * width * heads * nope,
    )(
        dec_lengths,
        piece_rows,
        decode_rows,
        w_kvdown,
        w_krope.T,
        kv_gain[None, :],
        cosine,
        sine,
        freq,
        prompt_latent,
        w_key,
        w_value,
    )

    shared = (
        w_query,
        keys,
        values,
        new_keys,
        new_values,
        new_rope,
        prompt_rope_key.T,
        cosine,
        sine,
    )
    total_rows = count * shards
    flops = 4 * total_rows * cached * heads * nope
    if direct:
        packed = call(
            functools.partial(attend_kernel, True, nope),
            (total_rows, packed_width),
            [VMEM] * (len(shared) + shards),
            "attend",
            flops,
        )(*shared, *blocks)
        sent = [packed[s * count : (s + 1) * count] for s in range(shards)]
        came = {s: shift(sent[s], "kv", shards - s) for s in steps}
        got = [sent[0]] + [came[s] for s in range(1, shards)]
    else:
        step_rows = min(64, total_rows)
        whole = [
            pl.BlockSpec(array.shape, lambda i, rank=array.ndim: (0,) * rank) for array in shared
        ]
        packed = pl.pallas_call(
            functools.partial(attend_kernel, False, nope),
            grid=(total_rows // step_rows,),
            out_shape=jax.ShapeDtypeStruct((total_rows, packed_width), BF16),
            in_specs=whole + [pl.BlockSpec((step_rows, w_qdown.shape[1]), lambda i: (i, 0))],
            out_specs=pl.BlockSpec((step_rows, packed_width), lambda i: (i, 0)),
            name="attend",
            compiler_params=pltpu.CompilerParams(vmem_limit_bytes=24 << 20),
        )(*shared, *blocks)
        got = lax.all_to_all(packed, "kv", split_axis=0, concat_axis=0, tiled=True)
        got = [got[s * count : (s + 1) * count] for s in range(shards)]

    dec_heads = call(
        functools.partial(decode_kernel, nope),
        (count, heads * value_dim),
        [SMEM] + [VMEM] * 9,
        "decode",
        4 * count * decode_latent.shape[1] * width * 4,
    )(
        dec_lengths,
        q_decode,
        w_query,
        w_key,
        w_value,
        decode_latent[0],
        decode_rope_key[0].T,
        dec_latent_rows,
        dec_rope_rows,
        freq,
    )

    term = call(
        functools.partial(combine_kernel, heads),
        (2 * count, model),
        [VMEM] * (2 + len(got)),
        "combine",
        2 * 2 * count * heads * value_dim * model,
    )(dec_heads, w_last, *got)
    terms = [term] + [shift(term, "tp", s) for s in range(1, lax.axis_size("tp"))]
    piece_out, decode_out = call(
        add_kernel, [(count, model), (1, model)], [VMEM] * len(terms), "add", 1000
    )(*terms)
    return (piece_out, decode_out, piece_latent, piece_rope, dec_latent, dec_rope)


def solution(mesh):
    rows = P(("dp", "kv"), None)
    cube = P(("dp", "kv"), None, None)
    by_head = P(None, "tp", None)
    in_specs = (
        rows,
        rows,
        rows,
        rows,
        cube,
        cube,
        P(("dp", "kv")),
        P(),
        P(),
        by_head,
        P(),
        P(),
        P(),
        by_head,
        by_head,
        P("tp", None, None),
    )
    return jax.shard_map(
        per_device, mesh=mesh, in_specs=in_specs, out_specs=(rows,) * 6, check_vma=False
    )
```

time: 46.5 us -> 31.4 us (0.68)
  matrix products: 13 us -> 0 us
  other arithmetic: 8.94 us -> 0 us
  Pallas kernels: 0 us -> 6.38 us
  local copies, waits for them, and re-layouts: 7.08 us -> 9.31 us
  waiting for transfers between devices: 3.6 us -> 2.55 us
  starting transfers between devices: 11.8 us -> 11.2 us
    dot_general x16 -> x0, matrix products: 10.2 us -> none  [the longest x1 2.16 us: per_device(): jnp.dot(rows, w_qdown, preferred_element_type=jnp.float32)]
    unnamed x47 -> x42, local copies, waits for them, and re-layouts: 1.33 us -> 9.3 us
    pallas_call x0 -> x6, Pallas kernels: none -> 6.38 us  [the longest x1 1.6 us: per_device(): call(functools.partial(keys_kernel, context), [(count, width), (1, width)...]
    unnamed x2 -> x0, matrix products: 2.76 us -> none
    slice x6 -> x1, local copies, waits for them, and re-layouts: 2.49 us -> 0.01 us  [per_device(): sent = [packed[s * count:(s + 1) * count] for s in range(shards)]]
    convert_element_type x9 -> x0, other arithmetic: 1.72 us -> none  [the longest x2 1.42 us: rotate(): angle = positions.astype(jnp.float32)[:, None] * inverse[None, :]]
    le x1 -> x0, other arithmetic: 1.34 us -> none  [per_device(): key_pos[None, None, :] <= query_pos[:, None, None]]
    add x6 -> x0, other arithmetic: 1.27 us -> none  [the longest x2 1.25 us: per_device(): context_len + owners[:, None] * piece_dev + offsets[None, :]]
  transfers between devices with their start and end apart: 7 -> 7, of which waited for: 3 -> 3; matrix products, arithmetic and copies ran while one was open for 37% -> 0% of each run, Pallas kernels for 0% -> 9%
where the time goes in v2:
time: 31.4 us; the launch traced here: 30.9 us
  starting transfers between devices  11.2 us (36%)
  local copies, waits for them, and re-layouts  9.31 us (30%)
  Pallas kernels  6.38 us (20%)
  waiting for transfers between devices  2.55 us (8%)
  between operations  1.47 us (5%)
    ppermute x7, starting transfers between devices, shift(): lax.ppermute(values, axis, [(i, (i + step) % size) for i in range(size)])  11.2 us
    unnamed x42, local copies, waits for them, and re-layouts  9.3 us
    ppermute x7, waiting for transfers between devices, shift(): lax.ppermute(values, axis, [(i, (i + step) % size) for i in range(size)])  2.55 us
    pallas_call x1, Pallas kernels, per_device(): call(functools.partial(keys_kernel, context), [(count, width), (1, width)...  1.6 us
    pallas_call x1, Pallas kernels, per_device(): call(functools.partial(attend_kernel, True, nope), (total_rows, packed_wi...  1.43 us
    pallas_call x1, Pallas kernels, per_device(): call(functools.partial(decode_kernel, nope), (count, heads * value_dim),...  1.22 us
    pallas_call x1, Pallas kernels, per_device(): call(query_latent_kernel, [(count, w_qdown.shape[1]), (count, w_qdown.sha...  0.8 us
    pallas_call x1, Pallas kernels, per_device(): call(functools.partial(combine_kernel, heads), (2 * count, model), [VMEM]...  0.68 us
  transfers between devices with their start and end apart: 7, of which 3 were waited for; matrix products, arithmetic and copies ran while one was open for 0% of the time, Pallas kernels for 9%

profile of v2, /device:TPU:0, one launch (start us, length us, event | category | flops | bytes accessed | tf_op | source)
XLA Modules:
  0.0 30.9 jit_solution(3681695393659714269)
XLA Ops:
  0.7 1.6 %copy-done.1 = bf16[2048,512]{1,0:T(8,128)(2,1)S(1)} copy-done((bf16[2048,512]{1,0:T(8,128)(2,1)S(1)}, bf16[2048,512]{1,0:T(8,128)(2,1)}, u32[]{:S(2)}) %copy-start.1) | copy-done | bytes 2097176
  2.2 0.8 %copy-done.8 = bf16[16,2048]{1,0:T(8,128)(2,1)S(1)} copy-done((bf16[16,2048]{1,0:T(8,128)(2,1)S(1)}, bf16[16,2048]{1,0:T(8,128)(2,1)}, u32[]{:S(2)}) %copy-start.8) | copy-done | bytes 65560
  3.1 0.7 %copy-done.15 = bf16[1,2048]{1,0:T(2,128)(2,1)S(1)} copy-done((bf16[1,2048]{1,0:T(2,128)(2,1)S(1)}, bf16[1,2048]{1,0:T(2,128)(2,1)}, u32[]{:S(2)}) %copy-start.15) | copy-done | bytes 4120
  3.8 0.7 %copy-done.18 = f32[512]{0:T(512)S(1)} copy-done((f32[512]{0:T(512)S(1)}, f32[512]{0:T(512)}, u32[]{:S(2)}) %copy-start.18) | copy-done | bytes 2072
  4.5 0.8 %query_latent.1 = (bf16[16,512]{1,0:T(8,128)(2,1)S(1)}, bf16[16,512]{1,0:T(8,128)(2,1)S(1)}) custom-call(bf16[16,2048]{1,0:T(8,128)(2,1)S(1)} %copy-done.8, bf16[1,2048]{1,0:T(2,128)(2,1)S(1)} %copy-done.15, bf16[2048,512]{1,0:T(8,128)(2,1)S(1)} %copy-done.1, f32[1,512]{1,0:T(1,128)S(1)} %bitcast.27), custom_call_target="tpu_custom_call" | custom-call | flops 67108864 | bytes 1048576 | tf_op jit(solution)/shard_map/query_latent/pallas_call | solution.py:399
  5.3 5.1 %collective-permute-start.2 = (bf16[16,512]{1,0:T(8,128)(2,1)S(1)}, bf16[16,512]{1,0:T(8,128)(2,1)S(1)}, u32[]{:S(2)}, u32[]{:S(2)}) collective-permute-start(bf16[16,512]{1,0:T(8,128)(2,1)S(1)} %get-tuple-element.29.refs_9_), channel_id=1, source_target_pairs={{0,6},{2,0},{4,2},{6,4},{1,7},{3,1},{5,3},{7,5},{8,14},{10,8},{12,... | collective-permute-start | bytes 49160 | tf_op jit(solution)/shard_map/ppermute | solution.py:349
  10.4 1.0 %collective-permute-start = (bf16[16,512]{1,0:T(8,128)(2,1)S(1)}, bf16[16,512]{1,0:T(8,128)(2,1)S(1)}, u32[]{:S(2)}, u32[]{:S(2)}) collective-permute-start(bf16[16,512]{1,0:T(8,128)(2,1)S(1)} %get-tuple-element.29.refs_9_), channel_id=1, source_target_pairs={{0,2},{2,4},{4,6},{6,0},{1,3},{3,5},{5,7},{7,1},{8,10},{10,12},{12... | collective-permute-start | bytes 49160 | tf_op jit(solution)/shard_map/ppermute | solution.py:349
  12.2 1.0 %copy-done.4 = bf16[512,8,64]{0,2,1:T(8,128)(2,1)S(1)} copy-done((bf16[512,8,64]{0,2,1:T(8,128)(2,1)S(1)}, bf16[512,8,64]{0,2,1:T(8,128)(2,1)}, u32[]{:S(2)}) %copy-start.4) | copy-done | bytes 524312
  13.2 1.0 %copy-done.6 = bf16[512,8,64]{0,2,1:T(8,128)(2,1)S(1)} copy-done((bf16[512,8,64]{0,2,1:T(8,128)(2,1)S(1)}, bf16[512,8,64]{0,2,1:T(8,128)(2,1)}, u32[]{:S(2)}) %copy-start.6) | copy-done | bytes 524312
  14.2 0.9 %copy-done.10 = bf16[256,512]{1,0:T(8,128)(2,1)S(1)} copy-done((bf16[256,512]{1,0:T(8,128)(2,1)S(1)}, bf16[256,512]{1,0:T(8,128)(2,1)}, u32[]{:S(2)}) %copy-start.10) | copy-done | bytes 262168
  15.2 0.8 %copy-done.11 = f32[64,128]{1,0:T(8,128)S(1)} copy-done((f32[64,128]{1,0:T(8,128)S(1)}, f32[64,128]{1,0:T(8,128)}, u32[]{:S(2)}) %copy-start.11) | copy-done | bytes 32792
  15.9 0.8 %copy-done.12 = f32[64,128]{1,0:T(8,128)S(1)} copy-done((f32[64,128]{1,0:T(8,128)S(1)}, f32[64,128]{1,0:T(8,128)}, u32[]{:S(2)}) %copy-start.12) | copy-done | bytes 32792
  16.7 0.9 %copy-done.13 = bf16[2048,32]{0,1:T(8,128)(2,1)S(1)} copy-done((bf16[2048,32]{0,1:T(8,128)(2,1)S(1)}, bf16[2048,32]{0,1:T(8,128)(2,1)}, u32[]{:S(2)}) %copy-start.13) | copy-done | bytes 131096
  17.6 1.6 %keys.1 = (bf16[16,512]{1,0:T(8,128)(2,1)}, bf16[1,512]{1,0:T(2,128)(2,1)}, bf16[16,32]{1,0:T(8,128)(2,1)}, bf16[1,32]{1,0:T(2,128)(2,1)}, bf16[256,512]{1,0:T(8...) custom-call(s32[1]{0:T(128)S(6)} %copy.25.lengths_ref, ...), custom_call_target="tpu_custom_call" | custom-call | flops 268435456 | bytes 4194304 | tf_op jit(solution)/shard_map/keys/pallas_call | solution.py:428
  19.3 1.4 %attend.1 = bf16[64,640]{1,0:T(8,128)(2,1)S(1)} custom-call(bf16[8,96,512]{2,1,0:T(8,128)(2,1)S(1)} %bitcast.16, bf16[256,512]{1,0:T(8,128)(2,1)S(1)} %get-tuple-element.24.refs_1_, bf16[256,512]{1,0:T(8,128)(2,1)S(1)} %get-tuple-element.25.refs_2_, bf16[16,512]{1,0:T(8,128)(2,1)S(1)} %get-tuple-element.26.refs_3_, ...), custom_call_target="tpu_custom_call" | custom-call | flops 33554432 | bytes 524288 | tf_op jit(solution)/shard_map/attend/pallas_call | solution.py:475
  20.7 2.5 %collective-permute-start.5 = (bf16[16,640]{1,0:T(8,128)(2,1)S(1)}, bf16[16,640]{1,0:T(8,128)(2,1)S(1)}, u32[]{:S(2)}, u32[]{:S(2)}) collective-permute-start(bf16[16,640]{1,0:T(8,128)(2,1)S(1)} %get-tuple-element.36), channel_id=1, source_target_pairs={{0,2},{2,4},{4,6},{6,0},{1,3},{3,5},{5,7},{7,1},{8,10},{10,12},{12... | collective-permute-start | bytes 61448 | tf_op jit(solution)/shard_map/ppermute | solution.py:349
  23.2 0.9 %collective-permute-start.4 = (bf16[16,640]{1,0:T(8,128)(2,1)S(1)}, bf16[16,640]{1,0:T(8,128)(2,1)S(1)}, u32[]{:S(2)}, u32[]{:S(2)}) collective-permute-start(bf16[16,640]{1,0:T(8,128)(2,1)S(1)} %get-tuple-element.37), channel_id=1, source_target_pairs={{0,4},{2,6},{4,0},{6,2},{1,5},{3,7},{5,1},{7,3},{8,12},{10,14},{12... | collective-permute-start | bytes 61448 | tf_op jit(solution)/shard_map/ppermute | solution.py:349
  24.1 1.5 %collective-permute-start.3 = (bf16[16,640]{1,0:T(8,128)(2,1)S(1)}, bf16[16,640]{1,0:T(8,128)(2,1)S(1)}, u32[]{:S(2)}, u32[]{:S(2)}) collective-permute-start(bf16[16,640]{1,0:T(8,128)(2,1)S(1)} %get-tuple-element.38), channel_id=1, source_target_pairs={{0,6},{2,0},{4,2},{6,4},{1,7},{3,1},{5,3},{7,5},{8,14},{10,8},{12,... | collective-permute-start | bytes 61448 | tf_op jit(solution)/shard_map/ppermute | solution.py:349
  25.7 1.2 %decode.1.dec_ref = bf16[16,512]{1,0:T(8,128)(2,1)S(1)} custom-call(s32[1]{0:T(128)S(6)} %copy.25.lengths_ref, bf16[16,512]{1,0:T(8,128)(2,1)S(1)} %get-tuple-element.21.q_ref, bf16[8,96,512]{2,1,0:T(8,128)(2,1)S(1)} %bitcast.17, bf16[512,512]{1,0:T(8,128)(2,1)S(1)} %bitcast.20, bf16[512,512]{1,0:T(8,128)(2,1)S(1)} %bitcast.22, ...), custom_call_target="tpu_custom_call" | custom-call | flops 67108864 | bytes 1048576 | tf_op jit(solution)/shard_map/decode/pallas_call | solution.py:502
  26.9 1.0 %collective-permute-done.4.refs_2_ = bf16[16,640]{1,0:T(8,128)(2,1)S(1)} collective-permute-done((bf16[16,640]{1,0:T(8,128)(2,1)S(1)}, bf16[16,640]{1,0:T(8,128)(2,1)S(1)}, u32[]{:S(2)}, u32[]{:S(2)}) %collective-permute-start.4) | collective-permute-done | bytes 20512 | tf_op jit(solution)/shard_map/ppermute | solution.py:349
  28.0 0.2 collective-permute-done.3.refs_1_
  28.2 0.7 %combine.1.refs_0_ = bf16[32,2048]{1,0:T(8,128)(2,1)S(1)} custom-call(bf16[16,512]{1,0:T(8,128)(2,1)S(1)} %decode.1.dec_ref, bf16[512,2048]{1,0:T(8,128)(2,1)S(1)} %bitcast.18, bf16[16,640]{1,0:T(8,128)(2,1)S(1)} %get-tuple-element.39.refs_0_, bf16[16,640]{1,0:T(8,128)(2,1)S(1)} %collective-permute-done.3.refs_1_, ...), custom_call_target="tpu_custom_call" | custom-call | flops 67108864 | bytes 1048576 | tf_op jit(solution)/shard_map/combine/pallas_call | solution.py:521
  28.9 1.3 %collective-permute-done.6.refs_1_ = bf16[32,2048]{1,0:T(8,128)(2,1)S(1)} collective-permute-done((bf16[32,2048]{1,0:T(8,128)(2,1)S(1)}, bf16[32,2048]{1,0:T(8,128)(2,1)S(1)}, u32[]{:S(2)}, u32[]{:S(2)}) %collective-permute-start.6) | collective-permute-done | bytes 131104 | tf_op jit(solution)/shard_map/ppermute | solution.py:349
  30.2 0.6 %add.1 = (bf16[16,2048]{1,0:T(8,128)(2,1)}, bf16[1,2048]{1,0:T(2,128)(2,1)}) custom-call(bf16[32,2048]{1,0:T(8,128)(2,1)S(1)} %combine.1.refs_0_, bf16[32,2048]{1,0:T(8,128)(2,1)S(1)} %collective-permute-done.6.refs_1_), custom_call_target="tpu_custom_call" | custom-call | flops 1000 | bytes 15 | tf_op jit(solution)/shard_map/add/pallas_call | solution.py:529
  (39 shorter events, 0.1 us)
Async XLA Ops:
  0.6 11.5 %copy-start.20 = (f32[1,128]{1,0:T(1,128)S(1)}, f32[1,128]{1,0:T(1,128)}, u32[]{:S(2)}) copy-start(f32[1,128]{1,0:T(1,128)} %constant.8.clone.freq_ref) | copy-start | bytes 1540
  0.6 1.6 %copy-start.1 = (bf16[2048,512]{1,0:T(8,128)(2,1)S(1)}, bf16[2048,512]{1,0:T(8,128)(2,1)}, u32[]{:S(2)}) copy-start(bf16[2048,512]{1,0:T(8,128)(2,1)} %w_hbm.1) | copy-start | bytes 6291460
  2.2 0.8 %copy-start.8 = (bf16[16,2048]{1,0:T(8,128)(2,1)S(1)}, bf16[16,2048]{1,0:T(8,128)(2,1)}, u32[]{:S(2)}) copy-start(bf16[16,2048]{1,0:T(8,128)(2,1)} %piece_ref.3) | copy-start | bytes 196612
  4.5 7.6 %copy-start.2 = (bf16[2048,512]{1,0:T(8,128)(2,1)S(1)}, bf16[2048,512]{1,0:T(8,128)(2,1)}, u32[]{:S(2)}) copy-start(bf16[2048,512]{1,0:T(8,128)(2,1)} %w_ref.1) | copy-start | bytes 6291460
  4.5 7.6 %copy-start.9 = (bf16[16,2048]{1,0:T(8,128)(2,1)S(1)}, bf16[16,2048]{1,0:T(8,128)(2,1)}, u32[]{:S(2)}) copy-start(bf16[16,2048]{1,0:T(8,128)(2,1)} %piece_ref.3) | copy-start | bytes 196612
  4.5 7.7 %copy-start.16 = (bf16[1,2048]{1,0:T(2,128)(2,1)S(1)}, bf16[1,2048]{1,0:T(2,128)(2,1)}, u32[]{:S(2)}) copy-start(bf16[1,2048]{1,0:T(2,128)(2,1)} %dec_ref.3) | copy-start | bytes 12292
  4.5 7.7 %copy-start.19 = (f32[512]{0:T(512)S(1)}, f32[512]{0:T(512)}, u32[]{:S(2)}) copy-start(f32[512]{0:T(512)} %param.31) | copy-start | bytes 6148
  5.3 14.0 %copy-start = (bf16[512,8,96]{0,2,1:T(8,128)(2,1)S(1)}, bf16[512,8,96]{0,2,1:T(8,128)(2,1)}, u32[]{:S(2)}) copy-start(bf16[512,8,96]{0,2,1:T(8,128)(2,1)} %param.28) | copy-start | bytes 2359300
  5.3 13.9 %collective-permute-start.2 = (bf16[16,512]{1,0:T(8,128)(2,1)S(1)}, bf16[16,512]{1,0:T(8,128)(2,1)S(1)}, u32[]{:S(2)}, u32[]{:S(2)}) collective-permute-start(bf16[16,512]{1,0:T(8,128)(2,1)S(1)} %get-tuple-element.29.refs_9_), channel_id=1, source_target_pairs={{0,6},{2,0},{4,2},{6,4},{1,7},{3,1},{5,3},{7,5},{8,14},{10,8},{12,... | collective-permute-start | bytes 49160 | tf_op jit(solution)/shard_map/ppermute | solution.py:349
  10.4 8.8 %collective-permute-start.1 = (bf16[16,512]{1,0:T(8,128)(2,1)S(1)}, bf16[16,512]{1,0:T(8,128)(2,1)S(1)}, u32[]{:S(2)}, u32[]{:S(2)}) collective-permute-start(bf16[16,512]{1,0:T(8,128)(2,1)S(1)} %get-tuple-element.29.refs_9_), channel_id=1, source_target_pairs={{0,4},{2,6},{4,0},{6,2},{1,5},{3,7},{5,1},{7,3},{8,12},{10,14},{12... | collective-permute-start | bytes 49160 | tf_op jit(solution)/shard_map/ppermute | solution.py:349
  10.4 8.8 %collective-permute-start = (bf16[16,512]{1,0:T(8,128)(2,1)S(1)}, bf16[16,512]{1,0:T(8,128)(2,1)S(1)}, u32[]{:S(2)}, u32[]{:S(2)}) collective-permute-start(bf16[16,512]{1,0:T(8,128)(2,1)S(1)} %get-tuple-element.29.refs_9_), channel_id=1, source_target_pairs={{0,2},{2,4},{4,6},{6,0},{1,3},{3,5},{5,7},{7,1},{8,10},{10,12},{12... | collective-permute-start | bytes 49160 | tf_op jit(solution)/shard_map/ppermute | solution.py:349
  12.1 1.0 %copy-start.4 = (bf16[512,8,64]{0,2,1:T(8,128)(2,1)S(1)}, bf16[512,8,64]{0,2,1:T(8,128)(2,1)}, u32[]{:S(2)}) copy-start(bf16[512,8,64]{0,2,1:T(8,128)(2,1)} %param.32) | copy-start | bytes 1572868
  13.2 1.0 %copy-start.6 = (bf16[512,8,64]{0,2,1:T(8,128)(2,1)S(1)}, bf16[512,8,64]{0,2,1:T(8,128)(2,1)}, u32[]{:S(2)}) copy-start(bf16[512,8,64]{0,2,1:T(8,128)(2,1)} %param.33) | copy-start | bytes 1572868
  14.2 0.9 %copy-start.10 = (bf16[256,512]{1,0:T(8,128)(2,1)S(1)}, bf16[256,512]{1,0:T(8,128)(2,1)}, u32[]{:S(2)}) copy-start(bf16[256,512]{1,0:T(8,128)(2,1)} %prompt_ref.1) | copy-start | bytes 786436
  16.7 0.9 %copy-start.13 = (bf16[2048,32]{0,1:T(8,128)(2,1)S(1)}, bf16[2048,32]{0,1:T(8,128)(2,1)}, u32[]{:S(2)}) copy-start(bf16[2048,32]{0,1:T(8,128)(2,1)} %param.30) | copy-start | bytes 393220
  17.6 1.6 %copy-start.17 = (bf16[256,32]{0,1:T(8,128)(2,1)S(1)}, bf16[256,32]{0,1:T(8,128)(2,1)}, u32[]{:S(2)}) copy-start(bf16[256,32]{0,1:T(8,128)(2,1)} %param.22) | copy-start | bytes 49156
  17.6 8.1 %copy-start.5 = (bf16[512,8,64]{0,2,1:T(8,128)(2,1)S(1)}, bf16[512,8,64]{0,2,1:T(8,128)(2,1)}, u32[]{:S(2)}) copy-start(bf16[512,8,64]{0,2,1:T(8,128)(2,1)} %param.32) | copy-start | bytes 1572868
  17.6 8.1 %copy-start.7 = (bf16[1,512,512]{2,1,0:T(8,128)(2,1)S(1)}, bf16[1,512,512]{2,1,0:T(8,128)(2,1)}, u32[]{:S(2)}) copy-start(bf16[1,512,512]{2,1,0:T(8,128)(2,1)} %param.23) | copy-start | bytes 1572868
  17.6 8.1 %copy-start.14 = (bf16[1,512,32]{1,2,0:T(8,128)(2,1)S(1)}, bf16[1,512,32]{1,2,0:T(8,128)(2,1)}, u32[]{:S(2)}) copy-start(bf16[1,512,32]{1,2,0:T(8,128)(2,1)} %param.24) | copy-start | bytes 98308
  19.2 8.9 %copy-start.3 = (bf16[8,64,2048]{2,1,0:T(8,128)(2,1)S(1)}, bf16[8,64,2048]{2,1,0:T(8,128)(2,1)}, u32[]{:S(2)}) copy-start(bf16[8,64,2048]{2,1,0:T(8,128)(2,1)} %param.34) | copy-start | bytes 6291460
  20.7 6.2 %collective-permute-start.5 = (bf16[16,640]{1,0:T(8,128)(2,1)S(1)}, bf16[16,640]{1,0:T(8,128)(2,1)S(1)}, u32[]{:S(2)}, u32[]{:S(2)}) collective-permute-start(bf16[16,640]{1,0:T(8,128)(2,1)S(1)} %get-tuple-element.36), channel_id=1, source_target_pairs={{0,2},{2,4},{4,6},{6,0},{1,3},{3,5},{5,7},{7,1},{8,10},{10,12},{12... | collective-permute-start | bytes 61448 | tf_op jit(solution)/shard_map/ppermute | solution.py:349
  23.2 4.7 %collective-permute-start.4 = (bf16[16,640]{1,0:T(8,128)(2,1)S(1)}, bf16[16,640]{1,0:T(8,128)(2,1)S(1)}, u32[]{:S(2)}, u32[]{:S(2)}) collective-permute-start(bf16[16,640]{1,0:T(8,128)(2,1)S(1)} %get-tuple-element.37), channel_id=1, source_target_pairs={{0,4},{2,6},{4,0},{6,2},{1,5},{3,7},{5,1},{7,3},{8,12},{10,14},{12... | collective-permute-start | bytes 61448 | tf_op jit(solution)/shard_map/ppermute | solution.py:349
  24.1 4.0 %collective-permute-start.3 = (bf16[16,640]{1,0:T(8,128)(2,1)S(1)}, bf16[16,640]{1,0:T(8,128)(2,1)S(1)}, u32[]{:S(2)}, u32[]{:S(2)}) collective-permute-start(bf16[16,640]{1,0:T(8,128)(2,1)S(1)} %get-tuple-element.38), channel_id=1, source_target_pairs={{0,6},{2,0},{4,2},{6,4},{1,7},{3,1},{5,3},{7,5},{8,14},{10,8},{12,... | collective-permute-start | bytes 61448 | tf_op jit(solution)/shard_map/ppermute | solution.py:349
  28.8 1.4 %collective-permute-start.6 = (bf16[32,2048]{1,0:T(8,128)(2,1)S(1)}, bf16[32,2048]{1,0:T(8,128)(2,1)S(1)}, u32[]{:S(2)}, u32[]{:S(2)}) collective-permute-start(bf16[32,2048]{1,0:T(8,128)(2,1)S(1)} %combine.1.refs_0_), channel_id=1, source_target_pairs={{0,1},{1,0},{2,3},{3,2},{4,5},{5,4},{6,7},{7,6},{8,9},{9,8},{10,11... | collective-permute-start | bytes 393224 | tf_op jit(solution)/shard_map/ppermute | solution.py:349
  (4 other events, 2.9 us)

commit v3 on v2

--- a/solution.py
+++ b/solution.py
@@ -59,14 +59,24 @@
     return jnp.broadcast_to(row.astype(F32), (rows, row.shape[1])).astype(row.dtype)
 
 
-def query_latent_kernel(piece_ref, dec_ref, w_hbm, gain_ref, out_ref, dec_out_ref, w_ref, sems):
-    chunks = sems.shape[0]
+def query_latent_kernel(
+    piece_hbm, dec_hbm, w_hbm, gain_hbm, out_ref, dec_out_ref, piece_ref, dec_ref, gain_ref, w_ref, sems
+):
+    chunks = sems.shape[0] - 3
     depth = w_ref.shape[0] // chunks
+    small = []
+    for c, (source, target) in enumerate(
+        [(piece_hbm, piece_ref), (dec_hbm, dec_ref), (gain_hbm, gain_ref)]
+    ):
+        small.append(pltpu.make_async_copy(source, target, sems.at[chunks + c]))
+        small[-1].start()
     copies = []
     for c in range(chunks):
         part = pl.ds(c * depth, depth)
         copies.append(pltpu.make_async_copy(w_hbm.at[part], w_ref.at[part], sems.at[c]))
         copies[-1].start()
+    for copy in small:
+        copy.wait()
     piece = piece_ref[...]
     rows = jnp.concatenate([piece, spread_rows(dec_ref[...], piece.shape[0])], 0)
     total = jnp.zeros((rows.shape[0], w_ref.shape[1]), F32)
@@ -349,6 +359,10 @@
     return lax.ppermute(values, axis, [(i, (i + step) % size) for i in range(size)])
 
 
+def in_hbm(array):
+    return pltpu.with_memory_space_constraint(array, pltpu.HBM)
+
+
 def rope_tables(context, rows, rope):
     half = rope // 2
     inverse = ROPE_BASE ** (-np.arange(half, dtype=np.float32) * 2.0 / rope)
@@ -399,11 +413,17 @@
     q_latent, q_decode = call(
         query_latent_kernel,
         [(count, w_qdown.shape[1]), (count, w_qdown.shape[1])],
-        [VMEM, VMEM, HBM, VMEM],
+        [HBM, HBM, HBM, HBM],
         "query_latent",
-        2 * 2 * count * model * w_qdown.shape[1],
-        scratch_shapes=[pltpu.VMEM(w_qdown.shape, BF16), pltpu.SemaphoreType.DMA((4,))],
-    )(piece_rows, decode_rows, w_qdown, q_gain[None, :])
+        2 * 2 * count * model * w_qdown.shape[1] * 100,
+        scratch_shapes=[
+            pltpu.VMEM(piece_rows.shape, BF16),
+            pltpu.VMEM(decode_rows.shape, BF16),
+            pltpu.VMEM((1, q_gain.shape[0]), F32),
+            pltpu.VMEM(w_qdown.shape, BF16),
+            pltpu.SemaphoreType.DMA((7,)),
+        ],
+    )(*[in_hbm(array) for array in (piece_rows, decode_rows, w_qdown, q_gain[None, :])])
 
     direct = shards <= MAX_PERMUTES
     if direct:

time: 31.4 us -> 24 us (0.76); the launches traced: 30.9 us -> 23.9 us
  local copies, waits for them, and re-layouts: 9.31 us -> 0.09 us
  waiting for transfers between devices: 2.55 us -> 4.32 us
  Pallas kernels: 6.38 us -> 7.65 us
  starting transfers between devices: 11.2 us -> 10.3 us
    unnamed x42 -> x32, local copies, waits for them, and re-layouts: 9.3 us -> 0.08 us
    ppermute x7, waiting for transfers between devices: 2.55 us -> 4.32 us  [shift(): lax.ppermute(values, axis, [(i, (i + step) % size) for i in range(size)])]
    pallas_call x1, Pallas kernels: 0.8 us -> 2.05 us  [per_device(): call(query_latent_kernel, [(count, w_qdown.shape[1]), (count, w_qdown.sha...]
    ppermute x7, starting transfers between devices: 11.2 us -> 10.3 us  [shift(): lax.ppermute(values, axis, [(i, (i + step) % size) for i in range(size)])]
  transfers between devices with their start and end apart: 7 -> 7, of which waited for: 3 -> 5; matrix products, arithmetic and copies ran while one was open for 0% -> 0% of each run, Pallas kernels for 9% -> 12%
where the time goes in v3:
time: 24 us; the launch traced here: 23.9 us
  starting transfers between devices  10.3 us (43%)
  Pallas kernels  7.65 us (32%)
  waiting for transfers between devices  4.32 us (18%)
  between operations  1.54 us (6%)
    ppermute x7, starting transfers between devices, shift(): lax.ppermute(values, axis, [(i, (i + step) % size) for i in range(size)])  10.3 us
    ppermute x7, waiting for transfers between devices, shift(): lax.ppermute(values, axis, [(i, (i + step) % size) for i in range(size)])  4.32 us
    pallas_call x1, Pallas kernels, per_device(): call(query_latent_kernel, [(count, w_qdown.shape[1]), (count, w_qdown.sha...  2.05 us
    pallas_call x1, Pallas kernels, per_device(): call(functools.partial(keys_kernel, context), [(count, width), (1, width)...  1.61 us
    pallas_call x1, Pallas kernels, per_device(): call(functools.partial(attend_kernel, True, nope), (total_rows, packed_wi...  1.43 us
    pallas_call x1, Pallas kernels, per_device(): call(functools.partial(decode_kernel, nope), (count, heads * value_dim),...  1.22 us
    pallas_call x1, Pallas kernels, per_device(): call(functools.partial(combine_kernel, heads), (2 * count, model), [VMEM]...  0.68 us
    pallas_call x1, Pallas kernels, per_device(): call(add_kernel, [(count, model), (1, model)], [VMEM] * len(terms), 'add'...  0.65 us
  transfers between devices with their start and end apart: 7, of which 5 were waited for; matrix products, arithmetic and copies ran while one was open for 0% of the time, Pallas kernels for 12%

profile of v3, /device:TPU:0, one launch (start us, length us, event | category | flops | bytes accessed | tf_op | source)
XLA Modules:
  0.0 23.9 jit_solution(708522588111041473)
XLA Ops:
  0.7 0.0 copy-start.7
  0.7 0.0 copy-start.8
  0.7 0.0 copy-start.15
  0.8 2.1 %query_latent.1 = (bf16[16,512]{1,0:T(8,128)(2,1)S(1)}, bf16[16,512]{1,0:T(8,128)(2,1)S(1)}) custom-call(bf16[16,2048]{1,0:T(8,128)(2,1)} %piece_ref.1, bf16[1,2048]{1,0:T(2,128)(2,1)} %dec_ref.1, bf16[2048,512]{1,0:T(8,128)(2,1)} %w_hbm.1, f32[1,512]{1,0:T(1,128)} %bitcast.28), custom_call_target="tpu_custom_call" | custom-call | flops 6710886400 | bytes 104857600 | tf_op jit(solution)/shard_map/query_latent/pallas_call | solution.py:413
  2.8 0.0 copy-start
  2.8 0.0 copy-start.12
  2.8 5.1 %collective-permute-start.2 = (bf16[16,512]{1,0:T(8,128)(2,1)S(1)}, bf16[16,512]{1,0:T(8,128)(2,1)S(1)}, u32[]{:S(2)}, u32[]{:S(2)}) collective-permute-start(bf16[16,512]{1,0:T(8,128)(2,1)S(1)} %get-tuple-element.29.refs_9_), channel_id=1, source_target_pairs={{0,6},{2,0},{4,2},{6,4},{1,7},{3,1},{5,3},{7,5},{8,14},{10,8},{12,... | collective-permute-start | bytes 49160 | tf_op jit(solution)/shard_map/ppermute | solution.py:359
  8.0 1.0 %collective-permute-start = (bf16[16,512]{1,0:T(8,128)(2,1)S(1)}, bf16[16,512]{1,0:T(8,128)(2,1)S(1)}, u32[]{:S(2)}, u32[]{:S(2)}) collective-permute-start(bf16[16,512]{1,0:T(8,128)(2,1)S(1)} %get-tuple-element.29.refs_9_), channel_id=1, source_target_pairs={{0,2},{2,4},{4,6},{6,0},{1,3},{3,5},{5,7},{7,1},{8,10},{10,12},{12... | collective-permute-start | bytes 49160 | tf_op jit(solution)/shard_map/ppermute | solution.py:359
  9.7 0.0 copy-start.5
  9.8 0.0 copy-start.11
  9.8 1.6 %keys.1 = (bf16[16,512]{1,0:T(8,128)(2,1)}, bf16[1,512]{1,0:T(2,128)(2,1)}, bf16[16,32]{1,0:T(8,128)(2,1)}, bf16[1,32]{1,0:T(2,128)(2,1)}, bf16[256,512]{1,0:T(8...) custom-call(s32[1]{0:T(128)S(6)} %copy.25.lengths_ref, ...), custom_call_target="tpu_custom_call" | custom-call | flops 268435456 | bytes 4194304 | tf_op jit(solution)/shard_map/keys/pallas_call | solution.py:448
  11.4 1.2 %collective-permute-done.1.refs_11_ = bf16[16,512]{1,0:T(8,128)(2,1)S(1)} collective-permute-done((bf16[16,512]{1,0:T(8,128)(2,1)S(1)}, bf16[16,512]{1,0:T(8,128)(2,1)S(1)}, u32[]{:S(2)}, u32[]{:S(2)}) %collective-permute-start.1) | collective-permute-done | bytes 16416 | tf_op jit(solution)/shard_map/ppermute | solution.py:359
  12.6 0.9 %collective-permute-done.refs_10_ = bf16[16,512]{1,0:T(8,128)(2,1)S(1)} collective-permute-done((bf16[16,512]{1,0:T(8,128)(2,1)S(1)}, bf16[16,512]{1,0:T(8,128)(2,1)S(1)}, u32[]{:S(2)}, u32[]{:S(2)}) %collective-permute-start) | collective-permute-done | bytes 16416 | tf_op jit(solution)/shard_map/ppermute | solution.py:359
  13.5 1.4 %attend.1 = bf16[64,640]{1,0:T(8,128)(2,1)S(1)} custom-call(bf16[8,96,512]{2,1,0:T(8,128)(2,1)S(1)} %bitcast.16, bf16[256,512]{1,0:T(8,128)(2,1)S(1)} %get-tuple-element.24.refs_1_, bf16[256,512]{1,0:T(8,128)(2,1)S(1)} %get-tuple-element.25.refs_2_, bf16[16,512]{1,0:T(8,128)(2,1)S(1)} %get-tuple-element.26.refs_3_, ...), custom_call_target="tpu_custom_call" | custom-call | flops 33554432 | bytes 524288 | tf_op jit(solution)/shard_map/attend/pallas_call | solution.py:495
  15.0 0.4 %collective-permute-start.5 = (bf16[16,640]{1,0:T(8,128)(2,1)S(1)}, bf16[16,640]{1,0:T(8,128)(2,1)S(1)}, u32[]{:S(2)}, u32[]{:S(2)}) collective-permute-start(bf16[16,640]{1,0:T(8,128)(2,1)S(1)} %get-tuple-element.36), channel_id=1, source_target_pairs={{0,2},{2,4},{4,6},{6,0},{1,3},{3,5},{5,7},{7,1},{8,10},{10,12},{12... | collective-permute-start | bytes 61448 | tf_op jit(solution)/shard_map/ppermute | solution.py:359
  15.4 0.9 %collective-permute-start.4 = (bf16[16,640]{1,0:T(8,128)(2,1)S(1)}, bf16[16,640]{1,0:T(8,128)(2,1)S(1)}, u32[]{:S(2)}, u32[]{:S(2)}) collective-permute-start(bf16[16,640]{1,0:T(8,128)(2,1)S(1)} %get-tuple-element.37), channel_id=1, source_target_pairs={{0,4},{2,6},{4,0},{6,2},{1,5},{3,7},{5,1},{7,3},{8,12},{10,14},{12... | collective-permute-start | bytes 61448 | tf_op jit(solution)/shard_map/ppermute | solution.py:359
  16.3 2.8 %collective-permute-start.3 = (bf16[16,640]{1,0:T(8,128)(2,1)S(1)}, bf16[16,640]{1,0:T(8,128)(2,1)S(1)}, u32[]{:S(2)}, u32[]{:S(2)}) collective-permute-start(bf16[16,640]{1,0:T(8,128)(2,1)S(1)} %get-tuple-element.38), channel_id=1, source_target_pairs={{0,6},{2,0},{4,2},{6,4},{1,7},{3,1},{5,3},{7,5},{8,14},{10,8},{12,... | collective-permute-start | bytes 61448 | tf_op jit(solution)/shard_map/ppermute | solution.py:359
  19.1 1.2 %decode.1.dec_ref = bf16[16,512]{1,0:T(8,128)(2,1)S(1)} custom-call(s32[1]{0:T(128)S(6)} %copy.25.lengths_ref, bf16[16,512]{1,0:T(8,128)(2,1)S(1)} %get-tuple-element.21.q_ref, bf16[8,96,512]{2,1,0:T(8,128)(2,1)S(1)} %bitcast.17, bf16[512,512]{1,0:T(8,128)(2,1)S(1)} %bitcast.20, bf16[512,512]{1,0:T(8,128)(2,1)S(1)} %bitcast.22, ...), custom_call_target="tpu_custom_call" | custom-call | flops 67108864 | bytes 1048576 | tf_op jit(solution)/shard_map/decode/pallas_call | solution.py:522
  20.3 0.3 %collective-permute-done.5.refs_3_ = bf16[16,640]{1,0:T(8,128)(2,1)S(1)} collective-permute-done((bf16[16,640]{1,0:T(8,128)(2,1)S(1)}, bf16[16,640]{1,0:T(8,128)(2,1)S(1)}, u32[]{:S(2)}, u32[]{:S(2)}) %collective-permute-start.5) | collective-permute-done | bytes 20512 | tf_op jit(solution)/shard_map/ppermute | solution.py:359
  20.6 0.6 %collective-permute-done.3.refs_1_ = bf16[16,640]{1,0:T(8,128)(2,1)S(1)} collective-permute-done((bf16[16,640]{1,0:T(8,128)(2,1)S(1)}, bf16[16,640]{1,0:T(8,128)(2,1)S(1)}, u32[]{:S(2)}, u32[]{:S(2)}) %collective-permute-start.3) | collective-permute-done | bytes 20512 | tf_op jit(solution)/shard_map/ppermute | solution.py:359
  21.2 0.7 %combine.1.refs_0_ = bf16[32,2048]{1,0:T(8,128)(2,1)S(1)} custom-call(bf16[16,512]{1,0:T(8,128)(2,1)S(1)} %decode.1.dec_ref, bf16[512,2048]{1,0:T(8,128)(2,1)S(1)} %bitcast.18, bf16[16,640]{1,0:T(8,128)(2,1)S(1)} %get-tuple-element.39.refs_0_, bf16[16,640]{1,0:T(8,128)(2,1)S(1)} %collective-permute-done.3.refs_1_, ...), custom_call_target="tpu_custom_call" | custom-call | flops 67108864 | bytes 1048576 | tf_op jit(solution)/shard_map/combine/pallas_call | solution.py:541
  21.9 0.0 collective-permute-start.6
  21.9 1.3 %collective-permute-done.6.refs_1_ = bf16[32,2048]{1,0:T(8,128)(2,1)S(1)} collective-permute-done((bf16[32,2048]{1,0:T(8,128)(2,1)S(1)}, bf16[32,2048]{1,0:T(8,128)(2,1)S(1)}, u32[]{:S(2)}, u32[]{:S(2)}) %collective-permute-start.6) | collective-permute-done | bytes 131104 | tf_op jit(solution)/shard_map/ppermute | solution.py:359
  23.2 0.6 %add.1 = (bf16[16,2048]{1,0:T(8,128)(2,1)}, bf16[1,2048]{1,0:T(2,128)(2,1)}) custom-call(bf16[32,2048]{1,0:T(8,128)(2,1)S(1)} %combine.1.refs_0_, bf16[32,2048]{1,0:T(8,128)(2,1)S(1)} %collective-permute-done.6.refs_1_), custom_call_target="tpu_custom_call" | custom-call | flops 1000 | bytes 15 | tf_op jit(solution)/shard_map/add/pallas_call | solution.py:549
  (29 shorter events, 0.1 us)
Async XLA Ops:
  0.6 9.0 %copy-start.1 = (bf16[2048,512]{1,0:T(8,128)(2,1)S(1)}, bf16[2048,512]{1,0:T(8,128)(2,1)}, u32[]{:S(2)}) copy-start(bf16[2048,512]{1,0:T(8,128)(2,1)} %w_ref.1) | copy-start | bytes 6291460
  0.6 9.0 %copy-start.3 = (bf16[512,8,64]{0,2,1:T(8,128)(2,1)S(1)}, bf16[512,8,64]{0,2,1:T(8,128)(2,1)}, u32[]{:S(2)}) copy-start(bf16[512,8,64]{0,2,1:T(8,128)(2,1)} %param.32) | copy-start | bytes 1572868
  0.7 9.0 %copy-start.4 = (bf16[512,8,64]{0,2,1:T(8,128)(2,1)S(1)}, bf16[512,8,64]{0,2,1:T(8,128)(2,1)}, u32[]{:S(2)}) copy-start(bf16[512,8,64]{0,2,1:T(8,128)(2,1)} %param.33) | copy-start | bytes 1572868
  0.7 9.0 %copy-start.6 = (bf16[256,512]{1,0:T(8,128)(2,1)S(1)}, bf16[256,512]{1,0:T(8,128)(2,1)}, u32[]{:S(2)}) copy-start(bf16[256,512]{1,0:T(8,128)(2,1)} %prompt_ref.1) | copy-start | bytes 786436
  0.7 9.0 %copy-start.7 = (f32[64,128]{1,0:T(8,128)S(1)}, f32[64,128]{1,0:T(8,128)}, u32[]{:S(2)}) copy-start(f32[64,128]{1,0:T(8,128)} %constant.7.clone.sin_ref.refs_8_) | copy-start | bytes 98308
  0.7 9.0 %copy-start.8 = (f32[64,128]{1,0:T(8,128)S(1)}, f32[64,128]{1,0:T(8,128)}, u32[]{:S(2)}) copy-start(f32[64,128]{1,0:T(8,128)} %constant.6.clone.cos_ref.refs_7_) | copy-start | bytes 98308
  0.7 9.0 %copy-start.9 = (bf16[2048,32]{0,1:T(8,128)(2,1)S(1)}, bf16[2048,32]{0,1:T(8,128)(2,1)}, u32[]{:S(2)}) copy-start(bf16[2048,32]{0,1:T(8,128)(2,1)} %param.30) | copy-start | bytes 393220
  0.7 9.0 %copy-start.10 = (bf16[16,2048]{1,0:T(8,128)(2,1)S(1)}, bf16[16,2048]{1,0:T(8,128)(2,1)}, u32[]{:S(2)}) copy-start(bf16[16,2048]{1,0:T(8,128)(2,1)} %piece_ref.1) | copy-start | bytes 196612
  0.7 9.0 %copy-start.13 = (bf16[1,2048]{1,0:T(2,128)(2,1)S(1)}, bf16[1,2048]{1,0:T(2,128)(2,1)}, u32[]{:S(2)}) copy-start(bf16[1,2048]{1,0:T(2,128)(2,1)} %dec_ref.1) | copy-start | bytes 12292
  0.7 9.0 %copy-start.14 = (f32[512]{0:T(512)S(1)}, f32[512]{0:T(512)}, u32[]{:S(2)}) copy-start(f32[512]{0:T(512)} %param.31) | copy-start | bytes 6148
  0.7 9.0 %copy-start.15 = (f32[1,128]{1,0:T(1,128)S(1)}, f32[1,128]{1,0:T(1,128)}, u32[]{:S(2)}) copy-start(f32[1,128]{1,0:T(1,128)} %constant.8.clone.freq_ref) | copy-start | bytes 1540
  2.8 10.7 %copy-start = (bf16[512,8,96]{0,2,1:T(8,128)(2,1)S(1)}, bf16[512,8,96]{0,2,1:T(8,128)(2,1)}, u32[]{:S(2)}) copy-start(bf16[512,8,96]{0,2,1:T(8,128)(2,1)} %param.28) | copy-start | bytes 2359300
  2.8 10.7 %copy-start.12 = (bf16[256,32]{0,1:T(8,128)(2,1)S(1)}, bf16[256,32]{0,1:T(8,128)(2,1)}, u32[]{:S(2)}) copy-start(bf16[256,32]{0,1:T(8,128)(2,1)} %param.22) | copy-start | bytes 49156
  2.8 8.5 %collective-permute-start.2 = (bf16[16,512]{1,0:T(8,128)(2,1)S(1)}, bf16[16,512]{1,0:T(8,128)(2,1)S(1)}, u32[]{:S(2)}, u32[]{:S(2)}) collective-permute-start(bf16[16,512]{1,0:T(8,128)(2,1)S(1)} %get-tuple-element.29.refs_9_), channel_id=1, source_target_pairs={{0,6},{2,0},{4,2},{6,4},{1,7},{3,1},{5,3},{7,5},{8,14},{10,8},{12,... | collective-permute-start | bytes 49160 | tf_op jit(solution)/shard_map/ppermute | solution.py:359
  8.0 4.6 %collective-permute-start.1 = (bf16[16,512]{1,0:T(8,128)(2,1)S(1)}, bf16[16,512]{1,0:T(8,128)(2,1)S(1)}, u32[]{:S(2)}, u32[]{:S(2)}) collective-permute-start(bf16[16,512]{1,0:T(8,128)(2,1)S(1)} %get-tuple-element.29.refs_9_), channel_id=1, source_target_pairs={{0,4},{2,6},{4,0},{6,2},{1,5},{3,7},{5,1},{7,3},{8,12},{10,14},{12... | collective-permute-start | bytes 49160 | tf_op jit(solution)/shard_map/ppermute | solution.py:359
  8.0 5.5 %collective-permute-start = (bf16[16,512]{1,0:T(8,128)(2,1)S(1)}, bf16[16,512]{1,0:T(8,128)(2,1)S(1)}, u32[]{:S(2)}, u32[]{:S(2)}) collective-permute-start(bf16[16,512]{1,0:T(8,128)(2,1)S(1)} %get-tuple-element.29.refs_9_), channel_id=1, source_target_pairs={{0,2},{2,4},{4,6},{6,0},{1,3},{3,5},{5,7},{7,1},{8,10},{10,12},{12... | collective-permute-start | bytes 49160 | tf_op jit(solution)/shard_map/ppermute | solution.py:359
  9.7 9.3 %copy-start.5 = (bf16[1,512,512]{2,1,0:T(8,128)(2,1)S(1)}, bf16[1,512,512]{2,1,0:T(8,128)(2,1)}, u32[]{:S(2)}) copy-start(bf16[1,512,512]{2,1,0:T(8,128)(2,1)} %param.23) | copy-start | bytes 1572868
  9.8 9.3 %copy-start.11 = (bf16[1,512,32]{1,2,0:T(8,128)(2,1)S(1)}, bf16[1,512,32]{1,2,0:T(8,128)(2,1)}, u32[]{:S(2)}) copy-start(bf16[1,512,32]{1,2,0:T(8,128)(2,1)} %param.24) | copy-start | bytes 98308
  13.5 7.7 %copy-start.2 = (bf16[8,64,2048]{2,1,0:T(8,128)(2,1)S(1)}, bf16[8,64,2048]{2,1,0:T(8,128)(2,1)}, u32[]{:S(2)}) copy-start(bf16[8,64,2048]{2,1,0:T(8,128)(2,1)} %param.34) | copy-start | bytes 6291460
  15.0 5.6 %collective-permute-start.5 = (bf16[16,640]{1,0:T(8,128)(2,1)S(1)}, bf16[16,640]{1,0:T(8,128)(2,1)S(1)}, u32[]{:S(2)}, u32[]{:S(2)}) collective-permute-start(bf16[16,640]{1,0:T(8,128)(2,1)S(1)} %get-tuple-element.36), channel_id=1, source_target_pairs={{0,2},{2,4},{4,6},{6,0},{1,3},{3,5},{5,7},{7,1},{8,10},{10,12},{12... | collective-permute-start | bytes 61448 | tf_op jit(solution)/shard_map/ppermute | solution.py:359
  15.4 5.2 %collective-permute-start.4 = (bf16[16,640]{1,0:T(8,128)(2,1)S(1)}, bf16[16,640]{1,0:T(8,128)(2,1)S(1)}, u32[]{:S(2)}, u32[]{:S(2)}) collective-permute-start(bf16[16,640]{1,0:T(8,128)(2,1)S(1)} %get-tuple-element.37), channel_id=1, source_target_pairs={{0,4},{2,6},{4,0},{6,2},{1,5},{3,7},{5,1},{7,3},{8,12},{10,14},{12... | collective-permute-start | bytes 61448 | tf_op jit(solution)/shard_map/ppermute | solution.py:359
  16.3 4.9 %collective-permute-start.3 = (bf16[16,640]{1,0:T(8,128)(2,1)S(1)}, bf16[16,640]{1,0:T(8,128)(2,1)S(1)}, u32[]{:S(2)}, u32[]{:S(2)}) collective-permute-start(bf16[16,640]{1,0:T(8,128)(2,1)S(1)} %get-tuple-element.38), channel_id=1, source_target_pairs={{0,6},{2,0},{4,2},{6,4},{1,7},{3,1},{5,3},{7,5},{8,14},{10,8},{12,... | collective-permute-start | bytes 61448 | tf_op jit(solution)/shard_map/ppermute | solution.py:359
  21.9 1.4 %collective-permute-start.6 = (bf16[32,2048]{1,0:T(8,128)(2,1)S(1)}, bf16[32,2048]{1,0:T(8,128)(2,1)S(1)}, u32[]{:S(2)}, u32[]{:S(2)}) collective-permute-start(bf16[32,2048]{1,0:T(8,128)(2,1)S(1)} %combine.1.refs_0_), channel_id=1, source_target_pairs={{0,1},{1,0},{2,3},{3,2},{4,5},{5,4},{6,7},{7,6},{8,9},{9,8},{10,11... | collective-permute-start | bytes 393224 | tf_op jit(solution)/shard_map/ppermute | solution.py:359

commit v4 on v3

--- a/solution.py
+++ b/solution.py
@@ -13,7 +13,6 @@
 MAX_PERMUTES = 8
 ROPE_BASE = 10000.0
 VMEM = pl.BlockSpec(memory_space=pltpu.VMEM)
-SMEM = pl.BlockSpec(memory_space=pltpu.SMEM)
 HBM = pl.BlockSpec(memory_space=pltpu.HBM)
 NT = (((1,), (1,)), ((), ()))
 F32 = jnp.float32
@@ -60,13 +59,27 @@
 
 
 def query_latent_kernel(
-    piece_hbm, dec_hbm, w_hbm, gain_hbm, out_ref, dec_out_ref, piece_ref, dec_ref, gain_ref, w_ref, sems
+    piece_hbm,
+    dec_hbm,
+    w_hbm,
+    gain_hbm,
+    out_ref,
+    dec_out_ref,
+    piece_ref,
+    dec_ref,
+    gain_ref,
+    w_ref,
+    sems,
 ):
     chunks = sems.shape[0] - 3
     depth = w_ref.shape[0] // chunks
     small = []
     for c, (source, target) in enumerate(
-        [(piece_hbm, piece_ref), (dec_hbm, dec_ref), (gain_hbm, gain_ref)]
+        [
+            (piece_hbm, piece_ref),
+            (dec_hbm, dec_ref),
+            (gain_hbm, gain_ref),
+        ]
     ):
         small.append(pltpu.make_async_copy(source, target, sems.at[chunks + c]))
         small[-1].start()
@@ -111,9 +124,6 @@
     value_ref,
     new_key_ref,
     new_value_ref,
-    new_rope_ref,
-    dec_rows_ref,
-    dec_rope_rows_ref,
 ):
     count = piece_ref.shape[0]
     rope = w_rope_ref.shape[0]
@@ -125,16 +135,13 @@
     index = lax.axis_index("kv")
     own = pl.ds(pl.multiple_of(index * count, count), count)
     new_rope = turn(raw[:count], cos_ref[own, :], sin_ref[own, :], rope).astype(BF16)
-    angle = lengths_ref[0].astype(F32) * freq_ref[...]
+    angle = lengths_ref[...] * freq_ref[...]
     sign = jnp.where(lane_index(angle.shape) % rope < rope // 2, -1.0, 1.0)
     dec_rope = turn(raw[count:], jnp.cos(angle), jnp.sin(angle) * sign, rope).astype(BF16)
     latent_ref[...] = latent[:count]
-    dec_latent_ref[...] = latent[count : count + 1]
-    rope_ref[...] = new_rope[:, :rope]
-    dec_rope_ref[...] = dec_rope[:1, :rope]
-    new_rope_ref[...] = new_rope
-    dec_rows_ref[...] = latent[count:]
-    dec_rope_rows_ref[...] = dec_rope
+    dec_latent_ref[...] = latent[count:]
+    rope_ref[...] = new_rope
+    dec_rope_ref[...] = dec_rope
     w_kup, w_vup = w_kup_ref[...], w_vup_ref[...]
     prompt = prompt_ref[...]
     key_ref[...] = dot_nt(prompt, w_kup).astype(BF16)
@@ -150,7 +157,7 @@
     return w_nope, w_rope
 
 
-def attend_kernel(relative, nope, *refs):
+def attend_kernel(slots, nope, *refs):
     (
         w_ref,
         key_ref,
@@ -162,19 +169,23 @@
         cos_ref,
         sin_ref,
     ) = refs[:9]
-    latent_refs, out_ref = refs[9:-1], refs[-1]
-    shards = lax.axis_size("kv")
     index = lax.axis_index("kv")
+    part = lax.axis_index("tp")
+    if slots:
+        shards = len(slots)
+        latent_refs, out_refs, out_ref = refs[9 : 9 + shards], refs[9 + shards : -1], refs[-1]
+    else:
+        latent_refs, out_ref = refs[9:-1], refs[-1]
     heads = w_ref.shape[0]
     rope = w_ref.shape[1] - nope
     count = new_key_ref.shape[0]
     latents = jnp.concatenate([ref[...] for ref in latent_refs], 0)
+    if slots:
+        owners = [lax.rem(index - pick(part, steps) + shards, shards) for steps in slots]
+    else:
+        first = pl.program_id(0) * (latents.shape[0] // count)
+        owners = [first + s for s in range(latents.shape[0] // count)]
     queries = latents.shape[0]
-    blocks = queries // count
-    first = 0 if relative else pl.program_id(0) * blocks
-    owners = []
-    for s in range(blocks):
-        owners.append(lax.rem(index - s + shards, shards) if relative else first + s)
     tables = [pl.ds(pl.multiple_of(owner * count, count), count) for owner in owners]
     cosine = jnp.concatenate([cos_ref[part, :] for part in tables], 0)
     sine = jnp.concatenate([sin_ref[part, :] for part in tables], 0)
@@ -210,15 +221,15 @@
             new.astype(BF16), new_value_ref[:, wide]
         )
         owner_lane = lane_index((queries, GROUP)) // nope
-        part = jnp.zeros((queries, GROUP), F32)
+        kept = jnp.zeros((queries, GROUP), F32)
         for j in range(per):
             own = slice(j * queries, (j + 1) * queries)
-            part = jnp.where(owner_lane == j, mixed[own], part)
+            kept = jnp.where(owner_lane == j, mixed[own], kept)
             h = g * per + j
             stats = jnp.where(
                 lane % heads == h, jnp.where(lane < 3 * heads, top[own], total[own]), stats
             )
-        out_ref[:, wide] = part.astype(BF16)
+        out_ref[:, wide] = kept.astype(BF16)
     high = stats.astype(BF16).astype(F32)
     rest = stats - high
     middle = rest.astype(BF16).astype(F32)
@@ -226,6 +237,10 @@
     stats = jnp.where(piece == 0, high, jnp.where(piece == 1, middle, rest - middle))
     stats = jnp.where(lane < 6 * heads, stats, 0.0)
     out_ref[:, heads * nope :] = stats.astype(BF16)
+    if slots:
+        for back, ref in enumerate(out_refs):
+            places = [[steps[t] for steps in slots].index(back) for t in range(len(slots[0]))]
+            ref[...] = block_at(out_ref, pick(part, places), count)
 
 
 def decode_kernel(
@@ -240,18 +255,28 @@
     new_latent_ref,
     new_rope_ref,
     freq_ref,
+    piece_latent_ref,
+    piece_rope_ref,
     out_ref,
+    latent_out_ref,
+    dec_latent_out_ref,
+    rope_out_ref,
+    dec_rope_out_ref,
 ):
     heads = w_ref.shape[0]
     rope = w_ref.shape[1] - nope
-    length = lengths_ref[0]
+    latent_out_ref[...] = piece_latent_ref[...]
+    dec_latent_out_ref[...] = new_latent_ref[:1, :]
+    rope_out_ref[...] = piece_rope_ref[:, :rope]
+    dec_rope_out_ref[...] = new_rope_ref[:1, :rope]
+    length = lengths_ref[...]
     scale = (nope + rope) ** (-0.5)
     latents = q_ref[...]
     rows = latents.shape[0]
     w_nope, w_rope = split_query_weights(w_ref, nope)
     q_nope = dot_nt(latents, w_nope)
     q_rope = dot_nt(latents, w_rope)
-    angle = length.astype(F32) * freq_ref[...]
+    angle = length * freq_ref[...]
     sign = jnp.where(lane_index(angle.shape) % rope < rope // 2, -1.0, 1.0)
     cosine, sine = jnp.cos(angle), jnp.sin(angle) * sign
     shape = q_nope.shape
@@ -269,7 +294,7 @@
     spread_rope = jnp.where(own_lane, turned, 0.0).astype(BF16)
     rope_keys = jnp.concatenate([rope_ref[...]] * heads, 0)
     cached = (dot_nt(absorbed, latent_ref[...]) + dot(spread_rope, rope_keys)) * scale
-    cached = jnp.where(lane_index(cached.shape) < length, cached, -1e30)
+    cached = jnp.where(lane_index(cached.shape).astype(F32) < length[:, :1], cached, -1e30)
     new_latent = new_latent_ref[...].astype(F32)
     new_rope = jnp.concatenate([new_rope_ref[...].astype(F32)] * (heads * rope // LANES), 1)
     own = (
@@ -291,13 +316,13 @@
 
 
 def combine_kernel(heads, dec_ref, w_ref, *refs):
-    got_refs, out_ref = refs[:-1], refs[-1]
     count = dec_ref.shape[0]
+    got, out_ref = [ref[...] for ref in refs[:-1]], refs[-1]
     width = w_ref.shape[0]
     value_dim = width // heads
 
-    def read(ref):
-        tail = ref[:, width:].astype(F32)
+    def read(block):
+        tail = block[:, width:].astype(F32)
         tail = (
             tail
             + pltpu.roll(tail, LANES - heads, 1)
@@ -317,12 +342,12 @@
             tiles.append(tile)
         return jnp.concatenate(tiles, 1)
 
-    stats = [read(ref) for ref in got_refs]
+    stats = [read(block) for block in got]
     best = functools.reduce(jnp.maximum, [top for top, _ in stats])
     factors = [jnp.exp(top - best) for top, _ in stats]
     total = sum(factor * total for factor, (_, total) in zip(factors, stats))
     mixed = sum(
-        ref[:, :width].astype(F32) * widen(factor) for ref, factor in zip(got_refs, factors)
+        block[:, :width].astype(F32) * widen(factor) for block, factor in zip(got, factors)
     )
     merged = (mixed / widen(total)).astype(BF16)
     rows = jnp.concatenate([merged, dec_ref[...]], 0)
@@ -339,7 +364,9 @@
 
 def call(kernel, outs, in_specs, name, flops, **extra):
     many = isinstance(outs, list)
-    shapes = [jax.ShapeDtypeStruct(shape, BF16) for shape in (outs if many else [outs])]
+    shapes = []
+    for out in outs if many else [outs]:
+        shapes.append(jax.ShapeDtypeStruct(out, BF16))
     limit = extra.pop("limit", 8 << 20)
     specs = [VMEM] * len(shapes)
     return pl.pallas_call(
@@ -354,9 +381,50 @@
     )
 
 
-def shift(values, axis, step):
-    size = lax.axis_size(axis)
-    return lax.ppermute(values, axis, [(i, (i + step) % size) for i in range(size)])
+def ring_pairs(shards, step):
+    return [(i, (i + step) % shards) for i in range(shards)]
+
+
+def mixed_pairs(shards, parts, taken):
+    return [
+        (i * parts + t, (i + taken[t % len(taken)]) % shards * parts + t)
+        for i in range(shards)
+        for t in range(parts)
+    ]
+
+
+def swap(values, axis, step):
+    return lax.ppermute(values, axis, ring_pairs(lax.axis_size(axis), step))
+
+
+def gather_plan(shards, parts):
+    steps = list(range(1, shards))
+    plan = []
+    while steps:
+        together = parts if parts == 2 and len(steps) >= 2 else 1
+        plan.append(steps[:together])
+        steps = steps[together:]
+    return plan
+
+
+def slot_steps(plan, parts):
+    slots = [[0] * parts]
+    for taken in plan:
+        for turned in range(len(taken)):
+            slots.append([taken[(t + turned) % len(taken)] for t in range(parts)])
+    return slots
+
+
+def pick(index, values):
+    chosen = jnp.int32(values[0])
+    for i, value in enumerate(values):
+        if value != values[0]:
+            chosen = jnp.where(index == i, value, chosen)
+    return chosen
+
+
+def block_at(ref, number, count):
+    return ref[pl.ds(pl.multiple_of(number * count, count), count), :]
 
 
 def in_hbm(array):
@@ -395,7 +463,7 @@
     w_vup,
     w_out,
 ):
-    shards = lax.axis_size("kv")
+    shards, parts = lax.axis_size("kv"), lax.axis_size("tp")
     count, model = piece_rows.shape
     cached, width = prompt_latent.shape
     context = cached * shards
@@ -413,7 +481,7 @@
     q_latent, q_decode = call(
         query_latent_kernel,
         [(count, w_qdown.shape[1]), (count, w_qdown.shape[1])],
-        [HBM, HBM, HBM, HBM],
+        [HBM] * 4,
         "query_latent",
         2 * 2 * count * model * w_qdown.shape[1] * 100,
         scratch_shapes=[
@@ -421,50 +489,40 @@
             pltpu.VMEM(decode_rows.shape, BF16),
             pltpu.VMEM((1, q_gain.shape[0]), F32),
             pltpu.VMEM(w_qdown.shape, BF16),
-            pltpu.SemaphoreType.DMA((7,)),
+            pltpu.SemaphoreType.DMA((4 + 3,)),
         ],
     )(*[in_hbm(array) for array in (piece_rows, decode_rows, w_qdown, q_gain[None, :])])
 
+    length = jnp.broadcast_to(dec_lengths.astype(F32)[:, None], (1, LANES))
     direct = shards <= MAX_PERMUTES
     if direct:
-        steps = sorted(range(1, shards), key=lambda s: -min(s, shards - s))
-        arrived = {s: shift(q_latent, "kv", s) for s in steps}
-        blocks = [q_latent] + [arrived[s] for s in range(1, shards)]
+        plan = gather_plan(shards, parts)
+        slots = slot_steps(plan, parts)
+        blocks = [q_latent]
+        for taken in plan:
+            blocks.append(lax.ppermute(q_latent, ("kv", "tp"), mixed_pairs(shards, parts, taken)))
+            if len(taken) > 1:
+                blocks.append(swap(blocks[-1], "tp", 1))
     else:
         blocks = [lax.all_gather(q_latent, "kv", axis=0, tiled=True)]
 
-    (
-        piece_latent,
-        dec_latent,
-        piece_rope,
-        dec_rope,
-        keys,
-        values,
-        new_keys,
-        new_values,
-        new_rope,
-        dec_latent_rows,
-        dec_rope_rows,
-    ) = call(
+    new_latent, dec_latent_rows, new_rope, dec_rope_rows, keys, values, new_keys, new_values = call(
         functools.partial(keys_kernel, context),
         [
             (count, width),
-            (1, width),
-            (count, rope),
-            (1, rope),
+            (count, width),
+            (count, LANES),
+            (count, LANES),
             (cached, heads * nope),
             (cached, heads * value_dim),
             (count, heads * nope),
             (count, heads * value_dim),
-            (count, LANES),
-            (count, width),
-            (count, LANES),
         ],
-        [SMEM] + [VMEM] * 11,
+        [VMEM] * 12,
         "keys",
         4 * cached * width * heads * nope,
     )(
-        dec_lengths,
+        length,
         piece_rows,
         decode_rows,
         w_kvdown,
@@ -492,23 +550,22 @@
     total_rows = count * shards
     flops = 4 * total_rows * cached * heads * nope
     if direct:
-        packed = call(
-            functools.partial(attend_kernel, True, nope),
-            (total_rows, packed_width),
+        sent = call(
+            functools.partial(attend_kernel, slots, nope),
+            [(count, packed_width)] * shards,
             [VMEM] * (len(shared) + shards),
             "attend",
             flops,
+            scratch_shapes=[pltpu.VMEM((total_rows, packed_width), BF16)],
         )(*shared, *blocks)
-        sent = [packed[s * count : (s + 1) * count] for s in range(shards)]
-        came = {s: shift(sent[s], "kv", shards - s) for s in steps}
-        got = [sent[0]] + [came[s] for s in range(1, shards)]
+        got = [sent[0]] + [swap(sent[shards - s], "kv", s) for s in range(1, shards)]
     else:
         step_rows = min(64, total_rows)
         whole = [
             pl.BlockSpec(array.shape, lambda i, rank=array.ndim: (0,) * rank) for array in shared
         ]
         packed = pl.pallas_call(
-            functools.partial(attend_kernel, False, nope),
+            functools.partial(attend_kernel, None, nope),
             grid=(total_rows // step_rows,),
             out_shape=jax.ShapeDtypeStruct((total_rows, packed_width), BF16),
             in_specs=whole + [pl.BlockSpec((step_rows, w_qdown.shape[1]), lambda i: (i, 0))],
@@ -519,14 +576,14 @@
         got = lax.all_to_all(packed, "kv", split_axis=0, concat_axis=0, tiled=True)
         got = [got[s * count : (s + 1) * count] for s in range(shards)]
 
-    dec_heads = call(
+    dec_heads, piece_latent, dec_latent, piece_rope, dec_rope = call(
         functools.partial(decode_kernel, nope),
-        (count, heads * value_dim),
-        [SMEM] + [VMEM] * 9,
+        [(count, heads * value_dim), (count, width), (1, width), (count, rope), (1, rope)],
+        [VMEM] * 12,
         "decode",
         4 * count * decode_latent.shape[1] * width * 4,
     )(
-        dec_lengths,
+        length,
         q_decode,
         w_query,
         w_key,
@@ -536,6 +593,8 @@
         dec_latent_rows,
         dec_rope_rows,
         freq,
+        new_latent,
+        new_rope,
     )
 
     term = call(
@@ -545,7 +604,7 @@
         "combine",
         2 * 2 * count * heads * value_dim * model,
     )(dec_heads, w_last, *got)
-    terms = [term] + [shift(term, "tp", s) for s in range(1, lax.axis_size("tp"))]
+    terms = [term] + [swap(term, "tp", s) for s in range(1, parts)]
     piece_out, decode_out = call(
         add_kernel, [(count, model), (1, model)], [VMEM] * len(terms), "add", 1000
     )(*terms)

time: 24 us -> 22.3 us (0.929)
  starting transfers between devices: 10.3 us -> 9.38 us
  waiting for transfers between devices: 4.32 us -> 3.5 us
    ppermute x7, starting transfers between devices: 10.3 us -> 9.38 us  [the longest x2 5.2 us: per_device(): lax.ppermute(q_latent, ('kv', 'tp'), mixed_pairs(shards, parts, taken))]
    ppermute x7, waiting for transfers between devices: 4.32 us -> 3.5 us  [the longest x5 2.39 us: swap(): return lax.ppermute(values, axis, ring_pairs(lax.axis_size(axis), step))]
  transfers between devices with their start and end apart: 7 -> 7, of which waited for: 5 -> 3; matrix products, arithmetic and copies ran while one was open for 0% -> 0% of each run, Pallas kernels for 12% -> 13%
where the time goes in v4:
time: 22.3 us; the launch traced here: 22.2 us
  starting transfers between devices  9.38 us (42%)
  Pallas kernels  7.64 us (34%)
  waiting for transfers between devices  3.5 us (16%)
  between operations  1.56 us (7%)
    ppermute x2, starting transfers between devices, per_device(): lax.ppermute(q_latent, ('kv', 'tp'), mixed_pairs(shards, parts, taken))  5.2 us
    ppermute x5, starting transfers between devices, swap(): return lax.ppermute(values, axis, ring_pairs(lax.axis_size(axis), step))  4.18 us
    ppermute x5, waiting for transfers between devices, swap(): return lax.ppermute(values, axis, ring_pairs(lax.axis_size(axis), step))  2.39 us
    pallas_call x1, Pallas kernels, per_device(): call(query_latent_kernel, [(count, w_qdown.shape[1]), (count, w_qdown.sha...  2.05 us
    pallas_call x1, Pallas kernels, per_device(): call(functools.partial(decode_kernel, nope), [(count, heads * value_dim),...  1.66 us
    pallas_call x1, Pallas kernels, per_device(): call(functools.partial(attend_kernel, slots, nope), [(count, packed_width...  1.44 us
    pallas_call x1, Pallas kernels, per_device(): call(functools.partial(keys_kernel, context), [(count, width), (count, wi...  1.16 us
    ppermute x2, waiting for transfers between devices, per_device(): lax.ppermute(q_latent, ('kv', 'tp'), mixed_pairs(shards, parts, taken))  1.1 us
  transfers between devices with their start and end apart: 7, of which 3 were waited for; matrix products, arithmetic and copies ran while one was open for 0% of the time, Pallas kernels for 13%

profile of v4, /device:TPU:0, one launch (start us, length us, event | category | flops | bytes accessed | tf_op | source)
XLA Modules:
  0.0 22.2 jit_solution(8453684888938772975)
XLA Ops:
  0.7 0.0 copy-start.7
  0.7 0.0 copy-start.8
  0.7 0.0 copy-start.15
  0.8 2.1 %query_latent.1 = (bf16[16,512]{1,0:T(8,128)(2,1)S(1)}, bf16[16,512]{1,0:T(8,128)(2,1)S(1)}) custom-call(bf16[16,2048]{1,0:T(8,128)(2,1)} %piece_ref.1, bf16[1,2048]{1,0:T(2,128)(2,1)} %dec_ref.1, bf16[2048,512]{1,0:T(8,128)(2,1)} %w_hbm.1, f32[1,512]{1,0:T(1,128)} %bitcast.29), custom_call_target="tpu_custom_call" | custom-call | flops 6710886400 | bytes 104857600 | tf_op jit(solution)/shard_map/query_latent/pallas_call | solution.py:481
  2.8 0.0 copy-start
  2.8 0.0 copy-start.12
  2.8 3.1 %collective-permute-start = (bf16[16,512]{1,0:T(8,128)(2,1)S(1)}, bf16[16,512]{1,0:T(8,128)(2,1)S(1)}, u32[]{:S(2)}, u32[]{:S(2)}) collective-permute-start(bf16[16,512]{1,0:T(8,128)(2,1)S(1)} %get-tuple-element.37.refs_9_), channel_id=1, source_target_pairs={{0,2},{1,5},{2,4},{3,7},{4,6},{5,1},{6,0},{7,3},{8,10},{9,13},{10,... | collective-permute-start | bytes 49160 | tf_op jit(solution)/shard_map/ppermute | solution.py:503
  5.9 2.1 %collective-permute-start.2 = (bf16[16,512]{1,0:T(8,128)(2,1)S(1)}, bf16[16,512]{1,0:T(8,128)(2,1)S(1)}, u32[]{:S(2)}, u32[]{:S(2)}) collective-permute-start(bf16[16,512]{1,0:T(8,128)(2,1)S(1)} %get-tuple-element.37.refs_9_), channel_id=1, source_target_pairs={{0,6},{1,7},{2,0},{3,1},{4,2},{5,3},{6,4},{7,5},{8,14},{9,15},{10,... | collective-permute-start | bytes 49160 | tf_op jit(solution)/shard_map/ppermute | solution.py:503
  8.7 1.1 %collective-permute-done.refs_10_ = bf16[16,512]{1,0:T(8,128)(2,1)S(1)} collective-permute-done((bf16[16,512]{1,0:T(8,128)(2,1)S(1)}, bf16[16,512]{1,0:T(8,128)(2,1)S(1)}, u32[]{:S(2)}, u32[]{:S(2)}) %collective-permute-start) | collective-permute-done | bytes 16416 | tf_op jit(solution)/shard_map/ppermute | solution.py:503
  9.9 0.0 copy-start.5
  9.9 0.0 copy-start.11
  9.9 1.2 %keys.1 = (bf16[16,512]{1,0:T(8,128)(2,1)S(1)}, bf16[16,512]{1,0:T(8,128)(2,1)S(1)}, bf16[16,128]{1,0:T(8,128)(2,1)S(1)}, bf16[16,128]{1,0:T(8,128)(2,1)S(1)}, b...) custom-call(f32[1,128]{1,0:T(1,128)S(1)} %broadcast_in_dim.15.length, ...), custom_call_target="tpu_custom_call" | custom-call | flops 268435456 | bytes 4194304 | tf_op jit(solution)/shard_map/keys/pallas_call | solution.py:509
  11.1 0.0 collective-permute-done.1.refs_11_
  11.1 1.4 %attend.1 = (bf16[16,640]{1,0:T(8,128)(2,1)S(1)}, bf16[16,640]{1,0:T(8,128)(2,1)S(1)}, bf16[16,640]{1,0:T(8,128)(2,1)S(1)}, bf16[16,640]{1,0:T(8,128)(2,1)S(1)}) custom-call(bf16[8,96,512]{2,1,0:T(8,128)(2,1)S(1)} %bitcast.17, bf16[256,512]{1,0:T(8,128)(2,1)S(1)} %get-tuple-element.33.refs_1_, bf16[256,512]{1,0:T(8,128)(2,1)S(1)} %get-tuple-element.34.refs_2_, ...), custom_call_target="tpu_custom_call" | custom-call | flops 33554432 | bytes 524288 | tf_op jit(solution)/shard_map/attend/pallas_call | solution.py:553
  12.6 0.2 collective-permute-start.3
  12.8 2.9 %collective-permute-start.4 = (bf16[16,640]{1,0:T(8,128)(2,1)S(1)}, bf16[16,640]{1,0:T(8,128)(2,1)S(1)}, u32[]{:S(2)}, u32[]{:S(2)}) collective-permute-start(bf16[16,640]{1,0:T(8,128)(2,1)S(1)} %get-tuple-element.40), channel_id=1, source_target_pairs={{0,4},{2,6},{4,0},{6,2},{1,5},{3,7},{5,1},{7,3},{8,12},{10,14},{12... | collective-permute-start | bytes 61448 | tf_op jit(solution)/shard_map/ppermute | solution.py:397
  15.7 1.1 %collective-permute-start.5 = (bf16[16,640]{1,0:T(8,128)(2,1)S(1)}, bf16[16,640]{1,0:T(8,128)(2,1)S(1)}, u32[]{:S(2)}, u32[]{:S(2)}) collective-permute-start(bf16[16,640]{1,0:T(8,128)(2,1)S(1)} %get-tuple-element.41), channel_id=1, source_target_pairs={{0,6},{2,0},{4,2},{6,4},{1,7},{3,1},{5,3},{7,5},{8,14},{10,8},{12,... | collective-permute-start | bytes 61448 | tf_op jit(solution)/shard_map/ppermute | solution.py:397
  16.7 1.7 %decode.1 = (bf16[16,512]{1,0:T(8,128)(2,1)S(1)}, bf16[16,512]{1,0:T(8,128)(2,1)}, bf16[1,512]{1,0:T(2,128)(2,1)}, bf16[16,32]{1,0:T(8,128)(2,1)}, bf16[1,32]{1,0:T(2,128)(2,1)}) custom-call(f32[1,128]{1,0:T(1,128)S(1)} %broadcast_in_dim.15.lengths_ref, bf16[16,512]{1,0:T(8,128)(2,1)S(1)} %get-tuple-element.27.q_ref, bf16[8,96,512]{2,1,0:T(8,128)(2,1)S(1)} %bitcast.18, ...), custom_call_target="tpu_custom_call" | custom-call | flops 67108864 | bytes 1048576 | tf_op jit(solution)/shard_map/decode/pallas_call | solution.py:579
  18.4 0.0 collective-permute-done.3.refs_1_
  18.4 1.0 %collective-permute-done.5.refs_3_ = bf16[16,640]{1,0:T(8,128)(2,1)S(1)} collective-permute-done((bf16[16,640]{1,0:T(8,128)(2,1)S(1)}, bf16[16,640]{1,0:T(8,128)(2,1)S(1)}, u32[]{:S(2)}, u32[]{:S(2)}) %collective-permute-start.5) | collective-permute-done | bytes 20512 | tf_op jit(solution)/shard_map/ppermute | solution.py:397
  19.4 0.7 %combine.1.refs_0_ = bf16[32,2048]{1,0:T(8,128)(2,1)S(1)} custom-call(bf16[16,512]{1,0:T(8,128)(2,1)S(1)} %get-tuple-element.32.dec_ref, bf16[512,2048]{1,0:T(8,128)(2,1)S(1)} %bitcast.19, bf16[16,640]{1,0:T(8,128)(2,1)S(1)} %get-tuple-element.38.refs_0_, bf16[16,640]{1,0:T(8,128)(2,1)S(1)} %collective-permute-done.3.refs_1_, ...), custom_call_target="tpu_custom_call" | custom-call | flops 67108864 | bytes 1048576 | tf_op jit(solution)/shard_map/combine/pallas_call | solution.py:600
  20.1 0.0 collective-permute-start.6
  20.2 1.3 %collective-permute-done.6.refs_1_ = bf16[32,2048]{1,0:T(8,128)(2,1)S(1)} collective-permute-done((bf16[32,2048]{1,0:T(8,128)(2,1)S(1)}, bf16[32,2048]{1,0:T(8,128)(2,1)S(1)}, u32[]{:S(2)}, u32[]{:S(2)}) %collective-permute-start.6) | collective-permute-done | bytes 131104 | tf_op jit(solution)/shard_map/ppermute | solution.py:397
  21.5 0.6 %add.1 = (bf16[16,2048]{1,0:T(8,128)(2,1)}, bf16[1,2048]{1,0:T(2,128)(2,1)}) custom-call(bf16[32,2048]{1,0:T(8,128)(2,1)S(1)} %combine.1.refs_0_, bf16[32,2048]{1,0:T(8,128)(2,1)S(1)} %collective-permute-done.6.refs_1_), custom_call_target="tpu_custom_call" | custom-call | flops 1000 | bytes 15 | tf_op jit(solution)/shard_map/add/pallas_call | solution.py:608
  (29 shorter events, 0.1 us)
Async XLA Ops:
  0.6 9.2 %copy-start.1 = (bf16[2048,512]{1,0:T(8,128)(2,1)S(1)}, bf16[2048,512]{1,0:T(8,128)(2,1)}, u32[]{:S(2)}) copy-start(bf16[2048,512]{1,0:T(8,128)(2,1)} %w_ref.1) | copy-start | bytes 6291460
  0.6 9.2 %copy-start.3 = (bf16[512,8,64]{0,2,1:T(8,128)(2,1)S(1)}, bf16[512,8,64]{0,2,1:T(8,128)(2,1)}, u32[]{:S(2)}) copy-start(bf16[512,8,64]{0,2,1:T(8,128)(2,1)} %param.32) | copy-start | bytes 1572868
  0.7 9.2 %copy-start.4 = (bf16[512,8,64]{0,2,1:T(8,128)(2,1)S(1)}, bf16[512,8,64]{0,2,1:T(8,128)(2,1)}, u32[]{:S(2)}) copy-start(bf16[512,8,64]{0,2,1:T(8,128)(2,1)} %param.33) | copy-start | bytes 1572868
  0.7 9.2 %copy-start.6 = (bf16[256,512]{1,0:T(8,128)(2,1)S(1)}, bf16[256,512]{1,0:T(8,128)(2,1)}, u32[]{:S(2)}) copy-start(bf16[256,512]{1,0:T(8,128)(2,1)} %prompt_ref.1) | copy-start | bytes 786436
  0.7 9.2 %copy-start.7 = (f32[64,128]{1,0:T(8,128)S(1)}, f32[64,128]{1,0:T(8,128)}, u32[]{:S(2)}) copy-start(f32[64,128]{1,0:T(8,128)} %constant.7.clone.sin_ref.refs_8_) | copy-start | bytes 98308
  0.7 9.2 %copy-start.8 = (f32[64,128]{1,0:T(8,128)S(1)}, f32[64,128]{1,0:T(8,128)}, u32[]{:S(2)}) copy-start(f32[64,128]{1,0:T(8,128)} %constant.6.clone.cos_ref.refs_7_) | copy-start | bytes 98308
  0.7 9.1 %copy-start.9 = (bf16[2048,32]{0,1:T(8,128)(2,1)S(1)}, bf16[2048,32]{0,1:T(8,128)(2,1)}, u32[]{:S(2)}) copy-start(bf16[2048,32]{0,1:T(8,128)(2,1)} %param.30) | copy-start | bytes 393220
  0.7 9.1 %copy-start.10 = (bf16[16,2048]{1,0:T(8,128)(2,1)S(1)}, bf16[16,2048]{1,0:T(8,128)(2,1)}, u32[]{:S(2)}) copy-start(bf16[16,2048]{1,0:T(8,128)(2,1)} %piece_ref.1) | copy-start | bytes 196612
  0.7 9.1 %copy-start.13 = (bf16[1,2048]{1,0:T(2,128)(2,1)S(1)}, bf16[1,2048]{1,0:T(2,128)(2,1)}, u32[]{:S(2)}) copy-start(bf16[1,2048]{1,0:T(2,128)(2,1)} %dec_ref.1) | copy-start | bytes 12292
  0.7 9.1 %copy-start.14 = (f32[512]{0:T(512)S(1)}, f32[512]{0:T(512)}, u32[]{:S(2)}) copy-start(f32[512]{0:T(512)} %param.31) | copy-start | bytes 6148
  0.7 9.1 %copy-start.15 = (f32[1,128]{1,0:T(1,128)S(1)}, f32[1,128]{1,0:T(1,128)}, u32[]{:S(2)}) copy-start(f32[1,128]{1,0:T(1,128)} %constant.8.clone.freq_ref) | copy-start | bytes 1540
  2.8 8.3 %copy-start = (bf16[512,8,96]{0,2,1:T(8,128)(2,1)S(1)}, bf16[512,8,96]{0,2,1:T(8,128)(2,1)}, u32[]{:S(2)}) copy-start(bf16[512,8,96]{0,2,1:T(8,128)(2,1)} %param.28) | copy-start | bytes 2359300
  2.8 8.3 %copy-start.12 = (bf16[256,32]{0,1:T(8,128)(2,1)S(1)}, bf16[256,32]{0,1:T(8,128)(2,1)}, u32[]{:S(2)}) copy-start(bf16[256,32]{0,1:T(8,128)(2,1)} %param.22) | copy-start | bytes 49156
  2.8 6.9 %collective-permute-start = (bf16[16,512]{1,0:T(8,128)(2,1)S(1)}, bf16[16,512]{1,0:T(8,128)(2,1)S(1)}, u32[]{:S(2)}, u32[]{:S(2)}) collective-permute-start(bf16[16,512]{1,0:T(8,128)(2,1)S(1)} %get-tuple-element.37.refs_9_), channel_id=1, source_target_pairs={{0,2},{1,5},{2,4},{3,7},{4,6},{5,1},{6,0},{7,3},{8,10},{9,13},{10,... | collective-permute-start | bytes 49160 | tf_op jit(solution)/shard_map/ppermute | solution.py:503
  5.9 5.1 %collective-permute-start.2 = (bf16[16,512]{1,0:T(8,128)(2,1)S(1)}, bf16[16,512]{1,0:T(8,128)(2,1)S(1)}, u32[]{:S(2)}, u32[]{:S(2)}) collective-permute-start(bf16[16,512]{1,0:T(8,128)(2,1)S(1)} %get-tuple-element.37.refs_9_), channel_id=1, source_target_pairs={{0,6},{1,7},{2,0},{3,1},{4,2},{5,3},{6,4},{7,5},{8,14},{9,15},{10,... | collective-permute-start | bytes 49160 | tf_op jit(solution)/shard_map/ppermute | solution.py:503
  9.8 1.3 %collective-permute-start.1 = (bf16[16,512]{1,0:T(8,128)(2,1)S(1)}, bf16[16,512]{1,0:T(8,128)(2,1)S(1)}, u32[]{:S(2)}, u32[]{:S(2)}) collective-permute-start(bf16[16,512]{1,0:T(8,128)(2,1)S(1)} %collective-permute-done.refs_10_), channel_id=1, source_target_pairs={{0,1},{1,0},{2,3},{3,2},{4,5},{5,4},{6,7},{7,6},{8,9},{9,8},{10,11... | collective-permute-start | bytes 49160 | tf_op jit(solution)/shard_map/ppermute | solution.py:397
  9.9 6.8 %copy-start.5 = (bf16[1,512,512]{2,1,0:T(8,128)(2,1)S(1)}, bf16[1,512,512]{2,1,0:T(8,128)(2,1)}, u32[]{:S(2)}) copy-start(bf16[1,512,512]{2,1,0:T(8,128)(2,1)} %param.23) | copy-start | bytes 1572868
  9.9 6.8 %copy-start.11 = (bf16[1,512,32]{1,2,0:T(8,128)(2,1)S(1)}, bf16[1,512,32]{1,2,0:T(8,128)(2,1)}, u32[]{:S(2)}) copy-start(bf16[1,512,32]{1,2,0:T(8,128)(2,1)} %param.24) | copy-start | bytes 98308
  11.1 8.4 %copy-start.2 = (bf16[8,64,2048]{2,1,0:T(8,128)(2,1)S(1)}, bf16[8,64,2048]{2,1,0:T(8,128)(2,1)}, u32[]{:S(2)}) copy-start(bf16[8,64,2048]{2,1,0:T(8,128)(2,1)} %param.34) | copy-start | bytes 6291460
  12.6 5.8 %collective-permute-start.3 = (bf16[16,640]{1,0:T(8,128)(2,1)S(1)}, bf16[16,640]{1,0:T(8,128)(2,1)S(1)}, u32[]{:S(2)}, u32[]{:S(2)}) collective-permute-start(bf16[16,640]{1,0:T(8,128)(2,1)S(1)} %get-tuple-element.39), channel_id=1, source_target_pairs={{0,2},{2,4},{4,6},{6,0},{1,3},{3,5},{5,7},{7,1},{8,10},{10,12},{12... | collective-permute-start | bytes 61448 | tf_op jit(solution)/shard_map/ppermute | solution.py:397
  12.8 5.6 %collective-permute-start.4 = (bf16[16,640]{1,0:T(8,128)(2,1)S(1)}, bf16[16,640]{1,0:T(8,128)(2,1)S(1)}, u32[]{:S(2)}, u32[]{:S(2)}) collective-permute-start(bf16[16,640]{1,0:T(8,128)(2,1)S(1)} %get-tuple-element.40), channel_id=1, source_target_pairs={{0,4},{2,6},{4,0},{6,2},{1,5},{3,7},{5,1},{7,3},{8,12},{10,14},{12... | collective-permute-start | bytes 61448 | tf_op jit(solution)/shard_map/ppermute | solution.py:397
  15.7 3.8 %collective-permute-start.5 = (bf16[16,640]{1,0:T(8,128)(2,1)S(1)}, bf16[16,640]{1,0:T(8,128)(2,1)S(1)}, u32[]{:S(2)}, u32[]{:S(2)}) collective-permute-start(bf16[16,640]{1,0:T(8,128)(2,1)S(1)} %get-tuple-element.41), channel_id=1, source_target_pairs={{0,6},{2,0},{4,2},{6,4},{1,7},{3,1},{5,3},{7,5},{8,14},{10,8},{12,... | collective-permute-start | bytes 61448 | tf_op jit(solution)/shard_map/ppermute | solution.py:397
  20.1 1.4 %collective-permute-start.6 = (bf16[32,2048]{1,0:T(8,128)(2,1)S(1)}, bf16[32,2048]{1,0:T(8,128)(2,1)S(1)}, u32[]{:S(2)}, u32[]{:S(2)}) collective-permute-start(bf16[32,2048]{1,0:T(8,128)(2,1)S(1)} %combine.1.refs_0_), channel_id=1, source_target_pairs={{0,1},{1,0},{2,3},{3,2},{4,5},{5,4},{6,7},{7,6},{8,9},{9,8},{10,11... | collective-permute-start | bytes 393224 | tf_op jit(solution)/shard_map/ppermute | solution.py:397

commit v5 on v4

--- a/solution.py
+++ b/solution.py
@@ -11,6 +11,7 @@
 LANES = 128
 GROUP = 256
 MAX_PERMUTES = 8
+LOG2_E = 1.4426950408889634
 ROPE_BASE = 10000.0
 VMEM = pl.BlockSpec(memory_space=pltpu.VMEM)
 HBM = pl.BlockSpec(memory_space=pltpu.HBM)
@@ -52,6 +53,11 @@
 def diagonal(values, count, width):
     owner = lane_index(values.shape) // width
     return jnp.concatenate([jnp.where(owner == j, values, 0.0) for j in range(count)], 0)
+
+
+def padded(values):
+    empty = jnp.zeros((LANES - values.shape[0], values.shape[1]), values.dtype)
+    return jnp.concatenate([values, empty], 0)
 
 
 def spread_rows(row, rows):
@@ -140,14 +146,14 @@
     dec_rope = turn(raw[count:], jnp.cos(angle), jnp.sin(angle) * sign, rope).astype(BF16)
     latent_ref[...] = latent[:count]
     dec_latent_ref[...] = latent[count:]
-    rope_ref[...] = new_rope
+    rope_ref[...] = padded(new_rope)
     dec_rope_ref[...] = dec_rope
     w_kup, w_vup = w_kup_ref[...], w_vup_ref[...]
     prompt = prompt_ref[...]
-    key_ref[...] = dot_nt(prompt, w_kup).astype(BF16)
+    key_ref[...] = dot_nt(w_kup, prompt).astype(BF16)
     value_ref[...] = dot_nt(prompt, w_vup).astype(BF16)
-    new_key_ref[...] = dot_nt(latent[:count], w_kup).astype(BF16)
-    new_value_ref[...] = dot_nt(latent[:count], w_vup).astype(BF16)
+    new_key_ref[...] = padded(dot_nt(latent[:count], w_kup).astype(BF16))
+    new_value_ref[...] = padded(dot_nt(latent[:count], w_vup).astype(BF16))
 
 
 def split_query_weights(w_ref, nope):
@@ -157,7 +163,7 @@
     return w_nope, w_rope
 
 
-def attend_kernel(slots, nope, *refs):
+def attend_kernel(slots, nope, count, *refs):
     (
         w_ref,
         key_ref,
@@ -178,7 +184,6 @@
         latent_refs, out_ref = refs[9:-1], refs[-1]
     heads = w_ref.shape[0]
     rope = w_ref.shape[1] - nope
-    count = new_key_ref.shape[0]
     latents = jnp.concatenate([ref[...] for ref in latent_refs], 0)
     if slots:
         owners = [lax.rem(index - pick(part, steps) + shards, shards) for steps in slots]
@@ -190,45 +195,72 @@
     cosine = jnp.concatenate([cos_ref[part, :] for part in tables], 0)
     sine = jnp.concatenate([sin_ref[part, :] for part in tables], 0)
     scale = (nope + rope) ** (-0.5)
-    w_nope, w_rope = split_query_weights(w_ref, nope)
-    q_nope = dot_nt(latents, w_nope).astype(BF16).astype(F32)
-    q_rope = dot_nt(latents, w_rope)
-    per = GROUP // nope
-    rope_keys = jnp.concatenate([rope_ref[...]] * (LANES // rope), 0)
+    per, pair, middle = GROUP // nope, LANES // nope, nope + rope // 2
+    old_rope = jnp.concatenate([rope_ref[...]] * (LANES // rope), 0)
     new_rope = new_rope_ref[...]
-    row = row_index((count, count))
-    column = lane_index((count, count))
+    row = row_index((count, LANES))
+    column = lane_index((count, LANES))
     allowed = jnp.concatenate(
-        [index * count + column <= owner * count + row for owner in owners] * per, 0
+        [
+            (column < count) & (index * count + column <= owner * count + row)
+            for owner in owners
+        ]
+        * pair,
+        0,
     )
     lane = lane_index((queries, LANES))
+    rate = scale * LOG2_E
     stats = jnp.zeros((queries, LANES), F32)
+    tiles = key_ref.shape[1] // LANES
+    ropes, nopes = [], []
+    for g in range(heads // per):
+        mine = range(g * per, (g + 1) * per)
+        rotary = [w_ref[h, nope:, :] for h in mine]
+        for h in mine:
+            rotary += [w_ref[h, middle:, :], w_ref[h, nope:middle, :]]
+        q_rope = dot_nt(latents, jnp.concatenate(rotary, 0))
+        ropes.append(q_rope[:, :LANES] * cosine + q_rope[:, LANES:] * sine)
+        q_nope = dot_nt(latents, jnp.concatenate([w_ref[h, :nope, :] for h in mine], 0))
+        nopes.append(q_nope.astype(BF16).astype(F32))
+    scores = []
+    for first in range(0, heads, pair):
+        g, p = first // per, first % per // pair
+        narrow = slice(first * nope, first * nope + LANES)
+        rows = slice(p * pair * queries, (p + 1) * pair * queries)
+        query = jnp.concatenate(
+            [
+                diagonal(nopes[g][:, p * LANES : (p + 1) * LANES], pair, nope),
+                diagonal(ropes[g], per, rope)[rows],
+            ],
+            1,
+        ).astype(BF16)
+        old = dot(query, jnp.concatenate([key_ref[narrow, :], old_rope], 0))
+        new = dot_nt(query, jnp.concatenate([new_key_ref[:, narrow], new_rope], 1))
+        new = jnp.where(allowed, new, -1e30)
+        scores.append([old[:, t * LANES : (t + 1) * LANES] for t in range(tiles)] + [new])
+    weights = []
+    for number, pieces in enumerate(scores):
+        top = jnp.max(functools.reduce(jnp.maximum, pieces), axis=-1, keepdims=True)
+        pieces = [jnp.exp2((piece - top) * rate) for piece in pieces]
+        total = jnp.sum(sum(pieces), axis=-1, keepdims=True)
+        weights.append([piece.astype(BF16) for piece in pieces])
+        for j in range(pair):
+            own = slice(j * queries, (j + 1) * queries)
+            stats = jnp.where(
+                lane % heads == number * pair + j,
+                jnp.where(lane < 3 * heads, top[own] * scale, total[own]),
+                stats,
+            )
     for g in range(heads // per):
         wide = slice(g * GROUP, (g + 1) * GROUP)
-        turned = turn(q_rope[:, g * LANES : (g + 1) * LANES], cosine, sine, rope)
-        spread = diagonal(q_nope[:, wide], per, nope).astype(BF16)
-        spread_rope = diagonal(turned, per, rope).astype(BF16)
-        old = (dot_nt(spread, key_ref[:, wide]) + dot(spread_rope, rope_keys)) * scale
-        new = (dot_nt(spread, new_key_ref[:, wide]) + dot_nt(spread_rope, new_rope)) * scale
-        new = jnp.where(allowed, new, -1e30)
-        top = jnp.maximum(
-            jnp.max(old, axis=-1, keepdims=True), jnp.max(new, axis=-1, keepdims=True)
-        )
-        old = jnp.exp(old - top)
-        new = jnp.exp(new - top)
-        total = jnp.sum(old, axis=-1, keepdims=True) + jnp.sum(new, axis=-1, keepdims=True)
-        mixed = dot(old.astype(BF16), value_ref[:, wide]) + dot(
-            new.astype(BF16), new_value_ref[:, wide]
-        )
+        mine = weights[g * per // pair : (g + 1) * per // pair]
+        old = jnp.concatenate([jnp.concatenate(pieces[:-1], 1) for pieces in mine], 0)
+        new = jnp.concatenate([pieces[-1] for pieces in mine], 0)
+        mixed = dot(old, value_ref[:, wide]) + dot(new, new_value_ref[:, wide])
         owner_lane = lane_index((queries, GROUP)) // nope
         kept = jnp.zeros((queries, GROUP), F32)
         for j in range(per):
-            own = slice(j * queries, (j + 1) * queries)
-            kept = jnp.where(owner_lane == j, mixed[own], kept)
-            h = g * per + j
-            stats = jnp.where(
-                lane % heads == h, jnp.where(lane < 3 * heads, top[own], total[own]), stats
-            )
+            kept = jnp.where(owner_lane == j, mixed[j * queries : (j + 1) * queries], kept)
         out_ref[:, wide] = kept.astype(BF16)
     high = stats.astype(BF16).astype(F32)
     rest = stats - high
@@ -267,7 +299,7 @@
     rope = w_ref.shape[1] - nope
     latent_out_ref[...] = piece_latent_ref[...]
     dec_latent_out_ref[...] = new_latent_ref[:1, :]
-    rope_out_ref[...] = piece_rope_ref[:, :rope]
+    rope_out_ref[...] = piece_rope_ref[: rope_out_ref.shape[0], :rope]
     dec_rope_out_ref[...] = new_rope_ref[:1, :rope]
     length = lengths_ref[...]
     scale = (nope + rope) ** (-0.5)
@@ -315,43 +347,27 @@
     out_ref[...] = jnp.broadcast_to(total, out_ref.shape).astype(BF16)
 
 
-def combine_kernel(heads, dec_ref, w_ref, *refs):
+def combine_kernel(heads, dec_ref, w_ref, chosen_ref, *refs):
     count = dec_ref.shape[0]
     got, out_ref = [ref[...] for ref in refs[:-1]], refs[-1]
     width = w_ref.shape[0]
-    value_dim = width // heads
-
-    def read(block):
-        tail = block[:, width:].astype(F32)
-        tail = (
-            tail
-            + pltpu.roll(tail, LANES - heads, 1)
-            + pltpu.roll(tail, LANES - 2 * heads, 1)
-        )
-        return tail, pltpu.roll(tail, LANES - 3 * heads, 1)
-
-    def widen(values):
-        per = LANES // value_dim
-        lane = lane_index((count, LANES)) // value_dim
-        tiles = []
-        for t in range(width // LANES):
-            tile = jnp.zeros((count, LANES), F32)
-            for j in range(per):
-                h = t * per + j
-                tile = jnp.where(lane == j, values[:, h : h + 1], tile)
-            tiles.append(tile)
-        return jnp.concatenate(tiles, 1)
-
-    stats = [read(block) for block in got]
-    best = functools.reduce(jnp.maximum, [top for top, _ in stats])
-    factors = [jnp.exp(top - best) for top, _ in stats]
-    total = sum(factor * total for factor, (_, total) in zip(factors, stats))
-    mixed = sum(
-        block[:, :width].astype(F32) * widen(factor) for block, factor in zip(got, factors)
-    )
-    merged = (mixed / widen(total)).astype(BF16)
-    rows = jnp.concatenate([merged, dec_ref[...]], 0)
+    tails = dot(jnp.concatenate([block[:, width:] for block in got], 0), chosen_ref[...])
+    tops = [tails[b * count : (b + 1) * count, :width] for b in range(len(got))]
+    totals = [tails[b * count : (b + 1) * count, width:] for b in range(len(got))]
+    best = functools.reduce(jnp.maximum, tops)
+    factors = [jnp.exp(top - best) for top in tops]
+    total = sum(factor * total for factor, total in zip(factors, totals))
+    mixed = sum(block[:, :width].astype(F32) * factor for block, factor in zip(got, factors))
+    rows = jnp.concatenate([(mixed / total).astype(BF16), dec_ref[...]], 0)
     out_ref[...] = dot(rows, w_ref[...]).astype(BF16)
+
+
+def chosen_lanes(heads, value_dim):
+    lane = np.arange(LANES)[:, None]
+    head = np.arange(heads * value_dim)[None, :] // value_dim
+    same = lane % heads == head
+    tops, totals = same & (lane < 3 * heads), same & (lane >= 3 * heads) & (lane < 6 * heads)
+    return np.concatenate([tops, totals], 1).astype(np.float32)
 
 
 def add_kernel(*refs):
@@ -511,12 +527,12 @@
         [
             (count, width),
             (count, width),
+            (LANES, LANES),
             (count, LANES),
-            (count, LANES),
-            (cached, heads * nope),
+            (heads * nope, cached),
             (cached, heads * value_dim),
-            (count, heads * nope),
-            (count, heads * value_dim),
+            (LANES, heads * nope),
+            (LANES, heads * value_dim),
         ],
         [VMEM] * 12,
         "keys",
@@ -551,7 +567,7 @@
     flops = 4 * total_rows * cached * heads * nope
     if direct:
         sent = call(
-            functools.partial(attend_kernel, slots, nope),
+            functools.partial(attend_kernel, slots, nope, count),
             [(count, packed_width)] * shards,
             [VMEM] * (len(shared) + shards),
             "attend",
@@ -565,7 +581,7 @@
             pl.BlockSpec(array.shape, lambda i, rank=array.ndim: (0,) * rank) for array in shared
         ]
         packed = pl.pallas_call(
-            functools.partial(attend_kernel, None, nope),
+            functools.partial(attend_kernel, None, nope, count),
             grid=(total_rows // step_rows,),
             out_shape=jax.ShapeDtypeStruct((total_rows, packed_width), BF16),
             in_specs=whole + [pl.BlockSpec((step_rows, w_qdown.shape[1]), lambda i: (i, 0))],
@@ -600,10 +616,10 @@
     term = call(
         functools.partial(combine_kernel, heads),
         (2 * count, model),
-        [VMEM] * (2 + len(got)),
+        [VMEM] * (3 + len(got)),
         "combine",
         2 * 2 * count * heads * value_dim * model,
-    )(dec_heads, w_last, *got)
+    )(dec_heads, w_last, jnp.asarray(chosen_lanes(heads, value_dim), BF16), *got)
     terms = [term] + [swap(term, "tp", s) for s in range(1, parts)]
     piece_out, decode_out = call(
         add_kernel, [(count, model), (1, model)], [VMEM] * len(terms), "add", 1000

time: 22.3 us -> 21.8 us (0.978)
  Pallas kernels: 7.64 us -> 7.12 us
    pallas_call x1, Pallas kernels: 1.44 us -> 0.96 us  [per_device(): call(functools.partial(attend_kernel, slots, nope, count), [(count, packe...]
where the time goes in v5:
time: 21.8 us; the launch traced here: 21.6 us
  starting transfers between devices  9.36 us (43%)
  Pallas kernels  7.12 us (33%)
  waiting for transfers between devices  3.51 us (16%)
  between operations  1.56 us (7%)
    ppermute x2, starting transfers between devices, per_device(): lax.ppermute(q_latent, ('kv', 'tp'), mixed_pairs(shards, parts, taken))  5.2 us
    ppermute x5, starting transfers between devices, swap(): return lax.ppermute(values, axis, ring_pairs(lax.axis_size(axis), step))  4.16 us
    ppermute x5, waiting for transfers between devices, swap(): return lax.ppermute(values, axis, ring_pairs(lax.axis_size(axis), step))  2.4 us
    pallas_call x1, Pallas kernels, per_device(): call(query_latent_kernel, [(count, w_qdown.shape[1]), (count, w_qdown.sha...  2.05 us
    pallas_call x1, Pallas kernels, per_device(): call(functools.partial(decode_kernel, nope), [(count, heads * value_dim),...  1.66 us
    pallas_call x1, Pallas kernels, per_device(): call(functools.partial(keys_kernel, context), [(count, width), (count, wi...  1.17 us
    ppermute x2, waiting for transfers between devices, per_device(): lax.ppermute(q_latent, ('kv', 'tp'), mixed_pairs(shards, parts, taken))  1.1 us
    pallas_call x1, Pallas kernels, per_device(): call(functools.partial(attend_kernel, slots, nope, count), [(count, packe...  0.96 us
  transfers between devices with their start and end apart: 7, of which 3 were waited for; matrix products, arithmetic and copies ran while one was open for 0% of the time, Pallas kernels for 13%

profile of v5, /device:TPU:0, one launch (start us, length us, event | category | flops | bytes accessed | tf_op | source)
XLA Modules:
  0.0 21.6 jit_solution(15851606108149916154)
XLA Ops:
  0.7 0.0 copy-start.8
  0.7 0.0 copy-start.9
  0.7 0.0 copy-start.16
  0.8 2.1 %query_latent.1 = (bf16[16,512]{1,0:T(8,128)(2,1)S(1)}, bf16[16,512]{1,0:T(8,128)(2,1)S(1)}) custom-call(bf16[16,2048]{1,0:T(8,128)(2,1)} %piece_ref.1, bf16[1,2048]{1,0:T(2,128)(2,1)} %dec_ref.1, bf16[2048,512]{1,0:T(8,128)(2,1)} %w_hbm.1, f32[1,512]{1,0:T(1,128)} %bitcast.29), custom_call_target="tpu_custom_call" | custom-call | flops 6710886400 | bytes 104857600 | tf_op jit(solution)/shard_map/query_latent/pallas_call | solution.py:497
  2.8 0.0 copy-start.13
  2.8 3.1 %collective-permute-start = (bf16[16,512]{1,0:T(8,128)(2,1)S(1)}, bf16[16,512]{1,0:T(8,128)(2,1)S(1)}, u32[]{:S(2)}, u32[]{:S(2)}) collective-permute-start(bf16[16,512]{1,0:T(8,128)(2,1)S(1)} %get-tuple-element.37.refs_9_), channel_id=1, source_target_pairs={{0,2},{1,5},{2,4},{3,7},{4,6},{5,1},{6,0},{7,3},{8,10},{9,13},{10,... | collective-permute-start | bytes 49160 | tf_op jit(solution)/shard_map/ppermute | solution.py:519
  5.9 2.1 %collective-permute-start.2 = (bf16[16,512]{1,0:T(8,128)(2,1)S(1)}, bf16[16,512]{1,0:T(8,128)(2,1)S(1)}, u32[]{:S(2)}, u32[]{:S(2)}) collective-permute-start(bf16[16,512]{1,0:T(8,128)(2,1)S(1)} %get-tuple-element.37.refs_9_), channel_id=1, source_target_pairs={{0,6},{1,7},{2,0},{3,1},{4,2},{5,3},{6,4},{7,5},{8,14},{9,15},{10,... | collective-permute-start | bytes 49160 | tf_op jit(solution)/shard_map/ppermute | solution.py:519
  8.7 1.1 %collective-permute-done.refs_10_ = bf16[16,512]{1,0:T(8,128)(2,1)S(1)} collective-permute-done((bf16[16,512]{1,0:T(8,128)(2,1)S(1)}, bf16[16,512]{1,0:T(8,128)(2,1)S(1)}, u32[]{:S(2)}, u32[]{:S(2)}) %collective-permute-start) | collective-permute-done | bytes 16416 | tf_op jit(solution)/shard_map/ppermute | solution.py:519
  9.9 0.0 copy-start.5
  9.9 0.0 copy-start.12
  9.9 1.2 %keys.1 = (bf16[16,512]{1,0:T(8,128)(2,1)S(1)}, bf16[16,512]{1,0:T(8,128)(2,1)S(1)}, bf16[128,128]{1,0:T(8,128)(2,1)S(1)}, bf16[16,128]{1,0:T(8,128)(2,1)S(1)}, ...) custom-call(f32[1,128]{1,0:T(1,128)S(1)} %broadcast_in_dim.15.length, ...), custom_call_target="tpu_custom_call" | custom-call | flops 268435456 | bytes 4194304 | tf_op jit(solution)/shard_map/keys/pallas_call | solution.py:525
  11.1 0.0 collective-permute-done.1.refs_11_
  11.2 0.0 copy-start.6
  11.2 1.0 %attend.1 = (bf16[16,640]{1,0:T(8,128)(2,1)S(1)}, bf16[16,640]{1,0:T(8,128)(2,1)S(1)}, bf16[16,640]{1,0:T(8,128)(2,1)S(1)}, bf16[16,640]{1,0:T(8,128)(2,1)S(1)}) custom-call(bf16[8,96,512]{2,1,0:T(8,128)(2,1)S(1)} %bitcast.17, bf16[512,256]{1,0:T(8,128)(2,1)S(1)} %get-tuple-element.33.refs_1_, bf16[256,512]{1,0:T(8,128)(2,1)S(1)} %get-tuple-element.34.refs_2_, ...), custom_call_target="tpu_custom_call" | custom-call | flops 33554432 | bytes 524288 | tf_op jit(solution)/shard_map/attend/pallas_call | solution.py:569
  12.1 0.2 collective-permute-start.3
  12.3 2.9 %collective-permute-start.4 = (bf16[16,640]{1,0:T(8,128)(2,1)S(1)}, bf16[16,640]{1,0:T(8,128)(2,1)S(1)}, u32[]{:S(2)}, u32[]{:S(2)}) collective-permute-start(bf16[16,640]{1,0:T(8,128)(2,1)S(1)} %get-tuple-element.40), channel_id=1, source_target_pairs={{0,4},{2,6},{4,0},{6,2},{1,5},{3,7},{5,1},{7,3},{8,12},{10,14},{12... | collective-permute-start | bytes 61448 | tf_op jit(solution)/shard_map/ppermute | solution.py:413
  15.2 1.1 %collective-permute-start.5 = (bf16[16,640]{1,0:T(8,128)(2,1)S(1)}, bf16[16,640]{1,0:T(8,128)(2,1)S(1)}, u32[]{:S(2)}, u32[]{:S(2)}) collective-permute-start(bf16[16,640]{1,0:T(8,128)(2,1)S(1)} %get-tuple-element.41), channel_id=1, source_target_pairs={{0,6},{2,0},{4,2},{6,4},{1,7},{3,1},{5,3},{7,5},{8,14},{10,8},{12,... | collective-permute-start | bytes 61448 | tf_op jit(solution)/shard_map/ppermute | solution.py:413
  16.3 1.7 %decode.1 = (bf16[16,512]{1,0:T(8,128)(2,1)S(1)}, bf16[16,512]{1,0:T(8,128)(2,1)}, bf16[1,512]{1,0:T(2,128)(2,1)}, bf16[16,32]{1,0:T(8,128)(2,1)}, bf16[1,32]{1,0:T(2,128)(2,1)}) custom-call(f32[1,128]{1,0:T(1,128)S(1)} %broadcast_in_dim.15.lengths_ref, bf16[16,512]{1,0:T(8,128)(2,1)S(1)} %get-tuple-element.27.q_ref, bf16[8,96,512]{2,1,0:T(8,128)(2,1)S(1)} %bitcast.18, ...), custom_call_target="tpu_custom_call" | custom-call | flops 67108864 | bytes 1048576 | tf_op jit(solution)/shard_map/decode/pallas_call | solution.py:595
  17.9 0.0 collective-permute-done.3.refs_1_
  18.0 1.0 %collective-permute-done.5.refs_3_ = bf16[16,640]{1,0:T(8,128)(2,1)S(1)} collective-permute-done((bf16[16,640]{1,0:T(8,128)(2,1)S(1)}, bf16[16,640]{1,0:T(8,128)(2,1)S(1)}, u32[]{:S(2)}, u32[]{:S(2)}) %collective-permute-start.5) | collective-permute-done | bytes 20512 | tf_op jit(solution)/shard_map/ppermute | solution.py:413
  19.0 0.6 %combine.1.refs_0_ = bf16[32,2048]{1,0:T(8,128)(2,1)S(1)} custom-call(bf16[16,512]{1,0:T(8,128)(2,1)S(1)} %get-tuple-element.32.dec_ref, bf16[512,2048]{1,0:T(8,128)(2,1)S(1)} %bitcast.19, bf16[128,1024]{1,0:T(8,128)(2,1)S(1)} %copy-done.6, bf16[16,640]{1,0:T(8,128)(2,1)S(1)} %get-tuple-element.38.refs_0_, ...), custom_call_target="tpu_custom_call" | custom-call | flops 67108864 | bytes 1048576 | tf_op jit(solution)/shard_map/combine/pallas_call | solution.py:616
  19.6 0.0 collective-permute-start.6
  19.7 1.3 %collective-permute-done.6.refs_1_ = bf16[32,2048]{1,0:T(8,128)(2,1)S(1)} collective-permute-done((bf16[32,2048]{1,0:T(8,128)(2,1)S(1)}, bf16[32,2048]{1,0:T(8,128)(2,1)S(1)}, u32[]{:S(2)}, u32[]{:S(2)}) %collective-permute-start.6) | collective-permute-done | bytes 131104 | tf_op jit(solution)/shard_map/ppermute | solution.py:413
  21.0 0.6 %add.1 = (bf16[16,2048]{1,0:T(8,128)(2,1)}, bf16[1,2048]{1,0:T(2,128)(2,1)}) custom-call(bf16[32,2048]{1,0:T(8,128)(2,1)S(1)} %combine.1.refs_0_, bf16[32,2048]{1,0:T(8,128)(2,1)S(1)} %collective-permute-done.6.refs_1_), custom_call_target="tpu_custom_call" | custom-call | flops 1000 | bytes 15 | tf_op jit(solution)/shard_map/add/pallas_call | solution.py:624
  (31 shorter events, 0.1 us)
Async XLA Ops:
  0.6 9.2 %copy-start.2 = (bf16[2048,512]{1,0:T(8,128)(2,1)S(1)}, bf16[2048,512]{1,0:T(8,128)(2,1)}, u32[]{:S(2)}) copy-start(bf16[2048,512]{1,0:T(8,128)(2,1)} %w_ref.1) | copy-start | bytes 6291460
  0.6 9.2 %copy-start.3 = (bf16[512,8,64]{0,2,1:T(8,128)(2,1)S(1)}, bf16[512,8,64]{0,2,1:T(8,128)(2,1)}, u32[]{:S(2)}) copy-start(bf16[512,8,64]{0,2,1:T(8,128)(2,1)} %param.33) | copy-start | bytes 1572868
  0.7 9.2 %copy-start.4 = (bf16[512,8,64]{0,2,1:T(8,128)(2,1)S(1)}, bf16[512,8,64]{0,2,1:T(8,128)(2,1)}, u32[]{:S(2)}) copy-start(bf16[512,8,64]{0,2,1:T(8,128)(2,1)} %param.34) | copy-start | bytes 1572868
  0.7 9.2 %copy-start.7 = (bf16[256,512]{1,0:T(8,128)(2,1)S(1)}, bf16[256,512]{1,0:T(8,128)(2,1)}, u32[]{:S(2)}) copy-start(bf16[256,512]{1,0:T(8,128)(2,1)} %prompt_ref.1) | copy-start | bytes 786436
  0.7 9.2 %copy-start.8 = (f32[64,128]{1,0:T(8,128)S(1)}, f32[64,128]{1,0:T(8,128)}, u32[]{:S(2)}) copy-start(f32[64,128]{1,0:T(8,128)} %constant.9.clone.sin_ref.refs_8_) | copy-start | bytes 98308
  0.7 9.2 %copy-start.9 = (f32[64,128]{1,0:T(8,128)S(1)}, f32[64,128]{1,0:T(8,128)}, u32[]{:S(2)}) copy-start(f32[64,128]{1,0:T(8,128)} %constant.8.clone.cos_ref.refs_7_) | copy-start | bytes 98308
  0.7 9.1 %copy-start.10 = (bf16[2048,32]{0,1:T(8,128)(2,1)S(1)}, bf16[2048,32]{0,1:T(8,128)(2,1)}, u32[]{:S(2)}) copy-start(bf16[2048,32]{0,1:T(8,128)(2,1)} %param.31) | copy-start | bytes 393220
  0.7 9.1 %copy-start.11 = (bf16[16,2048]{1,0:T(8,128)(2,1)S(1)}, bf16[16,2048]{1,0:T(8,128)(2,1)}, u32[]{:S(2)}) copy-start(bf16[16,2048]{1,0:T(8,128)(2,1)} %piece_ref.1) | copy-start | bytes 196612
  0.7 9.1 %copy-start.14 = (bf16[1,2048]{1,0:T(2,128)(2,1)S(1)}, bf16[1,2048]{1,0:T(2,128)(2,1)}, u32[]{:S(2)}) copy-start(bf16[1,2048]{1,0:T(2,128)(2,1)} %dec_ref.1) | copy-start | bytes 12292
  0.7 9.1 %copy-start.15 = (f32[512]{0:T(512)S(1)}, f32[512]{0:T(512)}, u32[]{:S(2)}) copy-start(f32[512]{0:T(512)} %param.32) | copy-start | bytes 6148
  0.7 9.1 %copy-start.16 = (f32[1,128]{1,0:T(1,128)S(1)}, f32[1,128]{1,0:T(1,128)}, u32[]{:S(2)}) copy-start(f32[1,128]{1,0:T(1,128)} %constant.10.clone.freq_ref) | copy-start | bytes 1540
  2.8 8.3 %copy-start = (bf16[512,8,96]{0,2,1:T(8,128)(2,1)S(1)}, bf16[512,8,96]{0,2,1:T(8,128)(2,1)}, u32[]{:S(2)}) copy-start(bf16[512,8,96]{0,2,1:T(8,128)(2,1)} %param.29) | copy-start | bytes 2359300
  2.8 8.3 %copy-start.13 = (bf16[256,32]{0,1:T(8,128)(2,1)S(1)}, bf16[256,32]{0,1:T(8,128)(2,1)}, u32[]{:S(2)}) copy-start(bf16[256,32]{0,1:T(8,128)(2,1)} %param.23) | copy-start | bytes 49156
  2.8 6.9 %collective-permute-start = (bf16[16,512]{1,0:T(8,128)(2,1)S(1)}, bf16[16,512]{1,0:T(8,128)(2,1)S(1)}, u32[]{:S(2)}, u32[]{:S(2)}) collective-permute-start(bf16[16,512]{1,0:T(8,128)(2,1)S(1)} %get-tuple-element.37.refs_9_), channel_id=1, source_target_pairs={{0,2},{1,5},{2,4},{3,7},{4,6},{5,1},{6,0},{7,3},{8,10},{9,13},{10,... | collective-permute-start | bytes 49160 | tf_op jit(solution)/shard_map/ppermute | solution.py:519
  5.9 5.2 %collective-permute-start.2 = (bf16[16,512]{1,0:T(8,128)(2,1)S(1)}, bf16[16,512]{1,0:T(8,128)(2,1)S(1)}, u32[]{:S(2)}, u32[]{:S(2)}) collective-permute-start(bf16[16,512]{1,0:T(8,128)(2,1)S(1)} %get-tuple-element.37.refs_9_), channel_id=1, source_target_pairs={{0,6},{1,7},{2,0},{3,1},{4,2},{5,3},{6,4},{7,5},{8,14},{9,15},{10,... | collective-permute-start | bytes 49160 | tf_op jit(solution)/shard_map/ppermute | solution.py:519
  9.8 1.3 %collective-permute-start.1 = (bf16[16,512]{1,0:T(8,128)(2,1)S(1)}, bf16[16,512]{1,0:T(8,128)(2,1)S(1)}, u32[]{:S(2)}, u32[]{:S(2)}) collective-permute-start(bf16[16,512]{1,0:T(8,128)(2,1)S(1)} %collective-permute-done.refs_10_), channel_id=1, source_target_pairs={{0,1},{1,0},{2,3},{3,2},{4,5},{5,4},{6,7},{7,6},{8,9},{9,8},{10,11... | collective-permute-start | bytes 49160 | tf_op jit(solution)/shard_map/ppermute | solution.py:413
  9.9 6.4 %copy-start.5 = (bf16[1,512,512]{2,1,0:T(8,128)(2,1)S(1)}, bf16[1,512,512]{2,1,0:T(8,128)(2,1)}, u32[]{:S(2)}) copy-start(bf16[1,512,512]{2,1,0:T(8,128)(2,1)} %param.24) | copy-start | bytes 1572868
  9.9 6.4 %copy-start.12 = (bf16[1,512,32]{1,2,0:T(8,128)(2,1)S(1)}, bf16[1,512,32]{1,2,0:T(8,128)(2,1)}, u32[]{:S(2)}) copy-start(bf16[1,512,32]{1,2,0:T(8,128)(2,1)} %param.25) | copy-start | bytes 98308
  11.1 7.8 %copy-start.1 = (bf16[8,64,2048]{2,1,0:T(8,128)(2,1)S(1)}, bf16[8,64,2048]{2,1,0:T(8,128)(2,1)}, u32[]{:S(2)}) copy-start(bf16[8,64,2048]{2,1,0:T(8,128)(2,1)} %param.35) | copy-start | bytes 6291460
  11.2 7.8 %copy-start.6 = (bf16[128,1024]{1,0:T(8,128)(2,1)S(1)}, bf16[128,1024]{1,0:T(8,128)(2,1)}, u32[]{:S(2)}) copy-start(bf16[128,1024]{1,0:T(8,128)(2,1)} %constant.11.clone.chosen_ref) | copy-start | bytes 786436
  12.1 5.8 %collective-permute-start.3 = (bf16[16,640]{1,0:T(8,128)(2,1)S(1)}, bf16[16,640]{1,0:T(8,128)(2,1)S(1)}, u32[]{:S(2)}, u32[]{:S(2)}) collective-permute-start(bf16[16,640]{1,0:T(8,128)(2,1)S(1)} %get-tuple-element.39), channel_id=1, source_target_pairs={{0,2},{2,4},{4,6},{6,0},{1,3},{3,5},{5,7},{7,1},{8,10},{10,12},{12... | collective-permute-start | bytes 61448 | tf_op jit(solution)/shard_map/ppermute | solution.py:413
  12.3 5.6 %collective-permute-start.4 = (bf16[16,640]{1,0:T(8,128)(2,1)S(1)}, bf16[16,640]{1,0:T(8,128)(2,1)S(1)}, u32[]{:S(2)}, u32[]{:S(2)}) collective-permute-start(bf16[16,640]{1,0:T(8,128)(2,1)S(1)} %get-tuple-element.40), channel_id=1, source_target_pairs={{0,4},{2,6},{4,0},{6,2},{1,5},{3,7},{5,1},{7,3},{8,12},{10,14},{12... | collective-permute-start | bytes 61448 | tf_op jit(solution)/shard_map/ppermute | solution.py:413
  15.2 3.8 %collective-permute-start.5 = (bf16[16,640]{1,0:T(8,128)(2,1)S(1)}, bf16[16,640]{1,0:T(8,128)(2,1)S(1)}, u32[]{:S(2)}, u32[]{:S(2)}) collective-permute-start(bf16[16,640]{1,0:T(8,128)(2,1)S(1)} %get-tuple-element.41), channel_id=1, source_target_pairs={{0,6},{2,0},{4,2},{6,4},{1,7},{3,1},{5,3},{7,5},{8,14},{10,8},{12,... | collective-permute-start | bytes 61448 | tf_op jit(solution)/shard_map/ppermute | solution.py:413
  19.6 1.4 %collective-permute-start.6 = (bf16[32,2048]{1,0:T(8,128)(2,1)S(1)}, bf16[32,2048]{1,0:T(8,128)(2,1)S(1)}, u32[]{:S(2)}, u32[]{:S(2)}) collective-permute-start(bf16[32,2048]{1,0:T(8,128)(2,1)S(1)} %combine.1.refs_0_), channel_id=1, source_target_pairs={{0,1},{1,0},{2,3},{3,2},{4,5},{5,4},{6,7},{7,6},{8,9},{9,8},{10,11... | collective-permute-start | bytes 393224 | tf_op jit(solution)/shard_map/ppermute | solution.py:413

commit v6 on v5

--- a/solution.py
+++ b/solution.py
@@ -13,6 +13,7 @@
 MAX_PERMUTES = 8
 LOG2_E = 1.4426950408889634
 ROPE_BASE = 10000.0
+CUTS = (0, 2, 4, 6, 7, 8)
 VMEM = pl.BlockSpec(memory_space=pltpu.VMEM)
 HBM = pl.BlockSpec(memory_space=pltpu.HBM)
 NT = (((1,), (1,)), ((), ()))
@@ -77,39 +78,46 @@
     w_ref,
     sems,
 ):
-    chunks = sems.shape[0] - 3
-    depth = w_ref.shape[0] // chunks
-    small = []
-    for c, (source, target) in enumerate(
-        [
-            (piece_hbm, piece_ref),
-            (dec_hbm, dec_ref),
-            (gain_hbm, gain_ref),
-        ]
-    ):
-        small.append(pltpu.make_async_copy(source, target, sems.at[chunks + c]))
-        small[-1].start()
+    depth = w_ref.shape[0] // CUTS[-1]
+    parts = [slice(a * depth, b * depth) for a, b in zip(CUTS[:-1], CUTS[1:])]
+    pairs = [(piece_hbm, piece_ref), (dec_hbm, dec_ref), (gain_hbm, gain_ref)]
+    small = len(pairs)
+    pairs += [(w_hbm.at[part], w_ref.at[part]) for part in parts]
     copies = []
-    for c in range(chunks):
-        part = pl.ds(c * depth, depth)
-        copies.append(pltpu.make_async_copy(w_hbm.at[part], w_ref.at[part], sems.at[c]))
+    for c, (source, target) in enumerate(pairs):
+        copies.append(pltpu.make_async_copy(source, target, sems.at[c]))
         copies[-1].start()
-    for copy in small:
+    for copy in copies[:small]:
         copy.wait()
     piece = piece_ref[...]
     rows = jnp.concatenate([piece, spread_rows(dec_ref[...], piece.shape[0])], 0)
     total = jnp.zeros((rows.shape[0], w_ref.shape[1]), F32)
-    for c in range(chunks):
-        copies[c].wait()
-        part = slice(c * depth, (c + 1) * depth)
+    for copy, part in zip(copies[small:], parts):
+        copy.wait()
         total = total + dot(rows[:, part], w_ref[part, :])
     latent = rms_scale(total, gain_ref[...]).astype(BF16)
     out_ref[...] = latent[: piece.shape[0]]
     dec_out_ref[...] = latent[piece.shape[0] :]
 
 
+def turn_weights(nope, w_ref, nope_out_ref, rope_out_ref):
+    heads = w_ref.shape[0]
+    middle = (nope + w_ref.shape[1]) // 2
+    per = GROUP // nope
+    w_nope = [w_ref[h, :nope, :] for h in range(heads)]
+    rotary = []
+    for g in range(heads // per):
+        mine = range(g * per, (g + 1) * per)
+        rotary += [w_ref[h, nope:, :] for h in mine]
+        for h in mine:
+            rotary += [w_ref[h, middle:, :], w_ref[h, nope:middle, :]]
+    nope_out_ref[...] = jnp.concatenate(w_nope, 0).T
+    rope_out_ref[...] = jnp.concatenate(rotary, 0).T
+
+
 def keys_kernel(
     context,
+    nope,
     lengths_ref,
     piece_ref,
     dec_ref,
@@ -122,6 +130,7 @@
     prompt_ref,
     w_kup_ref,
     w_vup_ref,
+    w_query_ref,
     latent_ref,
     dec_latent_ref,
     rope_ref,
@@ -130,7 +139,10 @@
     value_ref,
     new_key_ref,
     new_value_ref,
+    w_nope_ref,
+    w_turned_ref,
 ):
+    turn_weights(nope, w_query_ref, w_nope_ref, w_turned_ref)
     count = piece_ref.shape[0]
     rope = w_rope_ref.shape[0]
     piece = piece_ref[...]
@@ -146,13 +158,13 @@
     dec_rope = turn(raw[count:], jnp.cos(angle), jnp.sin(angle) * sign, rope).astype(BF16)
     latent_ref[...] = latent[:count]
     dec_latent_ref[...] = latent[count:]
-    rope_ref[...] = padded(new_rope)
+    rope_ref[...] = new_rope
     dec_rope_ref[...] = dec_rope
     w_kup, w_vup = w_kup_ref[...], w_vup_ref[...]
     prompt = prompt_ref[...]
     key_ref[...] = dot_nt(w_kup, prompt).astype(BF16)
     value_ref[...] = dot_nt(prompt, w_vup).astype(BF16)
-    new_key_ref[...] = padded(dot_nt(latent[:count], w_kup).astype(BF16))
+    new_key_ref[...] = dot_nt(latent[:count], w_kup).astype(BF16)
     new_value_ref[...] = padded(dot_nt(latent[:count], w_vup).astype(BF16))
 
 
@@ -165,7 +177,8 @@
 
 def attend_kernel(slots, nope, count, *refs):
     (
-        w_ref,
+        w_nope_ref,
+        w_rope_ref,
         key_ref,
         value_ref,
         new_key_ref,
@@ -174,16 +187,16 @@
         rope_ref,
         cos_ref,
         sin_ref,
-    ) = refs[:9]
+    ) = refs[:10]
     index = lax.axis_index("kv")
     part = lax.axis_index("tp")
     if slots:
         shards = len(slots)
-        latent_refs, out_refs, out_ref = refs[9 : 9 + shards], refs[9 + shards : -1], refs[-1]
+        latent_refs, out_refs, out_ref = refs[10 : 10 + shards], refs[10 + shards : -1], refs[-1]
     else:
-        latent_refs, out_ref = refs[9:-1], refs[-1]
-    heads = w_ref.shape[0]
-    rope = w_ref.shape[1] - nope
+        latent_refs, out_ref = refs[10:-1], refs[-1]
+    heads = w_nope_ref.shape[1] // nope
+    rope = rope_ref.shape[0]
     latents = jnp.concatenate([ref[...] for ref in latent_refs], 0)
     if slots:
         owners = [lax.rem(index - pick(part, steps) + shards, shards) for steps in slots]
@@ -195,7 +208,7 @@
     cosine = jnp.concatenate([cos_ref[part, :] for part in tables], 0)
     sine = jnp.concatenate([sin_ref[part, :] for part in tables], 0)
     scale = (nope + rope) ** (-0.5)
-    per, pair, middle = GROUP // nope, LANES // nope, nope + rope // 2
+    per, pair = GROUP // nope, LANES // nope
     old_rope = jnp.concatenate([rope_ref[...]] * (LANES // rope), 0)
     new_rope = new_rope_ref[...]
     row = row_index((count, LANES))
@@ -214,14 +227,10 @@
     tiles = key_ref.shape[1] // LANES
     ropes, nopes = [], []
     for g in range(heads // per):
-        mine = range(g * per, (g + 1) * per)
-        rotary = [w_ref[h, nope:, :] for h in mine]
-        for h in mine:
-            rotary += [w_ref[h, middle:, :], w_ref[h, nope:middle, :]]
-        q_rope = dot_nt(latents, jnp.concatenate(rotary, 0))
+        wide = slice(g * GROUP, (g + 1) * GROUP)
+        q_rope = dot(latents, w_rope_ref[:, wide])
         ropes.append(q_rope[:, :LANES] * cosine + q_rope[:, LANES:] * sine)
-        q_nope = dot_nt(latents, jnp.concatenate([w_ref[h, :nope, :] for h in mine], 0))
-        nopes.append(q_nope.astype(BF16).astype(F32))
+        nopes.append(dot(latents, w_nope_ref[:, wide]).astype(BF16).astype(F32))
     scores = []
     for first in range(0, heads, pair):
         g, p = first // per, first % per // pair
@@ -236,7 +245,8 @@
         ).astype(BF16)
         old = dot(query, jnp.concatenate([key_ref[narrow, :], old_rope], 0))
         new = dot_nt(query, jnp.concatenate([new_key_ref[:, narrow], new_rope], 1))
-        new = jnp.where(allowed, new, -1e30)
+        empty = jnp.zeros((new.shape[0], LANES - count), F32)
+        new = jnp.where(allowed, jnp.concatenate([new, empty], 1), -1e30)
         scores.append([old[:, t * LANES : (t + 1) * LANES] for t in range(tiles)] + [new])
     weights = []
     for number, pieces in enumerate(scores):
@@ -359,7 +369,7 @@
     total = sum(factor * total for factor, total in zip(factors, totals))
     mixed = sum(block[:, :width].astype(F32) * factor for block, factor in zip(got, factors))
     rows = jnp.concatenate([(mixed / total).astype(BF16), dec_ref[...]], 0)
-    out_ref[...] = dot(rows, w_ref[...]).astype(BF16)
+    out_ref[...] = dot(rows, w_ref[...])[: out_ref.shape[0]].astype(BF16)
 
 
 def chosen_lanes(heads, value_dim):
@@ -505,7 +515,7 @@
             pltpu.VMEM(decode_rows.shape, BF16),
             pltpu.VMEM((1, q_gain.shape[0]), F32),
             pltpu.VMEM(w_qdown.shape, BF16),
-            pltpu.SemaphoreType.DMA((4 + 3,)),
+            pltpu.SemaphoreType.DMA((len(CUTS) - 1 + 3,)),
         ],
     )(*[in_hbm(array) for array in (piece_rows, decode_rows, w_qdown, q_gain[None, :])])
 
@@ -522,19 +532,32 @@
     else:
         blocks = [lax.all_gather(q_latent, "kv", axis=0, tiled=True)]
 
-    new_latent, dec_latent_rows, new_rope, dec_rope_rows, keys, values, new_keys, new_values = call(
-        functools.partial(keys_kernel, context),
+    (
+        new_latent,
+        dec_latent_rows,
+        new_rope,
+        dec_rope_rows,
+        keys,
+        values,
+        new_keys,
+        new_values,
+        w_nope,
+        w_rope,
+    ) = call(
+        functools.partial(keys_kernel, context, nope),
         [
             (count, width),
             (count, width),
-            (LANES, LANES),
+            (count, LANES),
             (count, LANES),
             (heads * nope, cached),
             (cached, heads * value_dim),
-            (LANES, heads * nope),
+            (count, heads * nope),
             (LANES, heads * value_dim),
+            (w_qup.shape[0], heads * nope),
+            (w_qup.shape[0], heads * rope * 2),
         ],
-        [VMEM] * 12,
+        [VMEM] * 13,
         "keys",
         4 * cached * width * heads * nope,
     )(
@@ -550,10 +573,12 @@
         prompt_latent,
         w_key,
         w_value,
+        w_query,
     )
 
     shared = (
-        w_query,
+        w_nope,
+        w_rope,
         keys,
         values,
         new_keys,
@@ -615,7 +640,7 @@
 
     term = call(
         functools.partial(combine_kernel, heads),
-        (2 * count, model),
+        (count + 8, model),
         [VMEM] * (3 + len(got)),
         "combine",
         2 * 2 * count * heads * value_dim * model,

time: 21.8 us -> 21.5 us (0.986)
  no operation moved by 1% of the time
where the time goes in v6:
time: 21.5 us; the launch traced here: 21.4 us
  starting transfers between devices  9.31 us (43%)
  Pallas kernels  6.96 us (32%)
  waiting for transfers between devices  3.46 us (16%)
  between operations  1.56 us (7%)
    ppermute x2, starting transfers between devices, per_device(): lax.ppermute(q_latent, ('kv', 'tp'), mixed_pairs(shards, parts, taken))  5.2 us
    ppermute x5, starting transfers between devices, swap(): return lax.ppermute(values, axis, ring_pairs(lax.axis_size(axis), step))  4.11 us
    ppermute x5, waiting for transfers between devices, swap(): return lax.ppermute(values, axis, ring_pairs(lax.axis_size(axis), step))  2.36 us
    pallas_call x1, Pallas kernels, per_device(): call(query_latent_kernel, [(count, w_qdown.shape[1]), (count, w_qdown.sha...  2.03 us
    pallas_call x1, Pallas kernels, per_device(): call(functools.partial(decode_kernel, nope), [(count, heads * value_dim),...  1.66 us
    pallas_call x1, Pallas kernels, per_device(): call(functools.partial(keys_kernel, context, nope), [(count, width), (cou...  1.17 us
    ppermute x2, waiting for transfers between devices, per_device(): lax.ppermute(q_latent, ('kv', 'tp'), mixed_pairs(shards, parts, taken))  1.1 us
    pallas_call x1, Pallas kernels, per_device(): call(functools.partial(attend_kernel, slots, nope, count), [(count, packe...  0.82 us
  transfers between devices with their start and end apart: 7, of which 3 were waited for; matrix products, arithmetic and copies ran while one was open for 0% of the time, Pallas kernels for 13%

profile of v6, /device:TPU:0, one launch (start us, length us, event | category | flops | bytes accessed | tf_op | source)
XLA Modules:
  0.0 21.4 jit_solution(17341536870452324006)
XLA Ops:
  0.7 0.0 copy-start.8
  0.7 0.0 copy-start.9
  0.8 0.0 copy-start.16
  0.8 2.0 %query_latent.1 = (bf16[16,512]{1,0:T(8,128)(2,1)S(1)}, bf16[16,512]{1,0:T(8,128)(2,1)S(1)}) custom-call(bf16[16,2048]{1,0:T(8,128)(2,1)} %piece_ref.1, bf16[1,2048]{1,0:T(2,128)(2,1)} %dec_ref.1, bf16[2048,512]{1,0:T(8,128)(2,1)} %w_hbm.1, f32[1,512]{1,0:T(1,128)} %bitcast.29), custom_call_target="tpu_custom_call" | custom-call | flops 6710886400 | bytes 104857600 | tf_op jit(solution)/shard_map/query_latent/pallas_call | solution.py:507
  2.8 3.1 %collective-permute-start = (bf16[16,512]{1,0:T(8,128)(2,1)S(1)}, bf16[16,512]{1,0:T(8,128)(2,1)S(1)}, u32[]{:S(2)}, u32[]{:S(2)}) collective-permute-start(bf16[16,512]{1,0:T(8,128)(2,1)S(1)} %get-tuple-element.41.refs_10_), channel_id=1, source_target_pairs={{0,2},{1,5},{2,4},{3,7},{4,6},{5,1},{6,0},{7,3},{8,10},{9,13},{10,... | collective-permute-start | bytes 49160 | tf_op jit(solution)/shard_map/ppermute | solution.py:529
  5.9 2.1 %collective-permute-start.2 = (bf16[16,512]{1,0:T(8,128)(2,1)S(1)}, bf16[16,512]{1,0:T(8,128)(2,1)S(1)}, u32[]{:S(2)}, u32[]{:S(2)}) collective-permute-start(bf16[16,512]{1,0:T(8,128)(2,1)S(1)} %get-tuple-element.41.refs_10_), channel_id=1, source_target_pairs={{0,6},{1,7},{2,0},{3,1},{4,2},{5,3},{6,4},{7,5},{8,14},{9,15},{10,... | collective-permute-start | bytes 49160 | tf_op jit(solution)/shard_map/ppermute | solution.py:529
  8.7 1.1 %collective-permute-done.refs_11_ = bf16[16,512]{1,0:T(8,128)(2,1)S(1)} collective-permute-done((bf16[16,512]{1,0:T(8,128)(2,1)S(1)}, bf16[16,512]{1,0:T(8,128)(2,1)S(1)}, u32[]{:S(2)}, u32[]{:S(2)}) %collective-permute-start) | collective-permute-done | bytes 16416 | tf_op jit(solution)/shard_map/ppermute | solution.py:529
  9.9 0.0 copy-start.13
  9.9 0.0 copy-start.5
  9.9 1.2 %keys.1 = (bf16[16,512]{1,0:T(8,128)(2,1)S(1)}, bf16[16,512]{1,0:T(8,128)(2,1)S(1)}, bf16[16,128]{1,0:T(8,128)(2,1)S(1)}, bf16[16,128]{1,0:T(8,128)(2,1)S(1)}, b...) custom-call(f32[1,128]{1,0:T(1,128)S(1)} %broadcast_in_dim.15.length, ...), custom_call_target="tpu_custom_call" | custom-call | flops 268435456 | bytes 4194304 | tf_op jit(solution)/shard_map/keys/pallas_call | solution.py:546
  11.1 0.0 collective-permute-done.1.refs_12_
  11.1 0.0 copy-start.1
  11.1 0.0 copy-start.7
  11.1 0.8 %attend.1 = (bf16[16,640]{1,0:T(8,128)(2,1)S(1)}, bf16[16,640]{1,0:T(8,128)(2,1)S(1)}, bf16[16,640]{1,0:T(8,128)(2,1)S(1)}, bf16[16,640]{1,0:T(8,128)(2,1)S(1)}) custom-call(bf16[512,512]{1,0:T(8,128)(2,1)S(1)} %get-tuple-element.35.refs_0_, bf16[512,512]{1,0:T(8,128)(2,1)S(1)} %get-tuple-element.36.refs_1_, bf16[512,256]{1,0:T(8,128)(2,1)S(1)} %get-tuple-element.37.refs_2_, ...), custom_call_target="tpu_custom_call" | custom-call | flops 33554432 | bytes 524288 | tf_op jit(solution)/shard_map/attend/pallas_call | solution.py:594
  12.0 0.2 collective-permute-start.3
  12.1 2.9 %collective-permute-start.4 = (bf16[16,640]{1,0:T(8,128)(2,1)S(1)}, bf16[16,640]{1,0:T(8,128)(2,1)S(1)}, u32[]{:S(2)}, u32[]{:S(2)}) collective-permute-start(bf16[16,640]{1,0:T(8,128)(2,1)S(1)} %get-tuple-element.44), channel_id=1, source_target_pairs={{0,4},{2,6},{4,0},{6,2},{1,5},{3,7},{5,1},{7,3},{8,12},{10,14},{12... | collective-permute-start | bytes 61448 | tf_op jit(solution)/shard_map/ppermute | solution.py:423
  15.0 1.1 %collective-permute-start.5 = (bf16[16,640]{1,0:T(8,128)(2,1)S(1)}, bf16[16,640]{1,0:T(8,128)(2,1)S(1)}, u32[]{:S(2)}, u32[]{:S(2)}) collective-permute-start(bf16[16,640]{1,0:T(8,128)(2,1)S(1)} %get-tuple-element.45), channel_id=1, source_target_pairs={{0,6},{2,0},{4,2},{6,4},{1,7},{3,1},{5,3},{7,5},{8,14},{10,8},{12,... | collective-permute-start | bytes 61448 | tf_op jit(solution)/shard_map/ppermute | solution.py:423
  16.1 1.7 %decode.1 = (bf16[16,512]{1,0:T(8,128)(2,1)S(1)}, bf16[16,512]{1,0:T(8,128)(2,1)}, bf16[1,512]{1,0:T(2,128)(2,1)}, bf16[16,32]{1,0:T(8,128)(2,1)}, bf16[1,32]{1,0:T(2,128)(2,1)}) custom-call(f32[1,128]{1,0:T(1,128)S(1)} %broadcast_in_dim.15.lengths_ref, bf16[16,512]{1,0:T(8,128)(2,1)S(1)} %get-tuple-element.29.q_ref, bf16[8,96,512]{2,1,0:T(8,128)(2,1)S(1)} %bitcast.18, ...), custom_call_target="tpu_custom_call" | custom-call | flops 67108864 | bytes 1048576 | tf_op jit(solution)/shard_map/decode/pallas_call | solution.py:620
  17.7 0.0 collective-permute-done.3.refs_1_
  17.8 1.0 %collective-permute-done.5.refs_3_ = bf16[16,640]{1,0:T(8,128)(2,1)S(1)} collective-permute-done((bf16[16,640]{1,0:T(8,128)(2,1)S(1)}, bf16[16,640]{1,0:T(8,128)(2,1)S(1)}, u32[]{:S(2)}, u32[]{:S(2)}) %collective-permute-start.5) | collective-permute-done | bytes 20512 | tf_op jit(solution)/shard_map/ppermute | solution.py:423
  18.8 0.6 %combine.1.refs_0_ = bf16[24,2048]{1,0:T(8,128)(2,1)S(1)} custom-call(bf16[16,512]{1,0:T(8,128)(2,1)S(1)} %get-tuple-element.34.dec_ref, bf16[512,2048]{1,0:T(8,128)(2,1)S(1)} %bitcast.19, bf16[128,1024]{1,0:T(8,128)(2,1)S(1)} %copy-done.7, bf16[16,640]{1,0:T(8,128)(2,1)S(1)} %get-tuple-element.42.refs_0_, ...), custom_call_target="tpu_custom_call" | custom-call | flops 67108864 | bytes 1048576 | tf_op jit(solution)/shard_map/combine/pallas_call | solution.py:641
  19.4 0.0 collective-permute-start.6
  19.4 1.3 %collective-permute-done.6.refs_1_ = bf16[24,2048]{1,0:T(8,128)(2,1)S(1)} collective-permute-done((bf16[24,2048]{1,0:T(8,128)(2,1)S(1)}, bf16[24,2048]{1,0:T(8,128)(2,1)S(1)}, u32[]{:S(2)}, u32[]{:S(2)}) %collective-permute-start.6) | collective-permute-done | bytes 98336 | tf_op jit(solution)/shard_map/ppermute | solution.py:423
  20.7 0.6 %add.1 = (bf16[16,2048]{1,0:T(8,128)(2,1)}, bf16[1,2048]{1,0:T(2,128)(2,1)}) custom-call(bf16[24,2048]{1,0:T(8,128)(2,1)S(1)} %combine.1.refs_0_, bf16[24,2048]{1,0:T(8,128)(2,1)S(1)} %collective-permute-done.6.refs_1_), custom_call_target="tpu_custom_call" | custom-call | flops 1000 | bytes 15 | tf_op jit(solution)/shard_map/add/pallas_call | solution.py:649
  (31 shorter events, 0.1 us)
Async XLA Ops:
  0.6 9.1 %copy-start = (bf16[512,8,96]{0,2,1:T(8,128)(2,1)S(1)}, bf16[512,8,96]{0,2,1:T(8,128)(2,1)}, u32[]{:S(2)}) copy-start(bf16[512,8,96]{0,2,1:T(8,128)(2,1)} %param.29) | copy-start | bytes 2359300
  0.6 9.1 %copy-start.2 = (bf16[2048,512]{1,0:T(8,128)(2,1)S(1)}, bf16[2048,512]{1,0:T(8,128)(2,1)}, u32[]{:S(2)}) copy-start(bf16[2048,512]{1,0:T(8,128)(2,1)} %w_ref.1) | copy-start | bytes 6291460
  0.7 9.1 %copy-start.3 = (bf16[512,8,64]{0,2,1:T(8,128)(2,1)S(1)}, bf16[512,8,64]{0,2,1:T(8,128)(2,1)}, u32[]{:S(2)}) copy-start(bf16[512,8,64]{0,2,1:T(8,128)(2,1)} %param.33) | copy-start | bytes 1572868
  0.7 9.1 %copy-start.4 = (bf16[512,8,64]{0,2,1:T(8,128)(2,1)S(1)}, bf16[512,8,64]{0,2,1:T(8,128)(2,1)}, u32[]{:S(2)}) copy-start(bf16[512,8,64]{0,2,1:T(8,128)(2,1)} %param.34) | copy-start | bytes 1572868
  0.7 9.1 %copy-start.6 = (bf16[256,512]{1,0:T(8,128)(2,1)S(1)}, bf16[256,512]{1,0:T(8,128)(2,1)}, u32[]{:S(2)}) copy-start(bf16[256,512]{1,0:T(8,128)(2,1)} %prompt_ref.1) | copy-start | bytes 786436
  0.7 9.1 %copy-start.8 = (f32[64,128]{1,0:T(8,128)S(1)}, f32[64,128]{1,0:T(8,128)}, u32[]{:S(2)}) copy-start(f32[64,128]{1,0:T(8,128)} %constant.9.clone.sin_ref.refs_9_) | copy-start | bytes 98308
  0.7 9.1 %copy-start.9 = (f32[64,128]{1,0:T(8,128)S(1)}, f32[64,128]{1,0:T(8,128)}, u32[]{:S(2)}) copy-start(f32[64,128]{1,0:T(8,128)} %constant.8.clone.cos_ref.refs_8_) | copy-start | bytes 98308
  0.7 9.1 %copy-start.10 = (bf16[2048,32]{0,1:T(8,128)(2,1)S(1)}, bf16[2048,32]{0,1:T(8,128)(2,1)}, u32[]{:S(2)}) copy-start(bf16[2048,32]{0,1:T(8,128)(2,1)} %param.31) | copy-start | bytes 393220
  0.7 9.1 %copy-start.11 = (bf16[16,2048]{1,0:T(8,128)(2,1)S(1)}, bf16[16,2048]{1,0:T(8,128)(2,1)}, u32[]{:S(2)}) copy-start(bf16[16,2048]{1,0:T(8,128)(2,1)} %piece_ref.1) | copy-start | bytes 196612
  0.7 9.1 %copy-start.14 = (bf16[1,2048]{1,0:T(2,128)(2,1)S(1)}, bf16[1,2048]{1,0:T(2,128)(2,1)}, u32[]{:S(2)}) copy-start(bf16[1,2048]{1,0:T(2,128)(2,1)} %dec_ref.1) | copy-start | bytes 12292
  0.7 9.1 %copy-start.15 = (f32[512]{0:T(512)S(1)}, f32[512]{0:T(512)}, u32[]{:S(2)}) copy-start(f32[512]{0:T(512)} %param.32) | copy-start | bytes 6148
  0.8 9.1 %copy-start.16 = (f32[1,128]{1,0:T(1,128)S(1)}, f32[1,128]{1,0:T(1,128)}, u32[]{:S(2)}) copy-start(f32[1,128]{1,0:T(1,128)} %constant.10.clone.freq_ref) | copy-start | bytes 1540
  2.8 6.9 %collective-permute-start = (bf16[16,512]{1,0:T(8,128)(2,1)S(1)}, bf16[16,512]{1,0:T(8,128)(2,1)S(1)}, u32[]{:S(2)}, u32[]{:S(2)}) collective-permute-start(bf16[16,512]{1,0:T(8,128)(2,1)S(1)} %get-tuple-element.41.refs_10_), channel_id=1, source_target_pairs={{0,2},{1,5},{2,4},{3,7},{4,6},{5,1},{6,0},{7,3},{8,10},{9,13},{10,... | collective-permute-start | bytes 49160 | tf_op jit(solution)/shard_map/ppermute | solution.py:529
  5.9 5.2 %collective-permute-start.2 = (bf16[16,512]{1,0:T(8,128)(2,1)S(1)}, bf16[16,512]{1,0:T(8,128)(2,1)S(1)}, u32[]{:S(2)}, u32[]{:S(2)}) collective-permute-start(bf16[16,512]{1,0:T(8,128)(2,1)S(1)} %get-tuple-element.41.refs_10_), channel_id=1, source_target_pairs={{0,6},{1,7},{2,0},{3,1},{4,2},{5,3},{6,4},{7,5},{8,14},{9,15},{10,... | collective-permute-start | bytes 49160 | tf_op jit(solution)/shard_map/ppermute | solution.py:529
  9.8 1.4 %collective-permute-start.1 = (bf16[16,512]{1,0:T(8,128)(2,1)S(1)}, bf16[16,512]{1,0:T(8,128)(2,1)S(1)}, u32[]{:S(2)}, u32[]{:S(2)}) collective-permute-start(bf16[16,512]{1,0:T(8,128)(2,1)S(1)} %collective-permute-done.refs_11_), channel_id=1, source_target_pairs={{0,1},{1,0},{2,3},{3,2},{4,5},{5,4},{6,7},{7,6},{8,9},{9,8},{10,11... | collective-permute-start | bytes 49160 | tf_op jit(solution)/shard_map/ppermute | solution.py:423
  9.9 1.2 %copy-start.13 = (bf16[256,32]{0,1:T(8,128)(2,1)S(1)}, bf16[256,32]{0,1:T(8,128)(2,1)}, u32[]{:S(2)}) copy-start(bf16[256,32]{0,1:T(8,128)(2,1)} %param.23) | copy-start | bytes 49156
  9.9 6.2 %copy-start.5 = (bf16[1,512,512]{2,1,0:T(8,128)(2,1)S(1)}, bf16[1,512,512]{2,1,0:T(8,128)(2,1)}, u32[]{:S(2)}) copy-start(bf16[1,512,512]{2,1,0:T(8,128)(2,1)} %param.24) | copy-start | bytes 1572868
  9.9 6.2 %copy-start.12 = (bf16[1,512,32]{1,2,0:T(8,128)(2,1)S(1)}, bf16[1,512,32]{1,2,0:T(8,128)(2,1)}, u32[]{:S(2)}) copy-start(bf16[1,512,32]{1,2,0:T(8,128)(2,1)} %param.25) | copy-start | bytes 98308
  11.1 7.7 %copy-start.1 = (bf16[8,64,2048]{2,1,0:T(8,128)(2,1)S(1)}, bf16[8,64,2048]{2,1,0:T(8,128)(2,1)}, u32[]{:S(2)}) copy-start(bf16[8,64,2048]{2,1,0:T(8,128)(2,1)} %param.35) | copy-start | bytes 6291460
  11.1 7.7 %copy-start.7 = (bf16[128,1024]{1,0:T(8,128)(2,1)S(1)}, bf16[128,1024]{1,0:T(8,128)(2,1)}, u32[]{:S(2)}) copy-start(bf16[128,1024]{1,0:T(8,128)(2,1)} %constant.11.clone.chosen_ref) | copy-start | bytes 786436
  12.0 5.8 %collective-permute-start.3 = (bf16[16,640]{1,0:T(8,128)(2,1)S(1)}, bf16[16,640]{1,0:T(8,128)(2,1)S(1)}, u32[]{:S(2)}, u32[]{:S(2)}) collective-permute-start(bf16[16,640]{1,0:T(8,128)(2,1)S(1)} %get-tuple-element.43), channel_id=1, source_target_pairs={{0,2},{2,4},{4,6},{6,0},{1,3},{3,5},{5,7},{7,1},{8,10},{10,12},{12... | collective-permute-start | bytes 61448 | tf_op jit(solution)/shard_map/ppermute | solution.py:423
  12.1 5.7 %collective-permute-start.4 = (bf16[16,640]{1,0:T(8,128)(2,1)S(1)}, bf16[16,640]{1,0:T(8,128)(2,1)S(1)}, u32[]{:S(2)}, u32[]{:S(2)}) collective-permute-start(bf16[16,640]{1,0:T(8,128)(2,1)S(1)} %get-tuple-element.44), channel_id=1, source_target_pairs={{0,4},{2,6},{4,0},{6,2},{1,5},{3,7},{5,1},{7,3},{8,12},{10,14},{12... | collective-permute-start | bytes 61448 | tf_op jit(solution)/shard_map/ppermute | solution.py:423
  15.0 3.8 %collective-permute-start.5 = (bf16[16,640]{1,0:T(8,128)(2,1)S(1)}, bf16[16,640]{1,0:T(8,128)(2,1)S(1)}, u32[]{:S(2)}, u32[]{:S(2)}) collective-permute-start(bf16[16,640]{1,0:T(8,128)(2,1)S(1)} %get-tuple-element.45), channel_id=1, source_target_pairs={{0,6},{2,0},{4,2},{6,4},{1,7},{3,1},{5,3},{7,5},{8,14},{10,8},{12,... | collective-permute-start | bytes 61448 | tf_op jit(solution)/shard_map/ppermute | solution.py:423
  19.4 1.3 %collective-permute-start.6 = (bf16[24,2048]{1,0:T(8,128)(2,1)S(1)}, bf16[24,2048]{1,0:T(8,128)(2,1)S(1)}, u32[]{:S(2)}, u32[]{:S(2)}) collective-permute-start(bf16[24,2048]{1,0:T(8,128)(2,1)S(1)} %combine.1.refs_0_), channel_id=1, source_target_pairs={{0,1},{1,0},{2,3},{3,2},{4,5},{5,4},{6,7},{7,6},{8,9},{9,8},{10,11... | collective-permute-start | bytes 294920 | tf_op jit(solution)/shard_map/ppermute | solution.py:423
